TPU v7x, 32 devices: a whole 2x2x4 slice. The times are simulated.
32 devices in a mesh: rep: 2 (over x), fs: 4 (over z), tp: 4 (over y, core).
Axes of the slice: x: 2, y: 2, z: 4, core: 2. Of those that a mesh axis runs over, the one named last changes fastest.
Arguments:
- tokens: bfloat16 [3072, 2048], P(('rep', 'fs'), 'tp'), may hold values from -6 to 6
- norm_gain: bfloat16 [2048], replicated, may hold values from 0.099609375 to 1.8984375
- w_gate: bfloat16 [2048, 5120], P('fs', 'tp'), may hold values from -0.125 to 0.125
- w_up: bfloat16 [2048, 5120], P('fs', 'tp'), may hold values from -0.125 to 0.125
- w_down: bfloat16 [5120, 2048], P('tp', 'fs'), may hold values from -0.078125 to 0.078125
- cotangent: bfloat16 [3072, 2048], P(('rep', 'fs'), 'tp'), may hold values from -6 to 6
Outputs:
- grad_tokens: bfloat16 [3072, 2048], P(('rep', 'fs'), 'tp')
- grad_gain: float32 [2048], P('tp')
- grad_gate: float32 [2048, 5120], P('fs', 'tp')
- grad_up: float32 [2048, 5120], P('fs', 'tp')
- grad_down: float32 [5120, 2048], P('tp', 'fs')
- gate_up_sq: float32 [2, 2048], P(None, 'fs')
- down_sq: float32 [5120], P('tp')
All inputs are finite; a program needn't handle non-finite values.
Results may differ from a plain program's by a relative error of at most 0.018.
Values may be sent and summed in bfloat16 or wider, within the bound.
A program may use at most 128 MiB of HBM per device.

v0:
```python
import functools

import jax
import jax.numpy as jnp
from jax import lax
from jax.experimental import pallas as pl
from jax.experimental.pallas import tpu as pltpu
from jax.sharding import PartitionSpec as P

MESH = pl.DeviceIdType.MESH


def contract_last(left, right):
    return lax.dot_general(
        left, right, (((1,), (1,)), ((), ())), preferred_element_type=jnp.float32
    )


def contract_first(left, right):
    return lax.dot_general(
        left, right, (((0,), (0,)), ((), ())), preferred_element_type=jnp.float32
    )


def remote(source, target, send_sem, recv_sem, where):
    return pltpu.make_async_remote_copy(
        src_ref=source,
        dst_ref=target,
        send_sem=send_sem,
        recv_sem=recv_sem,
        device_id=where,
        device_id_type=MESH,
    )


def line_sends(z, n_fs, side, d):
    if side == 0:
        return jnp.logical_and(z >= d - 1, z <= n_fs - 2)
    return jnp.logical_and(z + d <= n_fs, z >= 1)


def line_receives(z, n_fs, side, d):
    return z >= d if side == 0 else z + d <= n_fs - 1


def greet(peers):
    barrier = pltpu.get_barrier_semaphore()
    for peer in peers:
        pl.semaphore_signal(barrier, inc=1, device_id=peer, device_id_type=MESH)
    pl.semaphore_wait(barrier, len(peers))


def keep_own(sources, holders, targets, sems):
    count = len(sources)
    loads = [
        pltpu.make_async_copy(sources[i], holders[i], sems.at[0, i]) for i in range(count)
    ]
    stores = [
        pltpu.make_async_copy(holders[i], targets[i], sems.at[1, i]) for i in range(count)
    ]
    for load in loads:
        load.start()

    def finish():
        for load, store in zip(loads, stores):
            load.wait()
            store.start()
        for store in stores:
            store.wait()

    return finish


def weights_kernel(n_fs, n_tp, *refs):
    tokens, cot, w_gate, w_up, w_down = refs[:5]
    whole_x, whole_dy, full_gate, full_up, full_down = refs[5:10]
    holders = refs[10:15]
    own_sem, ring_send, ring_recv, rep_send, rep_recv, tp_send, tp_recv = refs[15:]
    r, z, t = lax.axis_index("rep"), lax.axis_index("fs"), lax.axis_index("tp")
    right, left = lax.rem(z + 1, n_fs), lax.rem(z + n_fs - 1, n_fs)
    partner = {"rep": 1 - r}
    sources = (w_gate, w_up, w_down)
    targets = (full_gate, full_up, full_down)
    rows = w_gate.shape[0]
    hidden = w_down.shape[0]
    local = tokens.shape[1]

    def own_piece(m, half):
        size = (hidden if m == 2 else rows) // 2
        return sources[m].at[pl.ds(pl.multiple_of(half * size, size), size), :]

    def piece(m, owner, half):
        if m == 2:
            size = hidden // 2
            return targets[m].at[
                pl.ds(pl.multiple_of(half * size, size), size),
                pl.ds(pl.multiple_of(owner * rows, rows), rows),
            ]
        size = rows // 2
        return targets[m].at[
            pl.ds(pl.multiple_of(owner * rows + half * size, size), size), :
        ]

    peers = [{"fs": right}, {"fs": left}, partner]
    peers += [{"tp": lax.rem(t + j, n_tp)} for j in range(1, n_tp)]
    greet(peers)

    def owner_of(side, back):
        return lax.rem(z + (n_fs - back if side == 0 else back), n_fs)

    def hop(m, side, d):
        place = piece(m, owner_of(side, d - 1), r)
        return remote(
            own_piece(m, r) if d == 1 else place,
            place,
            ring_send.at[m, side, d - 1],
            ring_recv.at[m, side, d - 1],
            {"fs": right if side == 0 else left},
        )

    def arrival(m, side, d):
        place = piece(m, owner_of(side, d), r)
        return remote(
            place,
            place,
            ring_send.at[m, side, d - 1],
            ring_recv.at[m, side, d - 1],
            {"fs": right if side == 0 else left},
        )

    def across(m, side, d):
        place = piece(m, owner_of(side, d), r)
        return remote(
            place, place, rep_send.at[m, side, d - 1], rep_recv.at[m, side, d - 1], partner
        )

    for m in range(3):
        for side in range(2):

            @pl.when(line_sends(z, n_fs, side, 1))
            def _():
                hop(m, side, 1).start()

    ends = []
    for a, (source, target) in enumerate(((tokens, whole_x), (cot, whole_dy))):
        place = target.at[:, pl.ds(pl.multiple_of(t * local, local), local)]
        for j in range(1, n_tp):
            copy = remote(
                source,
                place,
                tp_send.at[a, j - 1],
                tp_recv.at[a, j - 1],
                {"tp": lax.rem(t + j, n_tp)},
            )
            copy.start()
            ends.append(copy)
    mine = pl.ds(pl.multiple_of(t * local, local), local)
    band = pl.ds(pl.multiple_of(z * rows, rows), rows)
    finish = keep_own(
        (tokens, cot, w_gate, w_up, w_down),
        holders,
        (
            whole_x.at[:, mine],
            whole_dy.at[:, mine],
            full_gate.at[band, :],
            full_up.at[band, :],
            full_down.at[:, band],
        ),
        own_sem,
    )
    finish()
    for d in range(1, n_fs):
        for m in range(3):
            for side in range(2):

                @pl.when(line_receives(z, n_fs, side, d))
                def _():
                    arrival(m, side, d).wait_recv()
                    if d < n_fs - 1:

                        @pl.when(line_sends(z, n_fs, side, d + 1))
                        def _():
                            hop(m, side, d + 1).start()

                    across(m, side, d).start()

    for d in range(1, n_fs):
        for m in range(3):
            for side in range(2):

                @pl.when(line_sends(z, n_fs, side, d))
                def _():
                    hop(m, side, d).wait_send()

                @pl.when(line_receives(z, n_fs, side, d))
                def _():
                    across(m, side, d).wait()

    for copy in ends:
        copy.wait()


def gather_weights(n_fs, n_tp, tokens, cot, w_gate, w_up, w_down):
    count, local = tokens.shape
    rows, hidden = w_gate.shape
    width = rows * n_fs
    dtype = tokens.dtype
    shapes = [
        (count, width),
        (count, width),
        (width, hidden),
        (width, hidden),
        (hidden, width),
    ]
    held = (tokens, cot, w_gate, w_up, w_down)
    moved = sum(2 * a * b for a, b in shapes)
    dma = pltpu.SemaphoreType.DMA
    return pl.pallas_call(
        functools.partial(weights_kernel, n_fs, n_tp),
        out_shape=[jax.ShapeDtypeStruct(s, dtype) for s in shapes],
        in_specs=[pl.BlockSpec(memory_space=pl.ANY)] * 5,
        out_specs=[pl.BlockSpec(memory_space=pl.ANY)] * 5,
        scratch_shapes=[pltpu.VMEM(a.shape, a.dtype) for a in held]
        + [
            dma((2, 5)),
            dma((3, 2, n_fs - 1)),
            dma((3, 2, n_fs - 1)),
            dma((3, 2, n_fs - 1)),
            dma((3, 2, n_fs - 1)),
            dma((2, n_tp - 1)),
            dma((2, n_tp - 1)),
        ],
        compiler_params=pltpu.CompilerParams(collective_id=0, has_side_effects=True),
        cost_estimate=pl.CostEstimate(flops=0, bytes_accessed=16 * moved, transcendentals=0),
        name="gather_weights",
    )(*held)


def tokens_kernel(n_fs, n_tp, n_act, n_swap, *refs):
    total = n_act + n_swap
    acts, swaps = refs[:n_act], refs[n_act:total]
    act_outs, swap_outs = refs[total : total + n_act], refs[total + n_act : 2 * total]
    holders = refs[2 * total : 3 * total]
    own_sem, ring_send, ring_recv = refs[3 * total : 3 * total + 3]
    swap_send, swap_recv, relay_send, relay_recv = refs[3 * total + 3 :]
    z, t = lax.axis_index("fs"), lax.axis_index("tp")
    right, left = lax.rem(z + 1, n_fs), lax.rem(z + n_fs - 1, n_fs)
    count = acts[0].shape[0]
    peers = [{"fs": lax.rem(z + j, n_fs)} for j in range(1, n_fs)]
    if n_swap:
        peers += [{"tp": lax.rem(t + j, n_tp)} for j in range(1, n_tp)]
    greet(peers)

    def rows_of(owner):
        return pl.ds(pl.multiple_of(owner * count, count), count)

    def owner_of(side, back):
        return lax.rem(z + (n_fs - back if side == 0 else back), n_fs)

    def hop(m, side, d):
        place = act_outs[m].at[rows_of(owner_of(side, d - 1)), :]
        return remote(
            acts[m] if d == 1 else place,
            place,
            ring_send.at[m, side, d - 1],
            ring_recv.at[m, side, d - 1],
            {"fs": right if side == 0 else left},
        )

    def arrival(m, side, d):
        place = act_outs[m].at[rows_of(owner_of(side, d)), :]
        return remote(
            place,
            place,
            ring_send.at[m, side, d - 1],
            ring_recv.at[m, side, d - 1],
            {"fs": right if side == 0 else left},
        )

    def swap(a, j):
        peer = lax.rem(z + j, n_fs)
        cut = swap_outs[a].shape[1]
        return remote(
            swaps[a].at[:, pl.ds(pl.multiple_of(peer * cut, cut), cut)],
            swap_outs[a].at[rows_of(z), :],
            swap_send.at[a, j - 1],
            swap_recv.at[a, j - 1],
            {"fs": peer},
        )

    def swapped(a, j):
        place = swap_outs[a].at[rows_of(owner_of(0, j)), :]
        return remote(
            place,
            place,
            swap_send.at[a, j - 1],
            swap_recv.at[a, j - 1],
            {"fs": lax.rem(z + j, n_fs)},
        )

    def relay(a, j, k):
        place = swap_outs[a].at[rows_of(owner_of(0, j)), :]
        return remote(
            place,
            place,
            relay_send.at[a, j - 1, k - 1],
            relay_recv.at[a, j - 1],
            {"tp": lax.rem(t + k, n_tp)},
        )

    hub = lax.rem(z, n_tp) == t

    def feeds(j):
        return lax.rem(lax.rem(z + j, n_fs), n_tp) == t

    for a in range(n_swap):
        for j in range(1, n_fs):

            @pl.when(feeds(j))
            def _():
                swap(a, j).start()

    for m in range(n_act):
        for side in range(2):

            @pl.when(line_sends(z, n_fs, side, 1))
            def _():
                hop(m, side, 1).start()

    sources = list(acts)
    for a in range(n_swap):
        cut = swap_outs[a].shape[1]
        sources.append(swaps[a].at[:, pl.ds(pl.multiple_of(z * cut, cut), cut)])
    finish = keep_own(
        sources, holders, [out.at[rows_of(z), :] for out in act_outs + swap_outs], own_sem
    )
    finish()
    if n_swap:

        @pl.when(hub)
        def _():
            for a in range(n_swap):
                for j in range(1, n_fs):
                    swapped(a, j).wait_recv()
                    for k in range(1, n_tp):
                        relay(a, j, k).start()

    for d in range(1, n_fs):
        for m in range(n_act):
            for side in range(2):

                @pl.when(line_receives(z, n_fs, side, d))
                def _():
                    arrival(m, side, d).wait_recv()
                    if d < n_fs - 1:

                        @pl.when(line_sends(z, n_fs, side, d + 1))
                        def _():
                            hop(m, side, d + 1).start()

    for d in range(1, n_fs):
        for m in range(n_act):
            for side in range(2):

                @pl.when(line_sends(z, n_fs, side, d))
                def _():
                    hop(m, side, d).wait_send()

    for a in range(n_swap):
        for j in range(1, n_fs):

            @pl.when(feeds(j))
            def _():
                swap(a, j).wait_send()

            @pl.when(hub)
            def _():
                for k in range(1, n_tp):
                    relay(a, j, k).wait_send()

            @pl.when(jnp.logical_not(hub))
            def _():
                relay(a, j, 1).wait_recv()


def gather_tokens(n_fs, n_tp, collective_id, acts, swaps):
    count = acts[0].shape[0]
    outs = [jax.ShapeDtypeStruct((n_fs * count, a.shape[1]), a.dtype) for a in acts]
    outs += [jax.ShapeDtypeStruct((n_fs * count, a.shape[1] // n_fs), a.dtype) for a in swaps]
    dma = pltpu.SemaphoreType.DMA
    total = len(outs)
    n_swap = max(len(swaps), 1)
    moved = sum(2 * o.shape[0] * o.shape[1] for o in outs)
    return pl.pallas_call(
        functools.partial(tokens_kernel, n_fs, n_tp, len(acts), len(swaps)),
        out_shape=outs,
        in_specs=[pl.BlockSpec(memory_space=pl.ANY)] * total,
        out_specs=[pl.BlockSpec(memory_space=pl.ANY)] * total,
        scratch_shapes=[pltpu.VMEM((count, o.shape[1]), o.dtype) for o in outs]
        + [
            dma((2, total)),
            dma((len(acts), 2, n_fs - 1)),
            dma((len(acts), 2, n_fs - 1)),
            dma((n_swap, n_fs - 1)),
            dma((n_swap, n_fs - 1)),
            dma((n_swap, n_fs - 1, n_tp - 1)),
            dma((n_swap, n_fs - 1)),
        ],
        compiler_params=pltpu.CompilerParams(
            collective_id=collective_id, has_side_effects=True
        ),
        cost_estimate=pl.CostEstimate(flops=0, bytes_accessed=16 * moved, transcendentals=0),
        name=f"gather_tokens_{collective_id}",
    )(*acts, *swaps)


def over_rep(part):
    part = part.astype(jnp.bfloat16)
    n_rep = lax.axis_size("rep")
    other = lax.ppermute(part, "rep", [(i, (i + 1) % n_rep) for i in range(n_rep)])
    return part, other


def added(pair):
    return pair[0].astype(jnp.float32) + pair[1].astype(jnp.float32)


def on_device(tokens, norm_gain, w_gate, w_up, w_down, cotangent):
    n_fs, n_tp = lax.axis_size("fs"), lax.axis_size("tp")
    whole_x, whole_dy, full_gate, full_up, full_down = gather_weights(
        n_fs, n_tp, tokens, cotangent, w_gate, w_up, w_down
    )
    width = whole_x.shape[1]
    wide_tokens = whole_x.astype(jnp.float32)
    gain_f = norm_gain.astype(jnp.float32)
    inverse = lax.rsqrt(jnp.mean(wide_tokens * wide_tokens, axis=-1, keepdims=True) + 1e-06)
    normed = (wide_tokens * inverse * gain_f).astype(jnp.bfloat16)
    gate = jnp.dot(normed, full_gate, preferred_element_type=jnp.float32)
    up_proj = jnp.dot(normed, full_up, preferred_element_type=jnp.float32)
    sigma = jax.nn.sigmoid(gate)
    active = gate * sigma
    hidden = (active * up_proj).astype(jnp.bfloat16)
    back = 0.5 * contract_last(whole_dy, full_down)
    d_up = (back * active).astype(jnp.bfloat16)
    d_gate = (back * up_proj * sigma * (1.0 + gate * (1.0 - sigma))).astype(jnp.bfloat16)

    all_hidden, rows_dy = gather_tokens(n_fs, n_tp, 1, [hidden], [whole_dy])
    down_pair = over_rep(0.5 * contract_first(all_hidden, rows_dy))

    partial_normed = contract_last(d_gate, full_gate) + contract_last(d_up, full_up)
    d_normed = lax.psum_scatter(
        partial_normed.astype(jnp.bfloat16), "tp", scatter_dimension=1, tiled=True
    ).astype(jnp.float32)

    all_gate, rows_normed = gather_tokens(n_fs, n_tp, 2, [d_gate], [normed])
    gate_pair = over_rep(contract_first(rows_normed, all_gate))
    (all_up,) = gather_tokens(n_fs, n_tp, 3, [d_up], [])
    up_pair = over_rep(contract_first(rows_normed, all_up))

    local_width = d_normed.shape[1]
    local_gain = lax.dynamic_slice_in_dim(
        gain_f, lax.axis_index("tp") * local_width, local_width, 0
    )
    local_tokens = tokens.astype(jnp.float32)
    scaled_grad = d_normed * local_gain
    rowdot = lax.psum(jnp.sum(scaled_grad * local_tokens, axis=-1), "tp")
    grad_tokens = (
        cotangent.astype(jnp.float32)
        + inverse * scaled_grad
        - local_tokens * inverse**3 * rowdot[:, None] / width
    ).astype(jnp.bfloat16)
    grad_gain = lax.psum(jnp.sum(d_normed * local_tokens * inverse, axis=0), ("rep", "fs"))

    grad_down = added(down_pair)
    down_sq = lax.psum(jnp.sum(grad_down * grad_down, axis=1), "fs")
    grad_gate = added(gate_pair)
    grad_up = added(up_pair)
    gate_up_sq = lax.psum(
        jnp.stack([jnp.sum(grad_gate * grad_gate, axis=1), jnp.sum(grad_up * grad_up, axis=1)]),
        "tp",
    )
    return (grad_tokens, grad_gain, grad_gate, grad_up, grad_down, gate_up_sq, down_sq)


def solution(mesh):
    placed = (
        P(("rep", "fs"), "tp"),
        P(),
        P("fs", "tp"),
        P("fs", "tp"),
        P("tp", "fs"),
        P(("rep", "fs"), "tp"),
    )
    return jax.shard_map(
        on_device,
        mesh=mesh,
        in_specs=placed,
        out_specs=(
            P(("rep", "fs"), "tp"),
            P("tp"),
            P("fs", "tp"),
            P("fs", "tp"),
            P("tp", "fs"),
            P(None, "fs"),
            P("tp"),
        ),
        check_vma=False,
    )
```

profile of v0, /device:TPU:0, one launch (start us, length us, event | category | flops | bytes accessed | tf_op | source)
XLA Modules:
  0.0 500.0 jit_solution(8675198434028722563)
XLA Ops:
  7.2 0.0 reduce-scatter.2.cloned.1.call-start
  7.2 0.7 convert_element_type.62
  7.9 149.3 %gather_weights.1 = (bf16[384,2048]{1,0:T(8,128)(2,1)}, bf16[384,2048]{1,0:T(8,128)(2,1)}, bf16[2048,1280]{1,0:T(8,128)(2,1)}, bf16[2048,1280]{1,0:T(8,128)(2,1)}, bf16[1280,2048]{1,0:T(8,128)(2,1)}) custom-call(bf16[384,512]{1,0:T(8,128)(2,1)} %refs_0_.1, bf16[384,512]{1,0:T(8,128)(2,1)} %refs_1_.1, bf16[512,1280]{1,0:T(8,128)(2,1)} %refs_2_.1, ...), custom_call_target="tpu_custom_call" | custom-call | bytes 301989888 | tf_op jit(solution)/shard_map/gather_weights/pallas_call | solution.py:218
  157.2 1.9 fusion
  159.2 5.3 %convolution_multiply_fusion.1 = f32[384,1280]{1,0:T(8,128)S(1)} fusion(bf16[384,2048]{1,0:T(8,128)(2,1)} %get-tuple-element.17.refs_1_, bf16[1280,2048]{1,0:T(8,128)(2,1)} %get-tuple-element.18), kind=kOutput, calls=%fused_computation.7 | convolution fusion | flops 2013757440 | bytes 8781824 | tf_op jit(solution)/shard_map/dot_general | solution.py:14
  164.6 0.4 fusion.2.refs_1_
  165.1 2.2 fusion.14
  167.3 0.0 slice-done
  167.3 0.3 slice-done.1
  167.6 3.7 multiply_convert_fusion
  171.4 2.2 fusion.15
  173.6 3.4 add_convert_fusion
  177.0 84.5 %gather_tokens_1.1 = (bf16[1536,1280]{1,0:T(8,128)(2,1)}, bf16[1536,512]{1,0:T(8,128)(2,1)}) custom-call(bf16[384,1280]{1,0:T(8,128)(2,1)} %get-tuple-element.40.refs_0_, bf16[384,2048]{1,0:T(8,128)(2,1)} %get-tuple-element.17.refs_1_), custom_call_target="tpu_custom_call" | custom-call | bytes 88080384 | tf_op jit(solution)/shard_map/gather_tokens_1/pallas_call | solution.py:394
  261.5 4.8 fusion.3
  266.4 0.6 collective-permute-start.2
  267.0 85.9 %gather_tokens_2.1 = (bf16[1536,1280]{1,0:T(8,128)(2,1)}, bf16[1536,512]{1,0:T(8,128)(2,1)}) custom-call(bf16[384,1280]{1,0:T(8,128)(2,1)} %copy-done.6, bf16[384,2048]{1,0:T(8,128)(2,1)} %copy-done), custom_call_target="tpu_custom_call" | custom-call | bytes 88080384 | tf_op jit(solution)/shard_map/gather_tokens_2/pallas_call | solution.py:394
  352.9 5.9 %convolution_convert_fusion.1 = bf16[512,1280]{1,0:T(8,128)(2,1)} fusion(bf16[1536,512]{1,0:T(8,128)(2,1)} %get-tuple-element.21, bf16[1536,1280]{1,0:T(8,128)(2,1)} %get-tuple-element.22), kind=kOutput, calls=%fused_computation.10 | convolution fusion | flops 2013921280 | bytes 6815744 | tf_op jit(solution)/shard_map/dot_general | solution.py:20
  358.8 1.5 collective-permute-start
  360.3 65.5 %gather_tokens_3.1 = bf16[1536,1280]{1,0:T(8,128)(2,1)} custom-call(bf16[384,1280]{1,0:T(8,128)(2,1)} %copy-done.5), custom_call_target="tpu_custom_call" | custom-call | bytes 62914560 | tf_op jit(solution)/shard_map/gather_tokens_3/pallas_call | solution.py:394
  425.9 5.5 %convolution_convert_fusion = bf16[512,1280]{1,0:T(8,128)(2,1)} fusion(bf16[1536,512]{1,0:T(8,128)(2,1)S(1)} %copy-done.8, bf16[1536,1280]{1,0:T(8,128)(2,1)} %gather_tokens_3.1), kind=kOutput, calls=%fused_computation.9 | convolution fusion | flops 2013921280 | bytes 6815744 | tf_op jit(solution)/shard_map/dot_general | solution.py:20
  431.4 0.5 collective-permute-start.1
  431.9 0.1 dynamic_slice.3
  432.0 2.2 multiply_reduce_fusion
  434.1 2.1 copy.13
  436.2 10.9 %psum.31 = f32[1280]{0:T(1024)} all-reduce(f32[1280]{0:T(1024)S(1)} %get-tuple-element.43), channel_id=1, replica_groups=mesh['rep'=2,'fs'=4,'tp'=4] {'fs'}, use_global_device_ids=true, to_apply=%region_10.0 | all-reduce | flops 1280 | bytes 10240 | tf_op jit(solution)/shard_map/psum | solution.py:475
  447.2 3.6 multiply_reduce_fusion.2
  450.8 8.4 %collective-permute-done.1 = bf16[512,1280]{1,0:T(8,128)(2,1)} collective-permute-done((bf16[512,1280]{1,0:T(8,128)(2,1)}, bf16[512,1280]{1,0:T(8,128)(2,1)}, u32[]{:S(2)}, u32[]{:S(2)}) %collective-permute-start.1) | collective-permute-done | bytes 1310752 | tf_op jit(solution)/shard_map/ppermute | solution.py:420
  459.2 3.6 multiply_reduce_fusion.1
  462.9 1.4 fusion.13
  464.2 20.5 %psum.29 = f32[512]{0:T(512)} all-reduce(f32[512]{0:T(512)S(1)} %get-tuple-element.32), channel_id=1, replica_groups=mesh['rep'=2,'fs'=4,'tp'=4] {'rep','fs'}, use_global_device_ids=true, to_apply=%region_5.0 | all-reduce | flops 512 | bytes 4096 | tf_op jit(solution)/shard_map/psum | solution.py:472
  484.7 6.4 %all-reduce = (f32[384]{0:T(512)S(1)}, f32[2,512]{1,0:T(2,128)}) all-reduce(f32[384]{0:T(512)S(1)} %get-tuple-element.33, f32[2,512]{1,0:T(2,128)S(1)} %pad_maximum_fusion), channel_id=1, replica_groups=mesh['rep'=2,'fs'=4,'tp'=4] {'tp'}, use_global_device_ids=true, to_apply=%region_3.0 | all-reduce | flops 1408 | bytes 11264 | tf_op jit(solution)/shard_map/psum | solution.py:466
  491.1 2.1 fusion.8
  (32 shorter events, 0.1 us)
Async XLA Ops:
  7.2 455.7 %reduce-scatter.2.cloned.1.call-start = ((), (), s32[]{:S(2)}) async-start(), calls=%async_computation.1 | async-start | bytes 1966080 | tf_op jit(solution)/shard_map/reduce_scatter | solution.py:451
  157.2 7.8 %slice-start.2 = ((s8[5242880]{0:T(1024)(128)(4,1)}), s8[4194304]{0:T(1024)(128)(4,1)S(1)}, s32[]{:S(2)}) async-start(s8[5242880]{0:T(1024)(128)(4,1)} %bitcast.22), calls=%async_computation.4 | async-start | bytes 8388608
  159.2 5.4 %copy-start.1 = (bf16[384,2048]{1,0:T(8,128)(2,1)S(1)}, bf16[384,2048]{1,0:T(8,128)(2,1)}, u32[]{:S(2)}) copy-start(bf16[384,2048]{1,0:T(8,128)(2,1)} %get-tuple-element.16) | copy-start | bytes 4718596
  159.2 5.8 %slice-start.3 = ((s8[5242880]{0:T(1024)(128)(4,1)}), s8[1048576]{0:T(1024)(128)(4,1)S(1)}, s32[]{:S(2)}) async-start(s8[5242880]{0:T(1024)(128)(4,1)} %bitcast.22), calls=%async_computation.5 | async-start | bytes 2097152
  164.6 2.8 slice-start
  165.0 2.3 copy-start
  165.1 2.6 slice-start.1
  171.4 2.2 copy-start.6
  171.4 2.2 copy-start.5
  266.4 92.5 %copy-start.4 = (bf16[1280,512]{0,1:T(8,128)(2,1)}, bf16[1280,512]{0,1:T(8,128)(2,1)S(1)}, u32[]{:S(2)}) copy-start(bf16[1280,512]{0,1:T(8,128)(2,1)S(1)} %fusion.3) | copy-start | bytes 3932164
  266.4 165.6 %collective-permute-start.2 = (bf16[1280,512]{0,1:T(8,128)(2,1)S(1)}, bf16[1280,512]{0,1:T(8,128)(2,1)}, u32[]{:S(2)}, u32[]{:S(2)}) collective-permute-start(bf16[1280,512]{0,1:T(8,128)(2,1)S(1)} %fusion.3), channel_id=1, source_target_pairs={{0,16},{16,0},{1,17},{17,1},{2,18},{18,2},{3,19},{19,3},{4,20},{20... | collective-permute-start | bytes 3932168 | tf_op jit(solution)/shard_map/ppermute | solution.py:420
  358.8 67.0 %copy-start.8 = (bf16[1536,512]{1,0:T(8,128)(2,1)S(1)}, bf16[1536,512]{1,0:T(8,128)(2,1)}, u32[]{:S(2)}) copy-start(bf16[1536,512]{1,0:T(8,128)(2,1)} %get-tuple-element.21) | copy-start | bytes 4718596
  358.8 88.4 %collective-permute-start = (bf16[512,1280]{1,0:T(8,128)(2,1)}, bf16[512,1280]{1,0:T(8,128)(2,1)}, u32[]{:S(2)}, u32[]{:S(2)}) collective-permute-start(bf16[512,1280]{1,0:T(8,128)(2,1)} %convolution_convert_fusion.1), channel_id=1, source_target_pairs={{0,16},{16,0},{1,17},{17,1},{2,18},{18,2},{3,19},{19,3},{4,20},{20... | collective-permute-start | bytes 3932168 | tf_op jit(solution)/shard_map/ppermute | solution.py:420
  425.9 6.0 %copy-start.7 = (bf16[2048]{0:T(1024)(128)(2,1)S(1)}, bf16[2048]{0:T(1024)(128)(2,1)}, u32[]{:S(2)}) copy-start(bf16[2048]{0:T(1024)(128)(2,1)} %param.7) | copy-start | bytes 12292
  431.4 27.8 %collective-permute-start.1 = (bf16[512,1280]{1,0:T(8,128)(2,1)}, bf16[512,1280]{1,0:T(8,128)(2,1)}, u32[]{:S(2)}, u32[]{:S(2)}) collective-permute-start(bf16[512,1280]{1,0:T(8,128)(2,1)} %convolution_convert_fusion), channel_id=1, source_target_pairs={{0,16},{16,0},{1,17},{17,1},{2,18},{18,2},{3,19},{19,3},{4,20},{20... | collective-permute-start | bytes 3932168 | tf_op jit(solution)/shard_map/ppermute | solution.py:420
  450.8 12.1 %copy-start.2 = (bf16[384,512]{1,0:T(8,128)(2,1)S(1)}, bf16[384,512]{1,0:T(8,128)(2,1)}, u32[]{:S(2)}) copy-start(bf16[384,512]{1,0:T(8,128)(2,1)} %refs_0_.1) | copy-start | bytes 1179652
  450.8 40.3 %copy-start.3 = (bf16[384,512]{1,0:T(8,128)(2,1)S(1)}, bf16[384,512]{1,0:T(8,128)(2,1)}, u32[]{:S(2)}) copy-start(bf16[384,512]{1,0:T(8,128)(2,1)} %refs_1_.1) | copy-start | bytes 1179652
Sparse Core Ops, SparseCore 0:
  177.1 27.0 reduce-scatter.1
where the time goes:
time: 501 us; the launch traced here: 500 us
  Pallas kernels  385 us (77%)
  blocking collectives  37.8 us (8%)
  matrix products  33.1 us (7%)
  other arithmetic  15.9 us (3%)
  between operations  14.3 us (3%)
  waiting for transfers between devices  8.43 us (2%)
    pallas_call x3, Pallas kernels, gather_tokens(): pl.pallas_call(functools.partial(tokens_kernel, n_fs, n_tp, len(acts), le...  236 us
    pallas_call x1, Pallas kernels, gather_weights(): pl.pallas_call(functools.partial(weights_kernel, n_fs, n_tp), out_shape=[...  149 us
    psum x1, blocking collectives, on_device(): lax.psum(jnp.sum(d_normed * local_tokens * inverse, axis=0), ('rep', 'fs'))  20.5 us
    dot_general x3, matrix products, contract_first(): lax.dot_general(left, right, (((0,), (0,)), ((), ())), preferred_element_...  16.2 us
    psum x1, blocking collectives, on_device(): down_sq = lax.psum(jnp.sum(grad_down * grad_down, axis=1), 'fs')  10.9 us
    dot_general x3, matrix products, contract_last(): lax.dot_general(left, right, (((1,), (1,)), ((), ())), preferred_element_...  10.9 us
  transfers between devices with their start and end apart: 4, of which 1 were waited for; matrix products, arithmetic and copies ran while one was open for 6% of the time, Pallas kernels for 47%

commit v1 on v0

--- a/solution.py
+++ b/solution.py
@@ -482,6 +482,814 @@
     return (grad_tokens, grad_gain, grad_gate, grad_up, grad_down, gate_up_sq, down_sq)
 
 
+CORES = 2
+
+
+def line_next(z, n_fs, side):
+    return z <= n_fs - 2 if side == 0 else z >= 1
+
+
+def pull_kernel(n_fs, *refs):
+    tokens, cot, w_gate, w_up, w_down = refs[:5]
+    outs = refs[5:10]
+    act_hold, weight_hold, down_hold = refs[10:13]
+    (own_sem, az_own, az_fwd, az_recv, ay_own, ay_fwd, ay_recv, ap_send, ap_recv) = refs[13:22]
+    (w_send, w_recv, wx_send, wx_recv, wp_send, wp_recv, wo_send, wo_recv) = refs[22:]
+    r, z, t = lax.axis_index("rep"), lax.axis_index("fs"), lax.axis_index("tp")
+    y, c = lax.div(t, CORES), lax.rem(t, CORES)
+    acts, weights = (tokens, cot), (w_gate, w_up, w_down)
+    half, local = tokens.shape[0] // CORES, tokens.shape[1]
+    rows = w_gate.shape[0]
+    kb = n_fs // CORES
+    width = w_gate.shape[1] // kb
+    partner = {"tp": y * CORES + 1 - c}
+    across = {"rep": 1 - r}
+    owner = lax.div(z, kb)
+
+    peers = [partner, across]
+    peers += [{"tp": (1 - y) * CORES + h} for h in range(CORES)]
+    for j in range(1, n_fs):
+        for h in range(CORES):
+            peers.append({"fs": lax.rem(z + j, n_fs), "tp": y * CORES + h})
+    greet(peers)
+
+    def own_act(a, h):
+        return acts[a].at[pl.ds(pl.multiple_of(h * half, half), half), :]
+
+    def act_place(a, source, column):
+        return outs[a].at[
+            pl.ds(pl.multiple_of(source * half, half), half),
+            pl.ds(pl.multiple_of(column * local, local), local),
+        ]
+
+    def source_of(side, d):
+        return z - d if side == 0 else z + d
+
+    def next_of(side):
+        return z + 1 if side == 0 else z - 1
+
+    def act_first(a, side, h):
+        return remote(
+            own_act(a, h),
+            act_place(a, z, t),
+            az_own.at[a, side, h],
+            az_recv.at[a, side, 0, c],
+            {"fs": next_of(side), "tp": y * CORES + h},
+        )
+
+    def act_arrival(a, side, d, core):
+        place = act_place(a, source_of(side, d), y * CORES + core)
+        return remote(
+            place, place, az_fwd.at[a, side, d - 1, core], az_recv.at[a, side, d - 1, core], partner
+        )
+
+    def act_forward(a, side, d, core):
+        place = act_place(a, source_of(side, d), y * CORES + core)
+        return remote(
+            place,
+            place,
+            az_fwd.at[a, side, d - 1, core],
+            az_recv.at[a, side, d, core],
+            {"fs": next_of(side)},
+        )
+
+    def act_over(a, side, d, core):
+        source = source_of(side, d)
+        place = act_place(a, source, y * CORES + core)
+        return remote(
+            place,
+            place,
+            ay_fwd.at[a, side, d - 1, core],
+            ay_recv.at[a, source, core],
+            {"tp": (1 - y) * CORES + c},
+        )
+
+    def act_over_own(a, h):
+        return remote(
+            own_act(a, h),
+            act_place(a, z, t),
+            ay_own.at[a, h],
+            ay_recv.at[a, z, c],
+            {"tp": (1 - y) * CORES + h},
+        )
+
+    def act_over_arrival(a, source, core):
+        place = act_place(a, source, (1 - y) * CORES + core)
+        return remote(place, place, ay_own.at[a, 0], ay_recv.at[a, source, core], partner)
+
+    def act_partner(a):
+        return remote(own_act(a, 1 - c), act_place(a, z, t), ap_send.at[a], ap_recv.at[a], partner)
+
+    def act_partner_arrival(a):
+        place = act_place(a, z, y * CORES + 1 - c)
+        return remote(place, place, ap_send.at[a], ap_recv.at[a], partner)
+
+    def block_of(m, k):
+        if m == 2:
+            return weights[m].at[pl.ds(pl.multiple_of(k * width, width), width), :]
+        return weights[m].at[:, pl.ds(pl.multiple_of(k * width, width), width)]
+
+    def band_of(m, source):
+        band = pl.ds(pl.multiple_of(source * rows, rows), rows)
+        return outs[2 + m].at[:, band] if m == 2 else outs[2 + m].at[band, :]
+
+    def quarter(m, source, rep, core):
+        if m == 2:
+            size = width // (2 * CORES)
+            return outs[4].at[
+                pl.ds(pl.multiple_of((rep * CORES + core) * size, size), size),
+                pl.ds(pl.multiple_of(source * rows, rows), rows),
+            ]
+        size = rows // (2 * CORES)
+        start = source * rows + (rep * CORES + core) * size
+        return outs[2 + m].at[pl.ds(pl.multiple_of(start, size), size), :]
+
+    def own_quarter(m, k, core):
+        if m == 2:
+            size = width // (2 * CORES)
+            start = k * width + (r * CORES + core) * size
+            return weights[m].at[pl.ds(pl.multiple_of(start, size), size), :]
+        size = rows // (2 * CORES)
+        return weights[m].at[
+            pl.ds(pl.multiple_of((r * CORES + core) * size, size), size),
+            pl.ds(k * width, width),
+        ]
+
+    def weight_send(m, k, core):
+        return remote(
+            own_quarter(m, k, core),
+            quarter(m, z, r, core),
+            w_send.at[m, k, core],
+            w_recv.at[m, z],
+            {"fs": kb * c + k, "tp": y * CORES + core},
+        )
+
+    def weight_arrival(m, source):
+        place = quarter(m, source, r, c)
+        return remote(place, place, wx_send.at[m, source], w_recv.at[m, source], partner)
+
+    def weight_across(m, source):
+        place = quarter(m, source, r, c)
+        return remote(place, place, wx_send.at[m, source], wx_recv.at[m, source], across)
+
+    def weight_across_arrival(m, source):
+        place = quarter(m, source, 1 - r, c)
+        return remote(place, place, wx_send.at[m, source], wx_recv.at[m, source], across)
+
+    def weight_beside(m, source, which):
+        place = quarter(m, source, r if which == 0 else 1 - r, c)
+        return remote(
+            place, place, wp_send.at[m, source, which], wp_recv.at[m, source, which], partner
+        )
+
+    def weight_beside_arrival(m, source, which):
+        place = quarter(m, source, r if which == 0 else 1 - r, 1 - c)
+        return remote(
+            place, place, wp_send.at[m, source, which], wp_recv.at[m, source, which], partner
+        )
+
+    def own_beside(m):
+        return remote(
+            block_of(m, z - kb * owner), band_of(m, z), wo_send.at[m], wo_recv.at[m], partner
+        )
+
+    def own_beside_arrival(m):
+        return remote(band_of(m, z), band_of(m, z), wo_send.at[m], wo_recv.at[m], partner)
+
+    for a in range(2):
+        for h in range(CORES):
+            for side in range(2):
+
+                @pl.when(line_next(z, n_fs, side))
+                def _():
+                    act_first(a, side, h).start()
+
+            act_over_own(a, h).start()
+    for a in range(2):
+        act_partner(a).start()
+
+    @pl.when(c == owner)
+    def _():
+        for m in range(3):
+            own_beside(m).start()
+
+    holders = [act_hold.at[0], act_hold.at[1]]
+    loads = [pltpu.make_async_copy(own_act(a, c), holders[a], own_sem.at[0, a]) for a in range(2)]
+    stores = [
+        pltpu.make_async_copy(holders[a], act_place(a, z, t), own_sem.at[1, a]) for a in range(2)
+    ]
+    for load in loads:
+        load.start()
+    for load, store in zip(loads, stores):
+        load.wait()
+        store.start()
+    for store in stores:
+        store.wait()
+
+    @pl.when(c == owner)
+    def _():
+        places = [weight_hold.at[0], weight_hold.at[1], down_hold]
+        loads = [
+            pltpu.make_async_copy(block_of(m, z - kb * owner), places[m], own_sem.at[0, 2 + m])
+            for m in range(3)
+        ]
+        stores = [
+            pltpu.make_async_copy(places[m], band_of(m, z), own_sem.at[1, 2 + m])
+            for m in range(3)
+        ]
+        for load in loads:
+            load.start()
+        for load, store in zip(loads, stores):
+            load.wait()
+            store.start()
+        for store in stores:
+            store.wait()
+
+    def act_round(d):
+        for a in range(2):
+            for core in range(CORES):
+                for side in range(2):
+
+                    @pl.when(line_receives(z, n_fs, side, d))
+                    def _():
+                        act_arrival(a, side, d, core).wait_recv()
+                        if d < n_fs - 1:
+
+                            @pl.when(line_next(z, n_fs, side))
+                            def _():
+                                act_forward(a, side, d, core).start()
+
+                        act_over(a, side, d, core).start()
+
+    def weight_round(d):
+        for m in range(3):
+            for side in range(2):
+
+                @pl.when(line_receives(z, n_fs, side, d))
+                def _():
+                    source = source_of(side, d)
+                    weight_arrival(m, source).wait_recv()
+                    weight_across(m, source).start()
+                    weight_beside(m, source, 0).start()
+
+    def across_round(d):
+        for m in range(3):
+            for side in range(2):
+
+                @pl.when(line_receives(z, n_fs, side, d))
+                def _():
+                    source = source_of(side, d)
+                    weight_across_arrival(m, source).wait_recv()
+                    weight_beside(m, source, 1).start()
+
+    act_round(1)
+    for m in range(3):
+        for k in range(kb):
+
+            @pl.when(kb * c + k != z)
+            def _():
+                for core in range(CORES):
+                    weight_send(m, k, core).start()
+
+    for d in range(1, n_fs):
+        if d + 1 < n_fs:
+            act_round(d + 1)
+        weight_round(d)
+        if d > 1:
+            across_round(d - 1)
+    across_round(n_fs - 1)
+
+    for d in range(1, n_fs):
+        for side in range(2):
+
+            @pl.when(line_receives(z, n_fs, side, d))
+            def _():
+                source = source_of(side, d)
+                for a in range(2):
+                    for core in range(CORES):
+                        act_over_arrival(a, source, core).wait_recv()
+                        act_over(a, side, d, core).wait_send()
+                        if d < n_fs - 1:
+
+                            @pl.when(line_next(z, n_fs, side))
+                            def _():
+                                act_forward(a, side, d, core).wait_send()
+
+                for m in range(3):
+                    weight_across(m, source).wait_send()
+                    for which in range(2):
+                        weight_beside_arrival(m, source, which).wait_recv()
+                        weight_beside(m, source, which).wait_send()
+
+    for a in range(2):
+        act_partner_arrival(a).wait_recv()
+        act_partner(a).wait_send()
+        for h in range(CORES):
+            act_over_arrival(a, z, h).wait_recv()
+            act_over_own(a, h).wait_send()
+            for side in range(2):
+
+                @pl.when(line_next(z, n_fs, side))
+                def _():
+                    act_first(a, side, h).wait_send()
+
+    for m in range(3):
+        for k in range(kb):
+
+            @pl.when(kb * c + k != z)
+            def _():
+                for core in range(CORES):
+                    weight_send(m, k, core).wait_send()
+
+    @pl.when(c == owner)
+    def _():
+        for m in range(3):
+            own_beside(m).wait_send()
+
+    @pl.when(c != owner)
+    def _():
+        for m in range(3):
+            own_beside_arrival(m).wait_recv()
+
+
+def pull(n_fs, n_tp, tokens, cot, w_gate, w_up, w_down):
+    half, local = tokens.shape[0] // CORES, tokens.shape[1]
+    rows, hidden = w_gate.shape
+    width = hidden * CORES // n_fs
+    model = rows * n_fs
+    dtype = tokens.dtype
+    shapes = [(half * n_fs, model)] * 2 + [(model, width)] * 2 + [(width, model)]
+    dma = pltpu.SemaphoreType.DMA
+    kb = n_fs // CORES
+    line = (2, 2, n_fs - 1, CORES)
+    return pl.pallas_call(
+        functools.partial(pull_kernel, n_fs),
+        out_shape=[jax.ShapeDtypeStruct(s, dtype) for s in shapes],
+        in_specs=[pl.BlockSpec(memory_space=pl.ANY)] * 5,
+        out_specs=[pl.BlockSpec(memory_space=pl.ANY)] * 5,
+        scratch_shapes=[
+            pltpu.VMEM((2, half, local), dtype),
+            pltpu.VMEM((2, rows, width), dtype),
+            pltpu.VMEM((width, rows), dtype),
+            dma((2, 5)),
+            dma((2, 2, CORES)),
+            dma(line),
+            dma(line),
+            dma((2, CORES)),
+            dma(line),
+            dma((2, n_fs, CORES)),
+            dma((2,)),
+            dma((2,)),
+            dma((3, kb, CORES)),
+            dma((3, n_fs)),
+            dma((3, n_fs)),
+            dma((3, n_fs)),
+            dma((3, n_fs, 2)),
+            dma((3, n_fs, 2)),
+            dma((3,)),
+            dma((3,)),
+        ],
+        compiler_params=pltpu.CompilerParams(collective_id=4, has_side_effects=True),
+        cost_estimate=pl.CostEstimate(
+            flops=0, bytes_accessed=sum(2 * a * b for a, b in shapes), transcendentals=0
+        ),
+        name="pull",
+    )(tokens, cot, w_gate, w_up, w_down)
+
+
+def push_kernel(n_fs, *refs):
+    partial, g_gate, g_up, g_down, inv = refs[:5]
+    o_gate, o_up, o_down, o_normed, o_inv = refs[5:10]
+    pair_wide, pair_tall, sum_wide, sum_tall, x_wide, x_tall, t_wide, t_tall = refs[10:18]
+    y_buf, d_buf, z_buf, n_buf = refs[18:22]
+    (p_send, p_recv, x_send, x_recv, z_send, z_recv, f_send, f_recv) = refs[22:30]
+    (y_send, y_recv, d_send, d_recv, n_send, n_recv, own_sem) = refs[30:]
+    r, z, t = lax.axis_index("rep"), lax.axis_index("fs"), lax.axis_index("tp")
+    y, c = lax.div(t, CORES), lax.rem(t, CORES)
+    kb = n_fs // CORES
+    half = partial.shape[0] // n_fs
+    reach = partial.shape[1] // 2
+    local = reach // CORES
+    width = g_gate.shape[1]
+    rows = g_gate.shape[0] // n_fs
+    strip = rows // 2
+    partner = {"tp": y * CORES + 1 - c}
+    across = {"rep": 1 - r}
+    beside = {"tp": (1 - y) * CORES + c}
+    owner = lax.div(z, kb)
+    grads, outs = (g_gate, g_up, g_down), (o_gate, o_up, o_down)
+
+    peers = [partner, across, beside]
+    for j in range(1, n_fs):
+        for h in range(CORES):
+            peers.append({"fs": lax.rem(z + j, n_fs), "tp": y * CORES + h})
+    greet(peers)
+
+    def slot(wide, tall, m, *where):
+        return tall.at[where] if m == 2 else wide.at[(m,) + where]
+
+    def strip_of(band, rep):
+        return pl.ds(pl.multiple_of(band * rows + rep * strip, strip), strip)
+
+    def grad_piece(m, band, rep):
+        if m == 2:
+            return grads[m].at[:, strip_of(band, rep)]
+        return grads[m].at[strip_of(band, rep), :]
+
+    def rep_of(j):
+        return 1 - r if j == 0 else r
+
+    def pair(m, k, j):
+        return remote(
+            grad_piece(m, kb * (1 - c) + k, rep_of(j)),
+            slot(pair_wide, pair_tall, m, k, j),
+            p_send.at[m, k, j],
+            p_recv.at[m, k, j],
+            partner,
+        )
+
+    def swap(m, k):
+        return remote(
+            slot(sum_wide, sum_tall, m, k),
+            slot(x_wide, x_tall, m, k),
+            x_send.at[m, k],
+            x_recv.at[m, k],
+            across,
+        )
+
+    def place(m, block, rep):
+        strips = pl.ds(pl.multiple_of(rep * strip, strip), strip)
+        blocks = pl.ds(pl.multiple_of(block * width, width), width)
+        return outs[m].at[blocks, strips] if m == 2 else outs[m].at[strips, blocks]
+
+    def deliver(m, k):
+        block = lax.rem(z, kb)
+        return remote(
+            slot(t_wide, t_tall, m, k),
+            place(m, block, r),
+            z_send.at[m, k],
+            z_recv.at[m, block],
+            {"fs": kb * c + k, "tp": y * CORES + owner},
+        )
+
+    def delivered(m, k):
+        return remote(place(m, k, r), place(m, k, r), z_send.at[m, k], z_recv.at[m, k], partner)
+
+    def keep(m, k):
+        return pltpu.make_async_copy(slot(t_wide, t_tall, m, k), place(m, k, r), own_sem.at[m])
+
+    def spread(m, k, source):
+        return remote(source, place(m, k, r), f_send.at[m, k], f_recv.at[m, k], across)
+
+    def spread_arrival(m, k):
+        return remote(
+            place(m, k, 1 - r), place(m, k, 1 - r), f_send.at[m, k], f_recv.at[m, k], across
+        )
+
+    def band_rows(band):
+        return pl.ds(pl.multiple_of(band * half, half), half)
+
+    def side_columns(which):
+        return pl.ds(pl.multiple_of(which * reach, reach), reach)
+
+    def over(j):
+        band = lax.rem(z + j, n_fs)
+        return remote(
+            partial.at[band_rows(band), side_columns(1 - y)],
+            y_buf.at[j],
+            y_send.at[j],
+            y_recv.at[j],
+            beside,
+        )
+
+    def normed_send(j):
+        return remote(
+            d_buf.at[j], z_buf.at[z], d_send.at[j], d_recv.at[z], {"fs": lax.rem(z + j, n_fs)}
+        )
+
+    def normed_arrival(j):
+        source = lax.rem(z + j, n_fs)
+        return remote(z_buf.at[source], z_buf.at[source], d_send.at[j], d_recv.at[source], partner)
+
+    def own_rows(core):
+        return pl.ds(pl.multiple_of(core * half, half), half)
+
+    def inv_send():
+        return remote(inv, o_inv.at[own_rows(c), :], n_send.at[0], n_recv.at[0], partner)
+
+    def inv_arrival():
+        at = o_inv.at[own_rows(1 - c), :]
+        return remote(at, at, n_send.at[0], n_recv.at[0], partner)
+
+    def last_send():
+        return remote(n_buf, o_normed.at[own_rows(c), :], n_send.at[1], n_recv.at[1], partner)
+
+    def last_arrival():
+        at = o_normed.at[own_rows(1 - c), :]
+        return remote(at, at, n_send.at[1], n_recv.at[1], partner)
+
+    items = [(m, k) for m in (2, 0, 1) for k in range(kb)]
+    order = list(range(1, n_fs)) + [0]
+    for m, k in items:
+        pair(m, k, 0).start()
+    for j in order:
+        over(j).start()
+    for m, k in items:
+        pair(m, k, 1).start()
+    inv_send().start()
+    o_inv[own_rows(c), :] = inv[...]
+
+    def added(m, k, j):
+        own = grad_piece(m, kb * c + k, rep_of(j))[...].astype(jnp.float32)
+        return own + slot(pair_wide, pair_tall, m, k, j)[...].astype(jnp.float32)
+
+    def put(wide, tall, m, k, value):
+        if m == 2:
+            tall[k] = value
+        else:
+            wide[m, k] = value
+
+    def first(m, k):
+        pair(m, k, 0).wait_recv()
+        put(sum_wide, sum_tall, m, k, added(m, k, 0).astype(jnp.bfloat16))
+        swap(m, k).start()
+
+    def second(m, k):
+        pair(m, k, 1).wait_recv()
+        swap(m, k).wait_recv()
+        whole = added(m, k, 1) + slot(x_wide, x_tall, m, k)[...].astype(jnp.float32)
+        put(t_wide, t_tall, m, k, whole.astype(jnp.bfloat16))
+        mine = kb * c + k == z
+
+        @pl.when(mine)
+        def _():
+            keep(m, k).start()
+            spread(m, k, slot(t_wide, t_tall, m, k)).start()
+
+        @pl.when(jnp.logical_not(mine))
+        def _():
+            deliver(m, k).start()
+
+    def third(m, k):
+        @pl.when(kb * c + k != z)
+        def _():
+            delivered(m, k).wait_recv()
+            spread(m, k, place(m, k, r)).start()
+
+    def normed_step(j):
+        over(j).wait_recv()
+        band = lax.rem(z + j, n_fs)
+        own = partial[band_rows(band), side_columns(y)].astype(jnp.float32)
+        d_buf[j] = (own + y_buf[j].astype(jnp.float32)).astype(jnp.bfloat16)
+        if j:
+            normed_send(j).start()
+
+    for m, k in items:
+        first(m, k)
+    n_items = len(items)
+    for i in range(n_items + 2):
+        if i < n_items:
+            second(*items[i])
+        if i < n_fs:
+            normed_step(order[i])
+        if i >= 2:
+            third(*items[i - 2])
+
+    for j in range(1, n_fs):
+        normed_arrival(j).wait_recv()
+    total = d_buf[0].astype(jnp.float32)
+    for j in range(1, n_fs):
+        total = total + z_buf[lax.rem(z + j, n_fs)].astype(jnp.float32)
+    total = total.astype(jnp.bfloat16)
+
+    @pl.when(c == 0)
+    def _():
+        o_normed[pl.ds(0, half), :] = total[:, :local]
+        n_buf[...] = total[:, local:]
+
+    @pl.when(c == 1)
+    def _():
+        o_normed[pl.ds(half, half), :] = total[:, local:]
+        n_buf[...] = total[:, :local]
+
+    last_send().start()
+
+    for m, k in items:
+        for j in range(2):
+            pair(m, k, j).wait_send()
+        swap(m, k).wait_send()
+        mine = kb * c + k == z
+
+        @pl.when(mine)
+        def _():
+            keep(m, k).wait()
+
+        @pl.when(jnp.logical_not(mine))
+        def _():
+            deliver(m, k).wait_send()
+
+        spread(m, k, place(m, k, r)).wait_send()
+        spread_arrival(m, k).wait_recv()
+    for j in range(n_fs):
+        over(j).wait_send()
+        if j:
+            normed_send(j).wait_send()
+    inv_send().wait_send()
+    inv_arrival().wait_recv()
+    last_send().wait_send()
+    last_arrival().wait_recv()
+
+
+def push(n_fs, partial, g_gate, g_up, g_down, inv):
+    kb = n_fs // CORES
+    half, model = partial.shape[0] // n_fs, partial.shape[1]
+    width, rows = g_gate.shape[1], g_gate.shape[0] // n_fs
+    strip = rows // 2
+    reach = model // 2
+    local = reach // CORES
+    dtype = partial.dtype
+    dma = pltpu.SemaphoreType.DMA
+    vmem = pl.BlockSpec(memory_space=pltpu.VMEM)
+    hbm = pl.BlockSpec(memory_space=pl.ANY)
+    wide, tall = (strip, width), (width, strip)
+    shapes = [(rows, kb * width)] * 2 + [(kb * width, rows)]
+    pairs = dma((3, kb, 2))
+    singles = dma((3, kb))
+    return pl.pallas_call(
+        functools.partial(push_kernel, n_fs),
+        out_shape=[jax.ShapeDtypeStruct(s, dtype) for s in shapes]
+        + [
+            jax.ShapeDtypeStruct((CORES * half, local), dtype),
+            jax.ShapeDtypeStruct((CORES * half, inv.shape[1]), inv.dtype),
+        ],
+        in_specs=[vmem] * 5,
+        out_specs=[hbm] * 3 + [vmem] * 2,
+        scratch_shapes=[
+            pltpu.VMEM((2, kb, 2) + wide, dtype),
+            pltpu.VMEM((kb, 2) + tall, dtype),
+            pltpu.VMEM((2, kb) + wide, dtype),
+            pltpu.VMEM((kb,) + tall, dtype),
+            pltpu.VMEM((2, kb) + wide, dtype),
+            pltpu.VMEM((kb,) + tall, dtype),
+            pltpu.VMEM((2, kb) + wide, dtype),
+            pltpu.VMEM((kb,) + tall, dtype),
+            pltpu.VMEM((n_fs, half, reach), dtype),
+            pltpu.VMEM((n_fs, half, reach), dtype),
+            pltpu.VMEM((n_fs, half, reach), dtype),
+            pltpu.VMEM((half, local), dtype),
+            pairs,
+            pairs,
+            singles,
+            singles,
+            singles,
+            singles,
+            singles,
+            singles,
+            dma((n_fs,)),
+            dma((n_fs,)),
+            dma((n_fs,)),
+            dma((n_fs,)),
+            dma((2,)),
+            dma((2,)),
+            dma((3,)),
+        ],
+        compiler_params=pltpu.CompilerParams(
+            collective_id=5, has_side_effects=True, vmem_limit_bytes=56 * 1024 * 1024
+        ),
+        cost_estimate=pl.CostEstimate(
+            flops=0, bytes_accessed=sum(2 * a * b for a, b in shapes), transcendentals=0
+        ),
+        name="push",
+    )(partial, g_gate, g_up, g_down, inv)
+
+
+def sums_kernel(n_fs, n_tp, n_rep, here, there, all_here, all_there, h_send, h_recv, o_send, o_recv):
+    r, z, t = lax.axis_index("rep"), lax.axis_index("fs"), lax.axis_index("tp")
+    groups = n_rep * n_fs
+    spot = r * n_fs + z
+
+    def group_of(j):
+        at = lax.rem(spot + j, groups)
+        return {"rep": lax.div(at, n_fs), "fs": lax.rem(at, n_fs)}
+
+    def lane_of(j):
+        return {"tp": lax.rem(t + j, n_tp)}
+
+    greet([lane_of(j) for j in range(1, n_tp)] + [group_of(j) for j in range(1, groups)])
+    sends = []
+    for j in range(1, n_tp):
+        sends.append(
+            remote(here, all_here.at[t], h_send.at[j - 1], h_recv.at[n_tp - j - 1], lane_of(j))
+        )
+    for j in range(1, groups):
+        sends.append(
+            remote(there, all_there.at[spot], o_send.at[j - 1], o_recv.at[groups - j - 1], group_of(j))
+        )
+    for copy in sends:
+        copy.start()
+    all_here[t] = here[...]
+    all_there[spot] = there[...]
+    for j in range(1, n_tp):
+        place = all_here.at[lax.rem(t + j, n_tp)]
+        remote(place, place, h_send.at[j - 1], h_recv.at[j - 1], lane_of(j)).wait_recv()
+    for j in range(1, groups):
+        place = all_there.at[lax.rem(spot + j, groups)]
+        remote(place, place, o_send.at[j - 1], o_recv.at[j - 1], group_of(j)).wait_recv()
+    for copy in sends:
+        copy.wait_send()
+
+
+def exchange_sums(n_fs, n_tp, n_rep, here, there):
+    dma = pltpu.SemaphoreType.DMA
+    vmem = pl.BlockSpec(memory_space=pltpu.VMEM)
+    groups = n_rep * n_fs
+    return pl.pallas_call(
+        functools.partial(sums_kernel, n_fs, n_tp, n_rep),
+        out_shape=[
+            jax.ShapeDtypeStruct((n_tp,) + here.shape, here.dtype),
+            jax.ShapeDtypeStruct((groups,) + there.shape, there.dtype),
+        ],
+        in_specs=[vmem] * 2,
+        out_specs=[vmem] * 2,
+        scratch_shapes=[dma((n_tp - 1,)), dma((n_tp - 1,)), dma((groups - 1,)), dma((groups - 1,))],
+        compiler_params=pltpu.CompilerParams(collective_id=6, has_side_effects=True),
+        name="exchange_sums",
+    )(here, there)
+
+
+def packed(parts):
+    flat = jnp.concatenate([p.reshape(-1) for p in parts])
+    size = -(-flat.shape[0] // 1024) * 1024
+    return jnp.pad(flat, (0, size - flat.shape[0])).reshape(-1, 128)
+
+
+def by_chip(tokens, norm_gain, w_gate, w_up, w_down, cotangent):
+    n_rep, n_fs, n_tp = lax.axis_size("rep"), lax.axis_size("fs"), lax.axis_size("tp")
+    count, local = tokens.shape
+    rows, wide = w_gate.shape
+    half = count // CORES
+    x, dy, f_gate, f_up, f_down = pull(n_fs, n_tp, tokens, cotangent, w_gate, w_up, w_down)
+    model = x.shape[1]
+    wide_tokens = x.astype(jnp.float32)
+    gain_f = norm_gain.astype(jnp.float32)
+    inverse = lax.rsqrt(jnp.mean(wide_tokens * wide_tokens, axis=-1, keepdims=True) + 1e-06)
+    normed = (wide_tokens * inverse * gain_f).astype(jnp.bfloat16)
+    gate = jnp.dot(normed, f_gate, preferred_element_type=jnp.float32)
+    up_proj = jnp.dot(normed, f_up, preferred_element_type=jnp.float32)
+    sigma = jax.nn.sigmoid(gate)
+    active = gate * sigma
+    hidden = (active * up_proj).astype(jnp.bfloat16)
+    back = 0.5 * contract_last(dy, f_down)
+    d_up = (back * active).astype(jnp.bfloat16)
+    d_gate = (back * up_proj * sigma * (1.0 + gate * (1.0 - sigma))).astype(jnp.bfloat16)
+    partial = (contract_last(d_gate, f_gate) + contract_last(d_up, f_up)).astype(jnp.bfloat16)
+    g_down = (0.5 * contract_first(hidden, dy)).astype(jnp.bfloat16)
+    g_gate = contract_first(normed, d_gate).astype(jnp.bfloat16)
+    g_up = contract_first(normed, d_up).astype(jnp.bfloat16)
+    own = lax.dynamic_slice_in_dim(inverse, lax.axis_index("fs") * half, half, 0)
+    s_gate, s_up, s_down, d_normed, inv = push(
+        n_fs, partial, g_gate, g_up, g_down, jnp.broadcast_to(own, (half, 128))
+    )
+
+    grad_gate, grad_up, grad_down = (s.astype(jnp.float32) for s in (s_gate, s_up, s_down))
+    d_normed = d_normed.astype(jnp.float32)
+    inv = inv[:, :1]
+    gain_here = lax.dynamic_slice_in_dim(gain_f, lax.axis_index("tp") * local, local, 0)
+    local_tokens = tokens.astype(jnp.float32)
+    scaled = d_normed * gain_here
+    here = packed(
+        [
+            jnp.sum(scaled * local_tokens, axis=-1),
+            jnp.sum(grad_gate * grad_gate, axis=1),
+            jnp.sum(grad_up * grad_up, axis=1),
+        ]
+    )
+    there = packed(
+        [
+            jnp.sum(d_normed * local_tokens * inv, axis=0),
+            jnp.sum(grad_down * grad_down, axis=1),
+        ]
+    )
+    all_here, all_there = exchange_sums(n_fs, n_tp, n_rep, here, there)
+    here = jnp.sum(all_here, axis=0).reshape(-1)
+    rowdot = here[:count]
+    gate_up_sq = here[count : count + 2 * rows].reshape(2, rows)
+    flat = all_there.reshape(n_rep, n_fs, -1)
+    grad_gain = jnp.sum(flat[:, :, :local], axis=(0, 1))
+    down_sq = jnp.sum(flat[0, :, local : local + wide], axis=0)
+    grad_tokens = (
+        cotangent.astype(jnp.float32)
+        + inv * scaled
+        - local_tokens * inv**3 * rowdot[:, None] / model
+    ).astype(jnp.bfloat16)
+    return (grad_tokens, grad_gain, grad_gate, grad_up, grad_down, gate_up_sq, down_sq)
+
+
+def fits_chips(mesh):
+    n_rep, n_fs, n_tp = mesh.shape["rep"], mesh.shape["fs"], mesh.shape["tp"]
+    return n_rep == 2 and n_tp == 2 * CORES and n_fs == 2 * CORES
+
+
 def solution(mesh):
     placed = (
         P(("rep", "fs"), "tp"),
@@ -492,7 +1300,7 @@
         P(("rep", "fs"), "tp"),
     )
     return jax.shard_map(
-        on_device,
+        by_chip if fits_chips(mesh) else on_device,
         mesh=mesh,
         in_specs=placed,
         out_specs=(

time: 501 us -> 271 us (0.54)
  Pallas kernels: 385 us -> 220 us
  blocking collectives: 37.8 us -> 0 us
  between operations: 14.3 us -> 0.79 us
  waiting for transfers between devices: 8.43 us -> 0 us
    pallas_call x4 -> x3, Pallas kernels: 385 us -> 220 us  [the longest x1 109 us: pull(): pl.pallas_call(functools.partial(pull_kernel, n_fs), out_shape=[jax.Shape...]
    psum x3 -> x0, blocking collectives: 37.8 us -> none  [the longest x1 20.5 us: on_device(): lax.psum(jnp.sum(d_normed * local_tokens * inverse, axis=0), ('rep', 'fs'))]
    ppermute x3 -> x0, waiting for transfers between devices: 8.39 us -> none  [over_rep(): lax.ppermute(part, 'rep', [(i, (i + 1) % n_rep) for i in range(n_rep)])]
    reduce_sum x5 -> x7, other arithmetic: 12.7 us -> 12 us  [the longest x1 3.06 us: by_chip(): jnp.sum(grad_down * grad_down, axis=1)]
  transfers between devices with their start and end apart: 4 -> 0, of which waited for: 1 -> 0; matrix products, arithmetic and copies ran while one was open for 6% -> 0% of each run, Pallas kernels for 47% -> 0%
where the time goes in v1:
time: 271 us; the launch traced here: 270 us
  Pallas kernels  220 us (81%)
  matrix products  29.5 us (11%)
  other arithmetic  16.2 us (6%)
  local copies, waits for them, and re-layouts  3.08 us (1%)
    pallas_call x1, Pallas kernels, pull(): pl.pallas_call(functools.partial(pull_kernel, n_fs), out_shape=[jax.Shape...  109 us
    pallas_call x1, Pallas kernels, push(): pl.pallas_call(functools.partial(push_kernel, n_fs), out_shape=[jax.Shape...  94.6 us
    pallas_call x1, Pallas kernels, exchange_sums(): pl.pallas_call(functools.partial(sums_kernel, n_fs, n_tp, n_rep), out_sha...  16.5 us
    dot_general x3, matrix products, contract_first(): lax.dot_general(left, right, (((0,), (0,)), ((), ())), preferred_element_...  12.3 us
    dot_general x3, matrix products, contract_last(): lax.dot_general(left, right, (((1,), (1,)), ((), ())), preferred_element_...  9.91 us

profile of v1, /device:TPU:0, one launch (start us, length us, event | category | flops | bytes accessed | tf_op | source)
XLA Modules:
  0.0 270.0 jit_solution(4075816878399042641)
XLA Ops:
  0.6 0.8 dynamic_slice.4
  1.4 0.7 convert_element_type.57
  2.1 109.3 %pull.1 = (bf16[768,2048]{1,0:T(8,128)(2,1)}, bf16[768,2048]{1,0:T(8,128)(2,1)}, bf16[2048,640]{1,0:T(8,128)(2,1)}, bf16[2048,640]{1,0:T(8,128)(2,1)}, bf16[640,2048]{1,0:T(8,128)(2,1)}) custom-call(bf16[384,512]{1,0:T(8,128)(2,1)} %refs_0_.1, bf16[384,512]{1,0:T(8,128)(2,1)} %refs_1_.1, bf16[512,1280]{1,0:T(8,128)(2,1)} %refs_2_.1, ...), custom_call_target="tpu_custom_call" | custom-call | bytes 14155776 | tf_op jit(solution)/shard_map/pull/pallas_call | solution.py:825
  111.4 2.7 %fusion = f32[768]{0:T(1024)S(1)} fusion(bf16[768,2048]{1,0:T(8,128)(2,1)} %get-tuple-element.21), kind=kLoop, calls=%fused_computation.2 | loop fusion | flops 4717824 | bytes 3148800 | tf_op jit(solution)/shard_map/reduce_sum | solution.py:1235
  114.2 0.1 dynamic-slice.3
  114.2 0.7 broadcast_in_dim.2.refs_4_
  115.0 0.0 copy-done.1
  115.0 4.6 %fusion.20 = f32[768,640]{1,0:T(8,128)S(1)} fusion(bf16[2048,640]{1,0:T(8,128)(2,1)} %get-tuple-element.23, bf16[768,2048]{1,0:T(8,128)(2,1)S(1)} %copy-done.1, f32[2048]{0:T(1024)S(1)} %convert_element_type.57, f32[768]{0:T(1024)S(1)} %add_rsqrt_fusion), kind=kOutput, calls=%fused_computation.45 | convolution fusion | flops 2019557376 | bytes 7744512 | tf_op jit(solution)/shard_map/dot_general | solution.py:1237
  119.6 0.0 copy-done.7
  119.6 0.0 copy-start.6
  119.6 0.0 copy-start.9
  119.6 2.7 fusion.22
  122.3 3.2 %multiply_convert_fusion.2 = (bf16[768,640]{1,0:T(8,128)(2,1)S(1)}, bf16[768,640]{1,0:T(8,128)(2,1)S(1)}) fusion(f32[768,640]{1,0:T(8,128)S(1)} %fusion.20, f32[768,640]{1,0:T(8,128)S(1)} %fusion.22, bf16[768,2048]{1,0:T(8,128)(2,1)S(1)} %copy-done.6, bf16[640,2048]{1,0:T(8,128)(2,1)S(1)} %copy-done.9), kind=kOutput, calls=%fused_computation.13 | convolution fusion | flops 2020147200 | bytes 11665408 | tf_op jit(solution)/shard_map/dot_general | solution.py:14
  125.5 3.9 %multiply_convert_fusion.refs_3_ = bf16[640,2048]{1,0:T(8,128)(2,1)} fusion(bf16[768,2048]{1,0:T(8,128)(2,1)S(1)} %copy-done.6, f32[768,640]{1,0:T(8,128)S(1)} %fusion.22, f32[768,640]{1,0:T(8,128)S(1)} %fusion.20), kind=kOutput, calls=%fused_computation.6 | convolution fusion | flops 2018836480 | bytes 9699328 | tf_op jit(solution)/shard_map/dot_general | solution.py:20
  129.4 4.2 %convolution_convert_fusion.refs_2_ = bf16[2048,640]{1,0:T(8,128)(2,1)} fusion(bf16[768,640]{1,0:T(8,128)(2,1)S(1)} %get-tuple-element.41, bf16[768,2048]{1,0:T(8,128)(2,1)S(1)} %copy-done.1, f32[2048]{0:T(1024)S(1)} %convert_element_type.57, f32[768]{0:T(1024)S(1)} %add_rsqrt_fusion), kind=kOutput, calls=%fused_computation.7 | convolution fusion | flops 2020868096 | bytes 6761472 | tf_op jit(solution)/shard_map/dot_general | solution.py:20
  133.6 4.2 %convolution_convert_fusion.1.refs_1_ = bf16[2048,640]{1,0:T(8,128)(2,1)} fusion(bf16[768,640]{1,0:T(8,128)(2,1)S(1)} %get-tuple-element.42, bf16[768,2048]{1,0:T(8,128)(2,1)S(1)} %copy-done.1, f32[2048]{0:T(1024)S(1)} %convert_element_type.57, f32[768]{0:T(1024)S(1)} %add_rsqrt_fusion), kind=kOutput, calls=%fused_computation.8 | convolution fusion | flops 2020868096 | bytes 6761472 | tf_op jit(solution)/shard_map/dot_general | solution.py:20
  137.8 2.6 fusion.24
  140.5 4.1 %add_convert_fusion.refs_0_ = bf16[768,2048]{1,0:T(8,128)(2,1)} fusion(f32[768,2048]{1,0:T(8,128)S(1)} %fusion.24, bf16[768,640]{1,0:T(8,128)(2,1)S(1)} %get-tuple-element.41, bf16[2048,640]{1,0:T(8,128)(2,1)S(1)} %copy-done.7), kind=kOutput, calls=%fused_computation.5 | convolution fusion | flops 2016411648 | bytes 13041664 | tf_op jit(solution)/shard_map/dot_general | solution.py:14
  144.5 94.6 %push.1 = (bf16[512,1280]{1,0:T(8,128)(2,1)}, bf16[512,1280]{1,0:T(8,128)(2,1)}, bf16[1280,512]{1,0:T(8,128)(2,1)}, bf16[384,512]{1,0:T(8,128)(2,1)}, f32[384,128]{1,0:T(8,128)}) custom-call(bf16[768,2048]{1,0:T(8,128)(2,1)} %add_convert_fusion.refs_0_, bf16[2048,640]{1,0:T(8,128)(2,1)} %convolution_convert_fusion.1.refs_1_, ...), custom_call_target="tpu_custom_call" | custom-call | bytes 3932160 | tf_op jit(solution)/shard_map/push/pallas_call | solution.py:1118
  239.2 1.3 fusion.14
  240.5 1.3 fusion.12
  241.8 3.1 %multiply_reduce_fusion = (f32[1280]{0:T(1024)S(1)}, f32[1280,512]{1,0:T(8,128)}) fusion(bf16[1280,512]{1,0:T(8,128)(2,1)} %get-tuple-element.28), kind=kLoop, calls=%fused_computation.9 | loop fusion | flops 1964800 | bytes 3937280 | tf_op jit(solution)/shard_map/reduce_sum | solution.py:1270
  244.9 0.6 fusion.15.there
  245.5 2.9 %multiply_reduce_fusion.1 = (f32[512]{0:T(512)S(1)}, f32[512,1280]{1,0:T(8,128)}, f32[512]{0:T(512)S(1)}, f32[512,1280]{1,0:T(8,128)}) fusion(bf16[512,1280]{1,0:T(8,128)(2,1)S(1)} %copy-done.5, bf16[512,1280]{1,0:T(8,128)(2,1)S(1)} %copy-done.4), kind=kLoop, calls=%fused_computation.10 | loop fusion | flops 3931136 | bytes 7868416 | tf_op jit(solution)/shard_map/reduce_sum | solution.py:1264
  248.3 0.6 fusion.16.here
  248.9 16.5 %exchange_sums.1 = (f32[4,16,128]{2,1,0:T(8,128)}, f32[8,16,128]{2,1,0:T(8,128)}) custom-call(f32[16,128]{1,0:T(8,128)} %fusion.16.here, f32[16,128]{1,0:T(8,128)} %fusion.15.there), custom_call_target="tpu_custom_call" | custom-call | tf_op jit(solution)/shard_map/exchange_sums/pallas_call | solution.py:1206
  265.4 0.8 reduce_sum.87
  266.2 1.1 fusion.7
  267.3 0.6 reshape.60
  267.9 0.9 reshape.59
  268.8 0.6 slice_reduce_fusion.2
  269.4 0.6 slice_reduce_fusion.1
  (19 shorter events, 0.0 us)
Async XLA Ops:
  111.4 3.6 %copy-start.1 = (bf16[768,2048]{1,0:T(8,128)(2,1)S(1)}, bf16[768,2048]{1,0:T(8,128)(2,1)}, u32[]{:S(2)}) copy-start(bf16[768,2048]{1,0:T(8,128)(2,1)} %get-tuple-element.21) | copy-start | bytes 9437188
  115.0 4.6 %copy-start.7 = (bf16[2048,640]{1,0:T(8,128)(2,1)S(1)}, bf16[2048,640]{1,0:T(8,128)(2,1)}, u32[]{:S(2)}) copy-start(bf16[2048,640]{1,0:T(8,128)(2,1)} %get-tuple-element.22) | copy-start | bytes 7864324
  119.6 2.7 %copy-start.6 = (bf16[768,2048]{1,0:T(8,128)(2,1)S(1)}, bf16[768,2048]{1,0:T(8,128)(2,1)}, u32[]{:S(2)}) copy-start(bf16[768,2048]{1,0:T(8,128)(2,1)} %get-tuple-element.19) | copy-start | bytes 9437188
  119.6 2.7 %copy-start.9 = (bf16[640,2048]{1,0:T(8,128)(2,1)S(1)}, bf16[640,2048]{1,0:T(8,128)(2,1)}, u32[]{:S(2)}) copy-start(bf16[640,2048]{1,0:T(8,128)(2,1)} %get-tuple-element.20) | copy-start | bytes 7864324
  133.6 4.2 %copy-start.8 = (bf16[2048,640]{1,0:T(8,128)(2,1)S(1)}, bf16[2048,640]{1,0:T(8,128)(2,1)}, u32[]{:S(2)}) copy-start(bf16[2048,640]{1,0:T(8,128)(2,1)} %get-tuple-element.23) | copy-start | bytes 7864324
  144.5 95.9 %copy-start = (bf16[384,512]{1,0:T(8,128)(2,1)S(1)}, bf16[384,512]{1,0:T(8,128)(2,1)}, u32[]{:S(2)}) copy-start(bf16[384,512]{1,0:T(8,128)(2,1)} %refs_0_.1) | copy-start | bytes 1179652
  239.2 6.3 %copy-start.4 = (bf16[512,1280]{1,0:T(8,128)(2,1)S(1)}, bf16[512,1280]{1,0:T(8,128)(2,1)}, u32[]{:S(2)}) copy-start(bf16[512,1280]{1,0:T(8,128)(2,1)} %get-tuple-element.26) | copy-start | bytes 3932164
  239.2 6.3 %copy-start.5 = (bf16[512,1280]{1,0:T(8,128)(2,1)S(1)}, bf16[512,1280]{1,0:T(8,128)(2,1)}, u32[]{:S(2)}) copy-start(bf16[512,1280]{1,0:T(8,128)(2,1)} %get-tuple-element.27) | copy-start | bytes 3932164
  245.5 20.7 %copy-start.2 = (bf16[384,512]{1,0:T(8,128)(2,1)S(1)}, bf16[384,512]{1,0:T(8,128)(2,1)}, u32[]{:S(2)}) copy-start(bf16[384,512]{1,0:T(8,128)(2,1)} %refs_1_.1) | copy-start | bytes 1179652
  245.5 20.7 %copy-start.3 = (bf16[384,512]{1,0:T(8,128)(2,1)S(1)}, bf16[384,512]{1,0:T(8,128)(2,1)}, u32[]{:S(2)}) copy-start(bf16[384,512]{1,0:T(8,128)(2,1)} %get-tuple-element.25) | copy-start | bytes 1179652

commit v2 on v1

--- a/solution.py
+++ b/solution.py
@@ -483,27 +483,41 @@
 
 
 CORES = 2
+LANES = 128
+TILE = 256
 
 
 def line_next(z, n_fs, side):
     return z <= n_fs - 2 if side == 0 else z >= 1
 
 
-def pull_kernel(n_fs, *refs):
-    tokens, cot, w_gate, w_up, w_down = refs[:5]
-    outs = refs[5:10]
-    act_hold, weight_hold, down_hold = refs[10:13]
-    (own_sem, az_own, az_fwd, az_recv, ay_own, ay_fwd, ay_recv, ap_send, ap_recv) = refs[13:22]
-    (w_send, w_recv, wx_send, wx_recv, wp_send, wp_recv, wo_send, wo_recv) = refs[22:]
+def layer_kernel(n_fs, *refs):
+    tokens, cot, w_gate, w_up, w_down, gain = refs[:6]
+    o_gate, o_up, o_down, o_normed, o_inv = refs[6:11]
+    full = refs[11:16]
+    x_full, dy_full, f_gate, f_up, f_down = full
+    normed, normed_t, hidden_t, act_f, slope_f, d_gate, d_up, inv_all = refs[16:24]
+    g_gate, g_up, g_down = refs[24:27]
+    pair_wide, pair_tall, sum_wide, sum_tall, x_wide, x_tall, t_wide, t_tall = refs[27:35]
+    y_buf, d_buf, z_buf, n_buf = refs[35:39]
+    (load_sem, az_own, az_fwd, az_recv, ay_own, ay_fwd, ay_recv, ap_send, ap_recv) = refs[39:48]
+    (w_send, w_recv, wx_send, wx_recv, wp_send, wp_recv, wo_send, wo_recv) = refs[48:56]
+    (p_send, p_recv, x_send, x_recv, z_send, z_recv, f_send, f_recv) = refs[56:64]
+    (y_send, y_recv, d_send, d_recv, n_send, n_recv, own_sem) = refs[64:]
     r, z, t = lax.axis_index("rep"), lax.axis_index("fs"), lax.axis_index("tp")
     y, c = lax.div(t, CORES), lax.rem(t, CORES)
     acts, weights = (tokens, cot), (w_gate, w_up, w_down)
+    grads, outs = (g_gate, g_up, g_down), (o_gate, o_up, o_down)
     half, local = tokens.shape[0] // CORES, tokens.shape[1]
+    count, model = x_full.shape
     rows = w_gate.shape[0]
     kb = n_fs // CORES
     width = w_gate.shape[1] // kb
+    strip = rows // 2
+    reach = model // 2
     partner = {"tp": y * CORES + 1 - c}
     across = {"rep": 1 - r}
+    beside = {"tp": (1 - y) * CORES + c}
     owner = lax.div(z, kb)
 
     peers = [partner, across]
@@ -517,7 +531,7 @@
         return acts[a].at[pl.ds(pl.multiple_of(h * half, half), half), :]
 
     def act_place(a, source, column):
-        return outs[a].at[
+        return full[a].at[
             pl.ds(pl.multiple_of(source * half, half), half),
             pl.ds(pl.multiple_of(column * local, local), local),
         ]
@@ -591,18 +605,18 @@
 
     def band_of(m, source):
         band = pl.ds(pl.multiple_of(source * rows, rows), rows)
-        return outs[2 + m].at[:, band] if m == 2 else outs[2 + m].at[band, :]
+        return full[2 + m].at[:, band] if m == 2 else full[2 + m].at[band, :]
 
     def quarter(m, source, rep, core):
         if m == 2:
             size = width // (2 * CORES)
-            return outs[4].at[
+            return full[4].at[
                 pl.ds(pl.multiple_of((rep * CORES + core) * size, size), size),
                 pl.ds(pl.multiple_of(source * rows, rows), rows),
             ]
         size = rows // (2 * CORES)
         start = source * rows + (rep * CORES + core) * size
-        return outs[2 + m].at[pl.ds(pl.multiple_of(start, size), size), :]
+        return full[2 + m].at[pl.ds(pl.multiple_of(start, size), size), :]
 
     def own_quarter(m, k, core):
         if m == 2:
@@ -656,7 +670,118 @@
     def own_beside_arrival(m):
         return remote(band_of(m, z), band_of(m, z), wo_send.at[m], wo_recv.at[m], partner)
 
-    for a in range(2):
+    def slot(wide, tall, m, *where):
+        return tall.at[where] if m == 2 else wide.at[(m,) + where]
+
+    def strip_of(band, rep):
+        return pl.ds(pl.multiple_of(band * rows + rep * strip, strip), strip)
+
+    def grad_piece(m, band, rep):
+        if m == 2:
+            return grads[m].at[:, strip_of(band, rep)]
+        return grads[m].at[strip_of(band, rep), :]
+
+    def rep_of(j):
+        return 1 - r if j == 0 else r
+
+    def pair(m, k, j):
+        return remote(
+            grad_piece(m, kb * (1 - c) + k, rep_of(j)),
+            slot(pair_wide, pair_tall, m, k, j),
+            p_send.at[m, k, j],
+            p_recv.at[m, k, j],
+            partner,
+        )
+
+    def swap(m, k):
+        return remote(
+            slot(sum_wide, sum_tall, m, k),
+            slot(x_wide, x_tall, m, k),
+            x_send.at[m, k],
+            x_recv.at[m, k],
+            across,
+        )
+
+    def place(m, block, rep):
+        strips = pl.ds(pl.multiple_of(rep * strip, strip), strip)
+        blocks = pl.ds(pl.multiple_of(block * width, width), width)
+        return outs[m].at[blocks, strips] if m == 2 else outs[m].at[strips, blocks]
+
+    def deliver(m, k):
+        block = lax.rem(z, kb)
+        return remote(
+            slot(t_wide, t_tall, m, k),
+            place(m, block, r),
+            z_send.at[m, k],
+            z_recv.at[m, block],
+            {"fs": kb * c + k, "tp": y * CORES + owner},
+        )
+
+    def delivered(m, k):
+        return remote(place(m, k, r), place(m, k, r), z_send.at[m, k], z_recv.at[m, k], partner)
+
+    def keep(m, k):
+        return pltpu.make_async_copy(slot(t_wide, t_tall, m, k), place(m, k, r), own_sem.at[m])
+
+    def spread(m, k, source):
+        return remote(source, place(m, k, r), f_send.at[m, k], f_recv.at[m, k], across)
+
+    def spread_arrival(m, k):
+        return remote(
+            place(m, k, 1 - r), place(m, k, 1 - r), f_send.at[m, k], f_recv.at[m, k], across
+        )
+
+    def band_rows(band):
+        return pl.ds(pl.multiple_of(band * half, half), half)
+
+    def side_columns(which):
+        return pl.ds(pl.multiple_of(which * reach, reach), reach)
+
+    def over(j):
+        band = lax.rem(z + j, n_fs)
+        return remote(
+            x_full.at[band_rows(band), side_columns(1 - y)],
+            y_buf.at[j],
+            y_send.at[j],
+            y_recv.at[j],
+            beside,
+        )
+
+    def normed_send(j):
+        return remote(
+            d_buf.at[j], z_buf.at[z], d_send.at[j], d_recv.at[z], {"fs": lax.rem(z + j, n_fs)}
+        )
+
+    def normed_arrival(j):
+        source = lax.rem(z + j, n_fs)
+        return remote(z_buf.at[source], z_buf.at[source], d_send.at[j], d_recv.at[source], partner)
+
+    def own_rows(core):
+        return pl.ds(pl.multiple_of(core * half, half), half)
+
+    def inv_send():
+        return remote(inv_all.at[band_rows(z), :], o_inv.at[own_rows(c), :], n_send.at[0], n_recv.at[0], partner)
+
+    def inv_arrival():
+        at = o_inv.at[own_rows(1 - c), :]
+        return remote(at, at, n_send.at[0], n_recv.at[0], partner)
+
+    def last_send():
+        return remote(n_buf, o_normed.at[own_rows(c), :], n_send.at[1], n_recv.at[1], partner)
+
+    def last_arrival():
+        at = o_normed.at[own_rows(1 - c), :]
+        return remote(at, at, n_send.at[1], n_recv.at[1], partner)
+
+    def loaded(a):
+        return pltpu.make_async_copy(own_act(a, c), act_place(a, z, t), load_sem.at[a])
+
+    def block_loaded(m):
+        return pltpu.make_async_copy(
+            block_of(m, z - kb * owner), band_of(m, z), load_sem.at[2 + m]
+        )
+
+    def act_start(a):
         for h in range(CORES):
             for side in range(2):
 
@@ -665,64 +790,38 @@
                     act_first(a, side, h).start()
 
             act_over_own(a, h).start()
-    for a in range(2):
         act_partner(a).start()
 
-    @pl.when(c == owner)
-    def _():
-        for m in range(3):
+    def own_start(m):
+        @pl.when(c == owner)
+        def _():
             own_beside(m).start()
 
-    holders = [act_hold.at[0], act_hold.at[1]]
-    loads = [pltpu.make_async_copy(own_act(a, c), holders[a], own_sem.at[0, a]) for a in range(2)]
-    stores = [
-        pltpu.make_async_copy(holders[a], act_place(a, z, t), own_sem.at[1, a]) for a in range(2)
-    ]
-    for load in loads:
-        load.start()
-    for load, store in zip(loads, stores):
-        load.wait()
-        store.start()
-    for store in stores:
-        store.wait()
-
-    @pl.when(c == owner)
-    def _():
-        places = [weight_hold.at[0], weight_hold.at[1], down_hold]
-        loads = [
-            pltpu.make_async_copy(block_of(m, z - kb * owner), places[m], own_sem.at[0, 2 + m])
-            for m in range(3)
-        ]
-        stores = [
-            pltpu.make_async_copy(places[m], band_of(m, z), own_sem.at[1, 2 + m])
-            for m in range(3)
-        ]
-        for load in loads:
-            load.start()
-        for load, store in zip(loads, stores):
-            load.wait()
-            store.start()
-        for store in stores:
-            store.wait()
-
-    def act_round(d):
-        for a in range(2):
-            for core in range(CORES):
-                for side in range(2):
-
-                    @pl.when(line_receives(z, n_fs, side, d))
-                    def _():
-                        act_arrival(a, side, d, core).wait_recv()
-                        if d < n_fs - 1:
-
-                            @pl.when(line_next(z, n_fs, side))
-                            def _():
-                                act_forward(a, side, d, core).start()
-
-                        act_over(a, side, d, core).start()
-
-    def weight_round(d):
-        for m in range(3):
+    def act_round(a, d):
+        for core in range(CORES):
+            for side in range(2):
+
+                @pl.when(line_receives(z, n_fs, side, d))
+                def _():
+                    act_arrival(a, side, d, core).wait_recv()
+                    if d < n_fs - 1:
+
+                        @pl.when(line_next(z, n_fs, side))
+                        def _():
+                            act_forward(a, side, d, core).start()
+
+                    act_over(a, side, d, core).start()
+
+    def weight_start(m):
+        for k in range(kb):
+
+            @pl.when(kb * c + k != z)
+            def _():
+                for core in range(CORES):
+                    weight_send(m, k, core).start()
+
+    def weight_round(ms, d):
+        for m in ms:
             for side in range(2):
 
                 @pl.when(line_receives(z, n_fs, side, d))
@@ -732,8 +831,8 @@
                     weight_across(m, source).start()
                     weight_beside(m, source, 0).start()
 
-    def across_round(d):
-        for m in range(3):
+    def across_round(ms, d):
+        for m in ms:
             for side in range(2):
 
                 @pl.when(line_receives(z, n_fs, side, d))
@@ -742,32 +841,27 @@
                     weight_across_arrival(m, source).wait_recv()
                     weight_beside(m, source, 1).start()
 
-    act_round(1)
-    for m in range(3):
-        for k in range(kb):
-
-            @pl.when(kb * c + k != z)
-            def _():
-                for core in range(CORES):
-                    weight_send(m, k, core).start()
-
-    for d in range(1, n_fs):
-        if d + 1 < n_fs:
-            act_round(d + 1)
-        weight_round(d)
-        if d > 1:
-            across_round(d - 1)
-    across_round(n_fs - 1)
-
-    for d in range(1, n_fs):
-        for side in range(2):
-
-            @pl.when(line_receives(z, n_fs, side, d))
-            def _():
-                source = source_of(side, d)
-                for a in range(2):
+    def act_ready(a):
+        for d in range(1, n_fs):
+            for side in range(2):
+
+                @pl.when(line_receives(z, n_fs, side, d))
+                def _():
                     for core in range(CORES):
-                        act_over_arrival(a, source, core).wait_recv()
+                        act_over_arrival(a, source_of(side, d), core).wait_recv()
+
+        act_partner_arrival(a).wait_recv()
+        for h in range(CORES):
+            act_over_arrival(a, z, h).wait_recv()
+        loaded(a).wait()
+
+    def act_sent(a):
+        for d in range(1, n_fs):
+            for side in range(2):
+
+                @pl.when(line_receives(z, n_fs, side, d))
+                def _():
+                    for core in range(CORES):
                         act_over(a, side, d, core).wait_send()
                         if d < n_fs - 1:
 
@@ -775,17 +869,8 @@
                             def _():
                                 act_forward(a, side, d, core).wait_send()
 
-                for m in range(3):
-                    weight_across(m, source).wait_send()
-                    for which in range(2):
-                        weight_beside_arrival(m, source, which).wait_recv()
-                        weight_beside(m, source, which).wait_send()
-
-    for a in range(2):
-        act_partner_arrival(a).wait_recv()
         act_partner(a).wait_send()
         for h in range(CORES):
-            act_over_arrival(a, z, h).wait_recv()
             act_over_own(a, h).wait_send()
             for side in range(2):
 
@@ -793,7 +878,35 @@
                 def _():
                     act_first(a, side, h).wait_send()
 
-    for m in range(3):
+    def weight_ready(ms):
+        for m in ms:
+            for d in range(1, n_fs):
+                for side in range(2):
+
+                    @pl.when(line_receives(z, n_fs, side, d))
+                    def _():
+                        for which in range(2):
+                            weight_beside_arrival(m, source_of(side, d), which).wait_recv()
+
+            @pl.when(c == owner)
+            def _():
+                block_loaded(m).wait()
+
+            @pl.when(c != owner)
+            def _():
+                own_beside_arrival(m).wait_recv()
+
+    def weight_sent(m):
+        for d in range(1, n_fs):
+            for side in range(2):
+
+                @pl.when(line_receives(z, n_fs, side, d))
+                def _():
+                    source = source_of(side, d)
+                    weight_across(m, source).wait_send()
+                    for which in range(2):
+                        weight_beside(m, source, which).wait_send()
+
         for k in range(kb):
 
             @pl.when(kb * c + k != z)
@@ -801,42 +914,319 @@
                 for core in range(CORES):
                     weight_send(m, k, core).wait_send()
 
+        @pl.when(c == owner)
+        def _():
+            own_beside(m).wait_send()
+
+    def tile(i, size):
+        return pl.ds(pl.multiple_of(i * size, size), size)
+
+    def normalize(i):
+        at = tile(i, LANES)
+        wide = x_full[at, :].astype(jnp.float32)
+        inv = lax.rsqrt(jnp.mean(wide * wide, axis=-1, keepdims=True) + 1e-06)
+        value = wide * inv * gain[...]
+        normed[at, :] = value.astype(jnp.bfloat16)
+        normed_t[:, at] = value.T.astype(jnp.bfloat16)
+        inv_all[at, :] = jnp.broadcast_to(inv, (LANES, LANES))
+
+    def forward(i):
+        at = tile(i, TILE)
+        gate = jnp.dot(normed[at, :], f_gate[...], preferred_element_type=jnp.float32)
+        up = jnp.dot(normed[at, :], f_up[...], preferred_element_type=jnp.float32)
+        sigma = jax.nn.sigmoid(gate)
+        active = gate * sigma
+        act_f[at, :] = active
+        slope_f[at, :] = up * sigma * (1.0 + gate * (1.0 - sigma))
+        hidden_t[:, at] = (active * up).T.astype(jnp.bfloat16)
+
+    def backward(i):
+        at = tile(i, TILE)
+        back = 0.5 * contract_last(dy_full[at, :], f_down[...])
+        d_up[at, :] = (back * act_f[at, :]).astype(jnp.bfloat16)
+        d_gate[at, :] = (back * slope_f[at, :]).astype(jnp.bfloat16)
+
+    def gradient(m, own, j, k):
+        band = kb * (c if own else 1 - c) + k
+        at = strip_of(band, 1 - r if j == 0 else r)
+        if m == 2:
+            value = 0.5 * jnp.dot(
+                hidden_t[...], dy_full[:, at], preferred_element_type=jnp.float32
+            )
+            g_down[:, at] = value.astype(jnp.bfloat16)
+        else:
+            right = d_gate if m == 0 else d_up
+            value = jnp.dot(normed_t[at, :], right[...], preferred_element_type=jnp.float32)
+            grads[m][at, :] = value.astype(jnp.bfloat16)
+
+    def gradients(m, j):
+        @pl.loop(0, kb)
+        def _(k):
+            gradient(m, False, j, k)
+            pair(m, k, j).start()
+
+        @pl.loop(0, kb)
+        def _(k):
+            gradient(m, True, j, k)
+
+    def pull_back(band, which):
+        at, columns = band_rows(band), side_columns(which)
+        value = contract_last(d_gate[at, :], f_gate[columns, :])
+        value = value + contract_last(d_up[at, :], f_up[columns, :])
+        x_full[at, columns] = value.astype(jnp.bfloat16)
+
+    def added(m, k, j):
+        own = grad_piece(m, kb * c + k, rep_of(j))[...].astype(jnp.float32)
+        return own + slot(pair_wide, pair_tall, m, k, j)[...].astype(jnp.float32)
+
+    def put(wide, tall, m, k, value):
+        if m == 2:
+            tall[k] = value
+        else:
+            wide[m, k] = value
+
+    def first(m, k):
+        pair(m, k, 0).wait_recv()
+        put(sum_wide, sum_tall, m, k, added(m, k, 0).astype(jnp.bfloat16))
+        swap(m, k).start()
+
+    def second(m, k):
+        pair(m, k, 1).wait_recv()
+        swap(m, k).wait_recv()
+        whole = added(m, k, 1) + slot(x_wide, x_tall, m, k)[...].astype(jnp.float32)
+        put(t_wide, t_tall, m, k, whole.astype(jnp.bfloat16))
+        mine = kb * c + k == z
+
+        @pl.when(mine)
+        def _():
+            keep(m, k).start()
+            spread(m, k, slot(t_wide, t_tall, m, k)).start()
+
+        @pl.when(jnp.logical_not(mine))
+        def _():
+            deliver(m, k).start()
+
+    def third(m, k):
+        @pl.when(kb * c + k != z)
+        def _():
+            delivered(m, k).wait_recv()
+            spread(m, k, place(m, k, r)).start()
+
+    def normed_step(j):
+        over(j).wait_recv()
+        band = lax.rem(z + j, n_fs)
+        own = x_full[band_rows(band), side_columns(y)].astype(jnp.float32)
+        d_buf[j] = (own + y_buf[j].astype(jnp.float32)).astype(jnp.bfloat16)
+        if j:
+            normed_send(j).start()
+
+
+    for a in range(2):
+        loaded(a).start()
+
     @pl.when(c == owner)
     def _():
         for m in range(3):
-            own_beside(m).wait_send()
-
-    @pl.when(c != owner)
+            block_loaded(m).start()
+
+    act_start(0)
+    own_start(0)
+    own_start(1)
+    act_round(0, 1)
+    weight_start(0)
+    weight_start(1)
+    act_round(0, 2)
+    act_start(1)
+    own_start(2)
+    for d in range(3, n_fs):
+        act_round(0, d)
+    weight_round((0, 1), 1)
+    weight_round((0, 1), 2)
+    across_round((0, 1), 1)
+    act_round(1, 1)
+    weight_start(2)
+    for d in range(3, n_fs):
+        weight_round((0, 1), d)
+        across_round((0, 1), d - 1)
+    act_round(1, 2)
+    across_round((0, 1), n_fs - 1)
+    act_ready(0)
+    pl.loop(0, count // LANES)(normalize)
+    weight_round((2,), 1)
+    weight_ready((0, 1))
+    pl.loop(0, count // TILE)(forward)
+    for d in range(3, n_fs):
+        act_round(1, d)
+    weight_round((2,), 2)
+    across_round((2,), 1)
+    for d in range(3, n_fs):
+        weight_round((2,), d)
+        across_round((2,), d - 1)
+    act_ready(1)
+    gradients(2, 0)
+    across_round((2,), n_fs - 1)
+    for k in range(kb):
+        first(2, k)
+    gradients(2, 1)
+    weight_ready((2,))
+    pl.loop(0, count // TILE)(backward)
+    gradients(0, 0)
+    for k in range(kb):
+        first(0, k)
+    for k in range(kb):
+        second(2, k)
+    gradients(1, 0)
+    for k in range(kb):
+        first(1, k)
+    gradients(0, 1)
+    act_sent(0)
+
+    @pl.loop(0, n_fs)
+    def _(i):
+        j = lax.rem(i + 1, n_fs)
+        pull_back(lax.rem(z + j, n_fs), 1 - y)
+        over(j).start()
+
+    gradients(1, 1)
+    for k in range(kb):
+        third(2, k)
+
+    @pl.loop(0, n_fs)
+    def _(i):
+        pull_back(i, y)
+
+    inv_send().start()
+    o_inv[own_rows(c), :] = inv_all[band_rows(z), :]
+    order = list(range(1, n_fs)) + [0]
+    items = [(m, k) for m in range(2) for k in range(kb)]
+    n_items = len(items)
+    for i in range(n_items + 2):
+        if i < n_items:
+            second(*items[i])
+        if i < n_fs:
+            normed_step(order[i])
+        if i >= 2:
+            third(*items[i - 2])
+    items += [(2, k) for k in range(kb)]
+
+    for j in range(1, n_fs):
+        normed_arrival(j).wait_recv()
+    total = d_buf[0].astype(jnp.float32)
+    for j in range(1, n_fs):
+        total = total + z_buf[lax.rem(z + j, n_fs)].astype(jnp.float32)
+    total = total.astype(jnp.bfloat16)
+
+    @pl.when(c == 0)
     def _():
-        for m in range(3):
-            own_beside_arrival(m).wait_recv()
-
-
-def pull(n_fs, n_tp, tokens, cot, w_gate, w_up, w_down):
+        o_normed[pl.ds(0, half), :] = total[:, :local]
+        n_buf[...] = total[:, local:]
+
+    @pl.when(c == 1)
+    def _():
+        o_normed[pl.ds(half, half), :] = total[:, local:]
+        n_buf[...] = total[:, :local]
+
+    last_send().start()
+
+    for m, k in items:
+        for j in range(2):
+            pair(m, k, j).wait_send()
+        swap(m, k).wait_send()
+        mine = kb * c + k == z
+
+        @pl.when(mine)
+        def _():
+            keep(m, k).wait()
+
+        @pl.when(jnp.logical_not(mine))
+        def _():
+            deliver(m, k).wait_send()
+
+        spread(m, k, place(m, k, r)).wait_send()
+        spread_arrival(m, k).wait_recv()
+    for j in range(n_fs):
+        over(j).wait_send()
+        if j:
+            normed_send(j).wait_send()
+    inv_send().wait_send()
+    inv_arrival().wait_recv()
+    last_send().wait_send()
+    last_arrival().wait_recv()
+
+
+    act_sent(1)
+    for m in range(3):
+        weight_sent(m)
+
+
+def layer(n_fs, tokens, cot, w_gate, w_up, w_down, gain):
     half, local = tokens.shape[0] // CORES, tokens.shape[1]
     rows, hidden = w_gate.shape
     width = hidden * CORES // n_fs
     model = rows * n_fs
+    count = half * n_fs
     dtype = tokens.dtype
-    shapes = [(half * n_fs, model)] * 2 + [(model, width)] * 2 + [(width, model)]
+    kb = n_fs // CORES
+    strip = rows // 2
+    reach = model // 2
+    wide, tall = (strip, width), (width, strip)
     dma = pltpu.SemaphoreType.DMA
-    kb = n_fs // CORES
-    line = (2, 2, n_fs - 1, CORES)
+    vmem = pl.BlockSpec(memory_space=pltpu.VMEM)
+    hbm = pl.BlockSpec(memory_space=pl.ANY)
+    line = dma((2, 2, n_fs - 1, CORES))
+    pairs, singles = dma((3, kb, 2)), dma((3, kb))
+
+    def bf(*shape):
+        return pltpu.VMEM(shape, dtype)
+
+    def f32(*shape):
+        return pltpu.VMEM(shape, jnp.float32)
+
+    shapes = [(rows, kb * width)] * 2 + [(kb * width, rows)]
     return pl.pallas_call(
-        functools.partial(pull_kernel, n_fs),
-        out_shape=[jax.ShapeDtypeStruct(s, dtype) for s in shapes],
-        in_specs=[pl.BlockSpec(memory_space=pl.ANY)] * 5,
-        out_specs=[pl.BlockSpec(memory_space=pl.ANY)] * 5,
+        functools.partial(layer_kernel, n_fs),
+        out_shape=[jax.ShapeDtypeStruct(s, dtype) for s in shapes]
+        + [
+            jax.ShapeDtypeStruct((CORES * half, local), dtype),
+            jax.ShapeDtypeStruct((CORES * half, LANES), jnp.float32),
+        ],
+        in_specs=[hbm] * 5 + [vmem],
+        out_specs=[hbm] * 3 + [vmem] * 2,
         scratch_shapes=[
-            pltpu.VMEM((2, half, local), dtype),
-            pltpu.VMEM((2, rows, width), dtype),
-            pltpu.VMEM((width, rows), dtype),
-            dma((2, 5)),
+            bf(count, model),
+            bf(count, model),
+            bf(model, width),
+            bf(model, width),
+            bf(width, model),
+            bf(count, model),
+            bf(model, count),
+            bf(width, count),
+            f32(count, width),
+            f32(count, width),
+            bf(count, width),
+            bf(count, width),
+            f32(count, LANES),
+            bf(model, width),
+            bf(model, width),
+            bf(width, model),
+            bf(2, kb, 2, *wide),
+            bf(kb, 2, *tall),
+            bf(2, kb, *wide),
+            bf(kb, *tall),
+            bf(2, kb, *wide),
+            bf(kb, *tall),
+            bf(2, kb, *wide),
+            bf(kb, *tall),
+            bf(n_fs, half, reach),
+            bf(n_fs, half, reach),
+            bf(n_fs, half, reach),
+            bf(half, local),
+            dma((5,)),
             dma((2, 2, CORES)),
-            dma(line),
-            dma(line),
+            line,
+            line,
             dma((2, CORES)),
-            dma(line),
+            line,
             dma((2, n_fs, CORES)),
             dma((2,)),
             dma((2,)),
@@ -848,295 +1238,6 @@
             dma((3, n_fs, 2)),
             dma((3,)),
             dma((3,)),
-        ],
-        compiler_params=pltpu.CompilerParams(collective_id=4, has_side_effects=True),
-        cost_estimate=pl.CostEstimate(
-            flops=0, bytes_accessed=sum(2 * a * b for a, b in shapes), transcendentals=0
-        ),
-        name="pull",
-    )(tokens, cot, w_gate, w_up, w_down)
-
-
-def push_kernel(n_fs, *refs):
-    partial, g_gate, g_up, g_down, inv = refs[:5]
-    o_gate, o_up, o_down, o_normed, o_inv = refs[5:10]
-    pair_wide, pair_tall, sum_wide, sum_tall, x_wide, x_tall, t_wide, t_tall = refs[10:18]
-    y_buf, d_buf, z_buf, n_buf = refs[18:22]
-    (p_send, p_recv, x_send, x_recv, z_send, z_recv, f_send, f_recv) = refs[22:30]
-    (y_send, y_recv, d_send, d_recv, n_send, n_recv, own_sem) = refs[30:]
-    r, z, t = lax.axis_index("rep"), lax.axis_index("fs"), lax.axis_index("tp")
-    y, c = lax.div(t, CORES), lax.rem(t, CORES)
-    kb = n_fs // CORES
-    half = partial.shape[0] // n_fs
-    reach = partial.shape[1] // 2
-    local = reach // CORES
-    width = g_gate.shape[1]
-    rows = g_gate.shape[0] // n_fs
-    strip = rows // 2
-    partner = {"tp": y * CORES + 1 - c}
-    across = {"rep": 1 - r}
-    beside = {"tp": (1 - y) * CORES + c}
-    owner = lax.div(z, kb)
-    grads, outs = (g_gate, g_up, g_down), (o_gate, o_up, o_down)
-
-    peers = [partner, across, beside]
-    for j in range(1, n_fs):
-        for h in range(CORES):
-            peers.append({"fs": lax.rem(z + j, n_fs), "tp": y * CORES + h})
-    greet(peers)
-
-    def slot(wide, tall, m, *where):
-        return tall.at[where] if m == 2 else wide.at[(m,) + where]
-
-    def strip_of(band, rep):
-        return pl.ds(pl.multiple_of(band * rows + rep * strip, strip), strip)
-
-    def grad_piece(m, band, rep):
-        if m == 2:
-            return grads[m].at[:, strip_of(band, rep)]
-        return grads[m].at[strip_of(band, rep), :]
-
-    def rep_of(j):
-        return 1 - r if j == 0 else r
-
-    def pair(m, k, j):
-        return remote(
-            grad_piece(m, kb * (1 - c) + k, rep_of(j)),
-            slot(pair_wide, pair_tall, m, k, j),
-            p_send.at[m, k, j],
-            p_recv.at[m, k, j],
-            partner,
-        )
-
-    def swap(m, k):
-        return remote(
-            slot(sum_wide, sum_tall, m, k),
-            slot(x_wide, x_tall, m, k),
-            x_send.at[m, k],
-            x_recv.at[m, k],
-            across,
-        )
-
-    def place(m, block, rep):
-        strips = pl.ds(pl.multiple_of(rep * strip, strip), strip)
-        blocks = pl.ds(pl.multiple_of(block * width, width), width)
-        return outs[m].at[blocks, strips] if m == 2 else outs[m].at[strips, blocks]
-
-    def deliver(m, k):
-        block = lax.rem(z, kb)
-        return remote(
-            slot(t_wide, t_tall, m, k),
-            place(m, block, r),
-            z_send.at[m, k],
-            z_recv.at[m, block],
-            {"fs": kb * c + k, "tp": y * CORES + owner},
-        )
-
-    def delivered(m, k):
-        return remote(place(m, k, r), place(m, k, r), z_send.at[m, k], z_recv.at[m, k], partner)
-
-    def keep(m, k):
-        return pltpu.make_async_copy(slot(t_wide, t_tall, m, k), place(m, k, r), own_sem.at[m])
-
-    def spread(m, k, source):
-        return remote(source, place(m, k, r), f_send.at[m, k], f_recv.at[m, k], across)
-
-    def spread_arrival(m, k):
-        return remote(
-            place(m, k, 1 - r), place(m, k, 1 - r), f_send.at[m, k], f_recv.at[m, k], across
-        )
-
-    def band_rows(band):
-        return pl.ds(pl.multiple_of(band * half, half), half)
-
-    def side_columns(which):
-        return pl.ds(pl.multiple_of(which * reach, reach), reach)
-
-    def over(j):
-        band = lax.rem(z + j, n_fs)
-        return remote(
-            partial.at[band_rows(band), side_columns(1 - y)],
-            y_buf.at[j],
-            y_send.at[j],
-            y_recv.at[j],
-            beside,
-        )
-
-    def normed_send(j):
-        return remote(
-            d_buf.at[j], z_buf.at[z], d_send.at[j], d_recv.at[z], {"fs": lax.rem(z + j, n_fs)}
-        )
-
-    def normed_arrival(j):
-        source = lax.rem(z + j, n_fs)
-        return remote(z_buf.at[source], z_buf.at[source], d_send.at[j], d_recv.at[source], partner)
-
-    def own_rows(core):
-        return pl.ds(pl.multiple_of(core * half, half), half)
-
-    def inv_send():
-        return remote(inv, o_inv.at[own_rows(c), :], n_send.at[0], n_recv.at[0], partner)
-
-    def inv_arrival():
-        at = o_inv.at[own_rows(1 - c), :]
-        return remote(at, at, n_send.at[0], n_recv.at[0], partner)
-
-    def last_send():
-        return remote(n_buf, o_normed.at[own_rows(c), :], n_send.at[1], n_recv.at[1], partner)
-
-    def last_arrival():
-        at = o_normed.at[own_rows(1 - c), :]
-        return remote(at, at, n_send.at[1], n_recv.at[1], partner)
-
-    items = [(m, k) for m in (2, 0, 1) for k in range(kb)]
-    order = list(range(1, n_fs)) + [0]
-    for m, k in items:
-        pair(m, k, 0).start()
-    for j in order:
-        over(j).start()
-    for m, k in items:
-        pair(m, k, 1).start()
-    inv_send().start()
-    o_inv[own_rows(c), :] = inv[...]
-
-    def added(m, k, j):
-        own = grad_piece(m, kb * c + k, rep_of(j))[...].astype(jnp.float32)
-        return own + slot(pair_wide, pair_tall, m, k, j)[...].astype(jnp.float32)
-
-    def put(wide, tall, m, k, value):
-        if m == 2:
-            tall[k] = value
-        else:
-            wide[m, k] = value
-
-    def first(m, k):
-        pair(m, k, 0).wait_recv()
-        put(sum_wide, sum_tall, m, k, added(m, k, 0).astype(jnp.bfloat16))
-        swap(m, k).start()
-
-    def second(m, k):
-        pair(m, k, 1).wait_recv()
-        swap(m, k).wait_recv()
-        whole = added(m, k, 1) + slot(x_wide, x_tall, m, k)[...].astype(jnp.float32)
-        put(t_wide, t_tall, m, k, whole.astype(jnp.bfloat16))
-        mine = kb * c + k == z
-
-        @pl.when(mine)
-        def _():
-            keep(m, k).start()
-            spread(m, k, slot(t_wide, t_tall, m, k)).start()
-
-        @pl.when(jnp.logical_not(mine))
-        def _():
-            deliver(m, k).start()
-
-    def third(m, k):
-        @pl.when(kb * c + k != z)
-        def _():
-            delivered(m, k).wait_recv()
-            spread(m, k, place(m, k, r)).start()
-
-    def normed_step(j):
-        over(j).wait_recv()
-        band = lax.rem(z + j, n_fs)
-        own = partial[band_rows(band), side_columns(y)].astype(jnp.float32)
-        d_buf[j] = (own + y_buf[j].astype(jnp.float32)).astype(jnp.bfloat16)
-        if j:
-            normed_send(j).start()
-
-    for m, k in items:
-        first(m, k)
-    n_items = len(items)
-    for i in range(n_items + 2):
-        if i < n_items:
-            second(*items[i])
-        if i < n_fs:
-            normed_step(order[i])
-        if i >= 2:
-            third(*items[i - 2])
-
-    for j in range(1, n_fs):
-        normed_arrival(j).wait_recv()
-    total = d_buf[0].astype(jnp.float32)
-    for j in range(1, n_fs):
-        total = total + z_buf[lax.rem(z + j, n_fs)].astype(jnp.float32)
-    total = total.astype(jnp.bfloat16)
-
-    @pl.when(c == 0)
-    def _():
-        o_normed[pl.ds(0, half), :] = total[:, :local]
-        n_buf[...] = total[:, local:]
-
-    @pl.when(c == 1)
-    def _():
-        o_normed[pl.ds(half, half), :] = total[:, local:]
-        n_buf[...] = total[:, :local]
-
-    last_send().start()
-
-    for m, k in items:
-        for j in range(2):
-            pair(m, k, j).wait_send()
-        swap(m, k).wait_send()
-        mine = kb * c + k == z
-
-        @pl.when(mine)
-        def _():
-            keep(m, k).wait()
-
-        @pl.when(jnp.logical_not(mine))
-        def _():
-            deliver(m, k).wait_send()
-
-        spread(m, k, place(m, k, r)).wait_send()
-        spread_arrival(m, k).wait_recv()
-    for j in range(n_fs):
-        over(j).wait_send()
-        if j:
-            normed_send(j).wait_send()
-    inv_send().wait_send()
-    inv_arrival().wait_recv()
-    last_send().wait_send()
-    last_arrival().wait_recv()
-
-
-def push(n_fs, partial, g_gate, g_up, g_down, inv):
-    kb = n_fs // CORES
-    half, model = partial.shape[0] // n_fs, partial.shape[1]
-    width, rows = g_gate.shape[1], g_gate.shape[0] // n_fs
-    strip = rows // 2
-    reach = model // 2
-    local = reach // CORES
-    dtype = partial.dtype
-    dma = pltpu.SemaphoreType.DMA
-    vmem = pl.BlockSpec(memory_space=pltpu.VMEM)
-    hbm = pl.BlockSpec(memory_space=pl.ANY)
-    wide, tall = (strip, width), (width, strip)
-    shapes = [(rows, kb * width)] * 2 + [(kb * width, rows)]
-    pairs = dma((3, kb, 2))
-    singles = dma((3, kb))
-    return pl.pallas_call(
-        functools.partial(push_kernel, n_fs),
-        out_shape=[jax.ShapeDtypeStruct(s, dtype) for s in shapes]
-        + [
-            jax.ShapeDtypeStruct((CORES * half, local), dtype),
-            jax.ShapeDtypeStruct((CORES * half, inv.shape[1]), inv.dtype),
-        ],
-        in_specs=[vmem] * 5,
-        out_specs=[hbm] * 3 + [vmem] * 2,
-        scratch_shapes=[
-            pltpu.VMEM((2, kb, 2) + wide, dtype),
-            pltpu.VMEM((kb, 2) + tall, dtype),
-            pltpu.VMEM((2, kb) + wide, dtype),
-            pltpu.VMEM((kb,) + tall, dtype),
-            pltpu.VMEM((2, kb) + wide, dtype),
-            pltpu.VMEM((kb,) + tall, dtype),
-            pltpu.VMEM((2, kb) + wide, dtype),
-            pltpu.VMEM((kb,) + tall, dtype),
-            pltpu.VMEM((n_fs, half, reach), dtype),
-            pltpu.VMEM((n_fs, half, reach), dtype),
-            pltpu.VMEM((n_fs, half, reach), dtype),
-            pltpu.VMEM((half, local), dtype),
             pairs,
             pairs,
             singles,
@@ -1154,13 +1255,10 @@
             dma((3,)),
         ],
         compiler_params=pltpu.CompilerParams(
-            collective_id=5, has_side_effects=True, vmem_limit_bytes=56 * 1024 * 1024
+            collective_id=4, has_side_effects=True, vmem_limit_bytes=67043328
         ),
-        cost_estimate=pl.CostEstimate(
-            flops=0, bytes_accessed=sum(2 * a * b for a, b in shapes), transcendentals=0
-        ),
-        name="push",
-    )(partial, g_gate, g_up, g_down, inv)
+        name="layer",
+    )(tokens, cot, w_gate, w_up, w_down, gain)
 
 
 def sums_kernel(n_fs, n_tp, n_rep, here, there, all_here, all_there, h_send, h_recv, o_send, o_recv):
@@ -1227,28 +1325,10 @@
     n_rep, n_fs, n_tp = lax.axis_size("rep"), lax.axis_size("fs"), lax.axis_size("tp")
     count, local = tokens.shape
     rows, wide = w_gate.shape
-    half = count // CORES
-    x, dy, f_gate, f_up, f_down = pull(n_fs, n_tp, tokens, cotangent, w_gate, w_up, w_down)
-    model = x.shape[1]
-    wide_tokens = x.astype(jnp.float32)
+    model = rows * n_fs
     gain_f = norm_gain.astype(jnp.float32)
-    inverse = lax.rsqrt(jnp.mean(wide_tokens * wide_tokens, axis=-1, keepdims=True) + 1e-06)
-    normed = (wide_tokens * inverse * gain_f).astype(jnp.bfloat16)
-    gate = jnp.dot(normed, f_gate, preferred_element_type=jnp.float32)
-    up_proj = jnp.dot(normed, f_up, preferred_element_type=jnp.float32)
-    sigma = jax.nn.sigmoid(gate)
-    active = gate * sigma
-    hidden = (active * up_proj).astype(jnp.bfloat16)
-    back = 0.5 * contract_last(dy, f_down)
-    d_up = (back * active).astype(jnp.bfloat16)
-    d_gate = (back * up_proj * sigma * (1.0 + gate * (1.0 - sigma))).astype(jnp.bfloat16)
-    partial = (contract_last(d_gate, f_gate) + contract_last(d_up, f_up)).astype(jnp.bfloat16)
-    g_down = (0.5 * contract_first(hidden, dy)).astype(jnp.bfloat16)
-    g_gate = contract_first(normed, d_gate).astype(jnp.bfloat16)
-    g_up = contract_first(normed, d_up).astype(jnp.bfloat16)
-    own = lax.dynamic_slice_in_dim(inverse, lax.axis_index("fs") * half, half, 0)
-    s_gate, s_up, s_down, d_normed, inv = push(
-        n_fs, partial, g_gate, g_up, g_down, jnp.broadcast_to(own, (half, 128))
+    s_gate, s_up, s_down, d_normed, inv = layer(
+        n_fs, tokens, cotangent, w_gate, w_up, w_down, gain_f[None, :]
     )
 
     grad_gate, grad_up, grad_down = (s.astype(jnp.float32) for s in (s_gate, s_up, s_down))

time: 271 us -> 228 us (0.84)
  matrix products: 29.5 us -> 0 us
  Pallas kernels: 220 us -> 210 us
    dot_general x8 -> x0, matrix products: 29.5 us -> none  [the longest x3 12.3 us: contract_first(): lax.dot_general(left, right, (((0,), (0,)), ((), ())), preferred_element_...]
    pallas_call x2 -> x1, Pallas kernels: 204 us -> 188 us  [layer(): pl.pallas_call(functools.partial(layer_kernel, n_fs), out_shape=[jax.Shap...]
    pallas_call x1, Pallas kernels: 16.5 us -> 22 us  [exchange_sums(): pl.pallas_call(functools.partial(sums_kernel, n_fs, n_tp, n_rep), out_sha...]
    reduce_sum x1 -> x0, other arithmetic: 2.72 us -> none  [by_chip(): jnp.mean(wide_tokens * wide_tokens, axis=-1, keepdims=True) + 1e-06]
where the time goes in v2:
time: 228 us
  Pallas kernels  210 us (92%)
  other arithmetic  14.3 us (6%)
  local copies, waits for them, and re-layouts  2.83 us (1%)
    pallas_call x1, Pallas kernels, layer(): pl.pallas_call(functools.partial(layer_kernel, n_fs), out_shape=[jax.Shap...  188 us
    pallas_call x1, Pallas kernels, exchange_sums(): pl.pallas_call(functools.partial(sums_kernel, n_fs, n_tp, n_rep), out_sha...  22 us

profile of v2, /device:TPU:0, one launch (start us, length us, event | category | flops | bytes accessed | tf_op | source)
XLA Modules:
  0.0 228.0 jit_solution(1639171770243477056)
XLA Ops:
  0.6 1.3 dynamic_slice.3
  2.0 1.3 convert_element_type.29
  3.3 188.2 %layer.1 = (bf16[512,1280]{1,0:T(8,128)(2,1)}, bf16[512,1280]{1,0:T(8,128)(2,1)}, bf16[1280,512]{1,0:T(8,128)(2,1)}, bf16[384,512]{1,0:T(8,128)(2,1)}, f32[384,128]{1,0:T(8,128)}) custom-call(bf16[384,512]{1,0:T(8,128)(2,1)} %refs_0_.1, bf16[384,512]{1,0:T(8,128)(2,1)} %refs_1_.1, bf16[512,1280]{1,0:T(8,128)(2,1)} %refs_2_.1, bf16[512,1280]{1,0:T(8,128)(2,1)} %refs_3_.1, ...), custom_call_target="tpu_custom_call" | custom-call | tf_op jit(solution)/shard_map/layer/pallas_call | solution.py:1186
  191.4 1.1 fusion.9
  192.5 1.5 fusion.8
  194.0 0.0 copy-start.3
  194.0 4.4 %multiply_reduce_fusion.1 = (f32[512]{0:T(512)S(1)}, f32[512,1280]{1,0:T(8,128)}, f32[512]{0:T(512)S(1)}, f32[512,1280]{1,0:T(8,128)}) fusion(bf16[512,1280]{1,0:T(8,128)(2,1)} %get-tuple-element.17, bf16[512,1280]{1,0:T(8,128)(2,1)} %get-tuple-element.16), kind=kLoop, calls=%fused_computation.1 | loop fusion | flops 3931136 | bytes 7868416 | tf_op jit(solution)/shard_map/reduce_sum | solution.py:1344
  198.4 0.0 copy-start
  198.4 0.0 copy-start.1
  198.4 0.0 copy-start.2
  198.4 0.0 copy-start.4
  198.4 0.6 fusion.11.here
  199.1 0.0 copy-done.3
  199.1 1.7 multiply_reduce_fusion
  200.8 0.6 fusion.10.there
  201.4 22.0 %exchange_sums.1 = (f32[4,16,128]{2,1,0:T(8,128)}, f32[8,16,128]{2,1,0:T(8,128)}) custom-call(f32[16,128]{1,0:T(8,128)} %fusion.11.here, f32[16,128]{1,0:T(8,128)} %fusion.10.there), custom_call_target="tpu_custom_call" | custom-call | tf_op jit(solution)/shard_map/exchange_sums/pallas_call | solution.py:1304
  223.4 0.8 reduce_sum.77
  224.2 0.0 copy-done
  224.2 0.0 copy-done.1
  224.2 0.0 copy-done.2
  224.2 0.0 copy-done.4
  224.2 1.1 fusion.3
  225.3 0.9 reshape.35
  226.2 0.6 slice_reduce_fusion.1
  226.8 0.6 slice_reduce_fusion.2
  227.4 0.6 reshape.36
  (2 shorter events, 0.0 us)
Async XLA Ops:
  194.0 5.1 %copy-start.3 = (bf16[1280,512]{1,0:T(8,128)(2,1)S(1)}, bf16[1280,512]{1,0:T(8,128)(2,1)}, u32[]{:S(2)}) copy-start(bf16[1280,512]{1,0:T(8,128)(2,1)} %get-tuple-element.18) | copy-start | bytes 3932164
  198.4 25.8 %copy-start = (bf16[384,512]{1,0:T(8,128)(2,1)S(1)}, bf16[384,512]{1,0:T(8,128)(2,1)}, u32[]{:S(2)}) copy-start(bf16[384,512]{1,0:T(8,128)(2,1)} %refs_0_.1) | copy-start | bytes 1179652
  198.4 25.8 %copy-start.1 = (bf16[384,512]{1,0:T(8,128)(2,1)S(1)}, bf16[384,512]{1,0:T(8,128)(2,1)}, u32[]{:S(2)}) copy-start(bf16[384,512]{1,0:T(8,128)(2,1)} %refs_1_.1) | copy-start | bytes 1179652
  198.4 25.8 %copy-start.2 = (bf16[384,512]{1,0:T(8,128)(2,1)S(1)}, bf16[384,512]{1,0:T(8,128)(2,1)}, u32[]{:S(2)}) copy-start(bf16[384,512]{1,0:T(8,128)(2,1)} %get-tuple-element.15) | copy-start | bytes 1179652
  198.4 25.8 %copy-start.4 = (f32[512]{0:T(512)S(1)}, f32[512]{0:T(512)}, u32[]{:S(2)}) copy-start(f32[512]{0:T(512)} %dynamic_slice.3) | copy-start | bytes 6148

commit v3 on v2

--- a/solution.py
+++ b/solution.py
@@ -491,23 +491,27 @@
     return z <= n_fs - 2 if side == 0 else z >= 1
 
 
-def layer_kernel(n_fs, *refs):
+def layer_kernel(n_fs, n_tp, *refs):
     tokens, cot, w_gate, w_up, w_down, gain = refs[:6]
-    o_gate, o_up, o_down, o_normed, o_inv = refs[6:11]
-    full = refs[11:16]
+    o_gate, o_up, o_down, o_tokens, o_gain, o_wide_sq, o_tall_sq = refs[6:13]
+    full = refs[13:18]
     x_full, dy_full, f_gate, f_up, f_down = full
-    normed, normed_t, hidden_t, act_f, slope_f, d_gate, d_up, inv_all = refs[16:24]
-    g_gate, g_up, g_down = refs[24:27]
-    pair_wide, pair_tall, sum_wide, sum_tall, x_wide, x_tall, t_wide, t_tall = refs[27:35]
-    y_buf, d_buf, z_buf, n_buf = refs[35:39]
-    (load_sem, az_own, az_fwd, az_recv, ay_own, ay_fwd, ay_recv, ap_send, ap_recv) = refs[39:48]
-    (w_send, w_recv, wx_send, wx_recv, wp_send, wp_recv, wo_send, wo_recv) = refs[48:56]
-    (p_send, p_recv, x_send, x_recv, z_send, z_recv, f_send, f_recv) = refs[56:64]
-    (y_send, y_recv, d_send, d_recv, n_send, n_recv, own_sem) = refs[64:]
+    normed, normed_t, hidden_t, act_f, slope_f, d_gate, d_up, inv_all = refs[18:26]
+    g_gate, g_up, g_down = refs[26:29]
+    pair_wide, pair_tall, sum_wide, sum_tall, x_wide, x_tall, t_wide, t_tall = refs[29:37]
+    y_buf, d_buf, z_buf, n_buf = refs[37:41]
+    v_gate, v_up, v_down, v_tokens, v_cot, v_normed, v_inv, v_out = refs[41:49]
+    lane_sq, row_all, gain_all, wide_all, tall_all = refs[49:54]
+    (load_sem, az_own, az_fwd, az_recv, ay_own, ay_fwd, ay_recv, ap_send, ap_recv) = refs[54:63]
+    (w_send, w_recv, wx_send, wx_recv, wp_send, wp_recv, wo_send, wo_recv) = refs[63:71]
+    (p_send, p_recv, x_send, x_recv, z_send, z_recv, f_send, f_recv) = refs[71:79]
+    (y_send, y_recv, d_send, d_recv, n_send, n_recv, own_sem) = refs[79:86]
+    (row_send, row_recv, gain_send, gain_recv) = refs[86:90]
+    (wide_send, wide_recv, tall_send, tall_recv, out_sem, total, gain_sum) = refs[90:]
     r, z, t = lax.axis_index("rep"), lax.axis_index("fs"), lax.axis_index("tp")
     y, c = lax.div(t, CORES), lax.rem(t, CORES)
     acts, weights = (tokens, cot), (w_gate, w_up, w_down)
-    grads, outs = (g_gate, g_up, g_down), (o_gate, o_up, o_down)
+    grads, outs = (g_gate, g_up, g_down), (v_gate, v_up, v_down)
     half, local = tokens.shape[0] // CORES, tokens.shape[1]
     count, model = x_full.shape
     rows = w_gate.shape[0]
@@ -525,6 +529,7 @@
     for j in range(1, n_fs):
         for h in range(CORES):
             peers.append({"fs": lax.rem(z + j, n_fs), "tp": y * CORES + h})
+        peers.append({"rep": 1 - r, "fs": lax.rem(z + j, n_fs)})
     greet(peers)
 
     def own_act(a, h):
@@ -721,7 +726,7 @@
         return remote(place(m, k, r), place(m, k, r), z_send.at[m, k], z_recv.at[m, k], partner)
 
     def keep(m, k):
-        return pltpu.make_async_copy(slot(t_wide, t_tall, m, k), place(m, k, r), own_sem.at[m])
+        return pltpu.make_async_copy(slot(t_wide, t_tall, m, k), place(m, k, r), own_sem.at[m, k])
 
     def spread(m, k, source):
         return remote(source, place(m, k, r), f_send.at[m, k], f_recv.at[m, k], across)
@@ -737,40 +742,54 @@
     def side_columns(which):
         return pl.ds(pl.multiple_of(which * reach, reach), reach)
 
-    def over(j):
-        band = lax.rem(z + j, n_fs)
+    def over(band):
         return remote(
             x_full.at[band_rows(band), side_columns(1 - y)],
-            y_buf.at[j],
-            y_send.at[j],
-            y_recv.at[j],
+            y_buf.at[band],
+            y_send.at[band],
+            y_recv.at[band],
             beside,
         )
 
-    def normed_send(j):
-        return remote(
-            d_buf.at[j], z_buf.at[z], d_send.at[j], d_recv.at[z], {"fs": lax.rem(z + j, n_fs)}
-        )
-
-    def normed_arrival(j):
-        source = lax.rem(z + j, n_fs)
-        return remote(z_buf.at[source], z_buf.at[source], d_send.at[j], d_recv.at[source], partner)
+    low = z < n_fs // 2
+    inner = jnp.logical_and(z > 0, z < n_fs - 1)
+    line_slot = jnp.where(low, 0, 1)
+
+    def line_band(i):
+        return jnp.where(low, n_fs - 1 - i, i)
+
+    def y_turn(i):
+        return jnp.where(jnp.logical_and(inner, i >= 2), n_fs + 1 - i, i)
+
+    def line_send(i, target):
+        band = line_band(i)
+        return remote(
+            d_buf.at[i],
+            z_buf.at[line_slot, band],
+            d_send.at[i],
+            d_recv.at[line_slot, band],
+            {"fs": target},
+        )
+
+    def line_arrival(which, band):
+        place = z_buf.at[which, band]
+        return remote(place, place, d_send.at[0], d_recv.at[which, band], partner)
 
     def own_rows(core):
         return pl.ds(pl.multiple_of(core * half, half), half)
 
     def inv_send():
-        return remote(inv_all.at[band_rows(z), :], o_inv.at[own_rows(c), :], n_send.at[0], n_recv.at[0], partner)
+        return remote(inv_all.at[band_rows(z), :], v_inv.at[own_rows(c), :], n_send.at[0], n_recv.at[0], partner)
 
     def inv_arrival():
-        at = o_inv.at[own_rows(1 - c), :]
+        at = v_inv.at[own_rows(1 - c), :]
         return remote(at, at, n_send.at[0], n_recv.at[0], partner)
 
     def last_send():
-        return remote(n_buf, o_normed.at[own_rows(c), :], n_send.at[1], n_recv.at[1], partner)
+        return remote(n_buf, v_normed.at[own_rows(c), :], n_send.at[1], n_recv.at[1], partner)
 
     def last_arrival():
-        at = o_normed.at[own_rows(1 - c), :]
+        at = v_normed.at[own_rows(1 - c), :]
         return remote(at, at, n_send.at[1], n_recv.at[1], partner)
 
     def loaded(a):
@@ -841,6 +860,14 @@
                     weight_across_arrival(m, source).wait_recv()
                     weight_beside(m, source, 1).start()
 
+    def weight_all(m):
+        for d in range(1, n_fs):
+            weight_round((m,), d)
+
+    def across_all(m):
+        for d in range(1, n_fs):
+            across_round((m,), d)
+
     def act_ready(a):
         for d in range(1, n_fs):
             for side in range(2):
@@ -925,7 +952,7 @@
         at = tile(i, LANES)
         wide = x_full[at, :].astype(jnp.float32)
         inv = lax.rsqrt(jnp.mean(wide * wide, axis=-1, keepdims=True) + 1e-06)
-        value = wide * inv * gain[...]
+        value = wide * inv * gain[...].astype(jnp.float32)
         normed[at, :] = value.astype(jnp.bfloat16)
         normed_t[:, at] = value.T.astype(jnp.bfloat16)
         inv_all[at, :] = jnp.broadcast_to(inv, (LANES, LANES))
@@ -1012,14 +1039,196 @@
             delivered(m, k).wait_recv()
             spread(m, k, place(m, k, r)).start()
 
-    def normed_step(j):
-        over(j).wait_recv()
-        band = lax.rem(z + j, n_fs)
+    def own_share(band):
+        over(band).wait_recv()
         own = x_full[band_rows(band), side_columns(y)].astype(jnp.float32)
-        d_buf[j] = (own + y_buf[j].astype(jnp.float32)).astype(jnp.bfloat16)
-        if j:
-            normed_send(j).start()
-
+        return own + y_buf[band].astype(jnp.float32)
+
+    def line_target(i):
+        if i == n_fs - 1:
+            return jnp.where(low, z - 1, z + 1)
+        return line_band(i)
+
+    def normed_outer(i):
+        @pl.when(jnp.logical_not(inner))
+        def _():
+            d_buf[i] = own_share(line_band(i)).astype(jnp.bfloat16)
+            line_send(i, jnp.where(low, z + 1, z - 1)).start()
+
+    def normed_inner(i):
+        @pl.when(inner)
+        def _():
+            band = line_band(i)
+            value = own_share(band)
+            if i < n_fs - 1:
+                line_arrival(line_slot, band).wait_recv()
+                value = value + z_buf[line_slot, band].astype(jnp.float32)
+            d_buf[i] = value.astype(jnp.bfloat16)
+            line_send(i, line_target(i)).start()
+
+    def normed_sent():
+        for i in range(n_fs):
+            if i < n_fs - 1:
+
+                @pl.when(jnp.logical_not(inner))
+                def _():
+                    line_send(i, jnp.where(low, z + 1, z - 1)).wait_send()
+
+            if i != n_fs - 2:
+
+                @pl.when(inner)
+                def _():
+                    line_send(i, line_target(i)).wait_send()
+
+    def normed_last():
+        value = own_share(z)
+        for which in range(2):
+            line_arrival(which, z).wait_recv()
+            value = value + z_buf[which, z].astype(jnp.float32)
+        total[...] = value
+
+        for core in range(CORES):
+
+            @pl.when(c == core)
+            def _():
+                mine = slice(core * local, (core + 1) * local)
+                theirs = slice((1 - core) * local, (2 - core) * local)
+                v_normed[core * half : (core + 1) * half, :] = total[:, mine].astype(jnp.bfloat16)
+                n_buf[...] = total[:, theirs].astype(jnp.bfloat16)
+
+        last_send().start()
+
+    def fold(value):
+        out = value[:, :LANES]
+        for i in range(1, value.shape[1] // LANES):
+            out = out + value[:, i * LANES : (i + 1) * LANES]
+        return out
+
+    def row_of(value):
+        return jnp.sum(value.T, axis=0, keepdims=True)
+
+    def lane_peer(j):
+        return {"tp": lax.rem(t + j, n_tp)}
+
+    def group_peer(j):
+        at = lax.rem(r * n_fs + z + j, 2 * n_fs)
+        return {"rep": lax.div(at, n_fs), "fs": lax.rem(at, n_fs)}
+
+    def fan(buffer, count_of, mine, send, recv, peer):
+        def sent(j):
+            return remote(
+                buffer.at[mine], buffer.at[mine], send.at[j - 1], recv.at[count_of - j - 1], peer(j)
+            )
+
+        def received(j):
+            place = buffer.at[lax.rem(mine + j, count_of)]
+            return remote(place, place, send.at[j - 1], recv.at[j - 1], peer(j))
+
+        return sent, received
+
+    row_fan = fan(row_all, n_tp, t, row_send, row_recv, lane_peer)
+    wide_fan = fan(wide_all, n_tp, t, wide_send, wide_recv, lane_peer)
+    gain_fan = fan(gain_all, 2 * n_fs, r * n_fs + z, gain_send, gain_recv, group_peer)
+    tall_fan = fan(
+        tall_all, n_fs, z, tall_send, tall_recv, lambda j: {"fs": lax.rem(z + j, n_fs)}
+    )
+
+    def fan_start(pair_of, count_of):
+        for j in range(1, count_of):
+            pair_of[0](j).start()
+
+    def fan_ready(pair_of, count_of):
+        for j in range(1, count_of):
+            pair_of[1](j).wait_recv()
+
+    def fan_sent(pair_of, count_of):
+        for j in range(1, count_of):
+            pair_of[0](j).wait_send()
+
+    def gain_here():
+        return gain[:, pl.ds(pl.multiple_of(t * local, local), local)].astype(jnp.float32)
+
+    def token_sums():
+        last_arrival().wait_recv()
+        inv_arrival().wait_recv()
+        for i in range(2):
+            own_loaded(i).wait()
+        gain_l = gain_here()
+        gain_sum[...] = jnp.zeros_like(gain_sum)
+
+        @pl.loop(0, CORES * half // LANES)
+        def _(i):
+            at = tile(i, LANES)
+            d_tokens = v_normed[at, :].astype(jnp.float32) * v_tokens[at, :].astype(jnp.float32)
+            row_all[t, :, at] = row_of(fold(d_tokens * gain_l))
+            inv = v_inv[at, :1]
+            gain_sum[...] += jnp.sum(d_tokens * inv, axis=0, keepdims=True)
+
+        gain_all[r * n_fs + z] = gain_sum[...]
+        fan_start(row_fan, n_tp)
+        fan_start(gain_fan, 2 * n_fs)
+
+    def token_grads():
+        fan_ready(row_fan, n_tp)
+        gain_l = gain_here()
+
+        @pl.loop(0, CORES * half // LANES)
+        def _(i):
+            at = tile(i, LANES)
+            dots = row_all[0, :, at]
+            for j in range(1, n_tp):
+                dots = dots + row_all[j, :, at]
+            rowdot = jnp.broadcast_to(dots, (LANES, LANES)).T[:, :1]
+            inv = v_inv[at, :1]
+            value = v_cot[at, :].astype(jnp.float32)
+            value = value + inv * (v_normed[at, :].astype(jnp.float32) * gain_l)
+            scale = inv**3 * rowdot / model
+            value = value - v_tokens[at, :].astype(jnp.float32) * scale
+            v_out[at, :] = value.astype(jnp.bfloat16)
+
+        pltpu.make_async_copy(v_out, o_tokens, out_sem.at[3, 0]).start()
+
+    def own_loaded(i):
+        source, target = ((tokens, v_tokens), (cot, v_cot))[i]
+        return pltpu.make_async_copy(source, target, load_sem.at[5 + i])
+
+    def block_out(m, k):
+        at = pl.ds(k * width, width)
+        if m == 2:
+            return pltpu.make_async_copy(v_down.at[at, :], o_down.at[at, :], out_sem.at[m, k])
+        return pltpu.make_async_copy(
+            outs[m].at[:, at], (o_gate, o_up)[m].at[:, at], out_sem.at[m, k]
+        )
+
+    def squares(m, k):
+        spread_arrival(m, k).wait_recv()
+        mine = kb * c + k == z
+
+        @pl.when(mine)
+        def _():
+            keep(m, k).wait()
+
+        block_out(m, k).start()
+        if m == 2:
+
+            @pl.loop(0, width // LANES)
+            def _(i):
+                at = pl.ds(pl.multiple_of(k * width + i * LANES, LANES), LANES)
+                value = v_down[at, :].astype(jnp.float32)
+                tall_all[z, :, at] = row_of(fold(value * value))
+        else:
+
+            @pl.loop(0, rows // LANES)
+            def _(i):
+                at = tile(i, LANES)
+                value = outs[m][at, k * width : (k + 1) * width].astype(jnp.float32)
+                part = fold(value * value)
+                if k > 0:
+                    part = part + lane_sq[m, at, :]
+                if k < kb - 1:
+                    lane_sq[m, at, :] = part
+                else:
+                    wide_all[t, m : m + 1, at] = row_of(part)
 
     for a in range(2):
         loaded(a).start()
@@ -1032,134 +1241,134 @@
     act_start(0)
     own_start(0)
     own_start(1)
+    for i in range(2):
+        own_loaded(i).start()
     act_round(0, 1)
+    act_round(0, 2)
     weight_start(0)
     weight_start(1)
-    act_round(0, 2)
     act_start(1)
     own_start(2)
     for d in range(3, n_fs):
         act_round(0, d)
-    weight_round((0, 1), 1)
-    weight_round((0, 1), 2)
-    across_round((0, 1), 1)
+    weight_all(0)
     act_round(1, 1)
-    weight_start(2)
-    for d in range(3, n_fs):
-        weight_round((0, 1), d)
-        across_round((0, 1), d - 1)
-    act_round(1, 2)
-    across_round((0, 1), n_fs - 1)
+    weight_all(1)
+    across_all(0)
     act_ready(0)
     pl.loop(0, count // LANES)(normalize)
-    weight_round((2,), 1)
+    inv_send().start()
+    v_inv[own_rows(c), :] = inv_all[band_rows(z), :]
+    weight_start(2)
+    across_all(1)
+    act_round(1, 2)
     weight_ready((0, 1))
     pl.loop(0, count // TILE)(forward)
+    weight_all(2)
     for d in range(3, n_fs):
         act_round(1, d)
-    weight_round((2,), 2)
-    across_round((2,), 1)
-    for d in range(3, n_fs):
-        weight_round((2,), d)
-        across_round((2,), d - 1)
+    across_all(2)
     act_ready(1)
     gradients(2, 0)
-    across_round((2,), n_fs - 1)
     for k in range(kb):
         first(2, k)
     gradients(2, 1)
     weight_ready((2,))
     pl.loop(0, count // TILE)(backward)
+    act_sent(0)
+
+    @pl.loop(0, n_fs)
+    def _(i):
+        band = line_band(y_turn(i))
+        pull_back(band, 1 - y)
+        over(band).start()
+
     gradients(0, 0)
     for k in range(kb):
         first(0, k)
-    for k in range(kb):
-        second(2, k)
     gradients(1, 0)
     for k in range(kb):
         first(1, k)
     gradients(0, 1)
-    act_sent(0)
-
-    @pl.loop(0, n_fs)
-    def _(i):
-        j = lax.rem(i + 1, n_fs)
-        pull_back(lax.rem(z + j, n_fs), 1 - y)
-        over(j).start()
-
-    gradients(1, 1)
     for k in range(kb):
-        third(2, k)
+        second(2, k)
 
     @pl.loop(0, n_fs)
     def _(i):
         pull_back(i, y)
 
-    inv_send().start()
-    o_inv[own_rows(c), :] = inv_all[band_rows(z), :]
-    order = list(range(1, n_fs)) + [0]
-    items = [(m, k) for m in range(2) for k in range(kb)]
-    n_items = len(items)
-    for i in range(n_items + 2):
-        if i < n_items:
-            second(*items[i])
-        if i < n_fs:
-            normed_step(order[i])
-        if i >= 2:
-            third(*items[i - 2])
-    items += [(2, k) for k in range(kb)]
-
+    gradients(1, 1)
+    second(0, 0)
+    normed_outer(0)
+    second(0, 1)
+    third(2, 0)
+    third(2, 1)
+    normed_outer(1)
+    second(1, 0)
+    normed_inner(n_fs - 1)
+    normed_inner(0)
+    second(1, 1)
+    normed_outer(2)
+    third(0, 0)
+    third(0, 1)
+    normed_inner(1)
+    third(1, 0)
+    third(1, 1)
+    normed_last()
+    squares(2, 0)
+    squares(2, 1)
+    fan_start(tall_fan, n_fs)
+    token_sums()
+    squares(0, 0)
+    squares(0, 1)
+    token_grads()
+    squares(1, 0)
+    squares(1, 1)
+    fan_start(wide_fan, n_tp)
+    fan_ready(gain_fan, 2 * n_fs)
+    gain_total = gain_all[0]
+    for j in range(1, 2 * n_fs):
+        gain_total = gain_total + gain_all[j]
+    o_gain[...] = gain_total
+    fan_ready(tall_fan, n_fs)
+    tall_total = tall_all[0]
     for j in range(1, n_fs):
-        normed_arrival(j).wait_recv()
-    total = d_buf[0].astype(jnp.float32)
-    for j in range(1, n_fs):
-        total = total + z_buf[lax.rem(z + j, n_fs)].astype(jnp.float32)
-    total = total.astype(jnp.bfloat16)
-
-    @pl.when(c == 0)
-    def _():
-        o_normed[pl.ds(0, half), :] = total[:, :local]
-        n_buf[...] = total[:, local:]
-
-    @pl.when(c == 1)
-    def _():
-        o_normed[pl.ds(half, half), :] = total[:, local:]
-        n_buf[...] = total[:, :local]
-
-    last_send().start()
-
-    for m, k in items:
-        for j in range(2):
-            pair(m, k, j).wait_send()
-        swap(m, k).wait_send()
-        mine = kb * c + k == z
-
-        @pl.when(mine)
-        def _():
-            keep(m, k).wait()
-
-        @pl.when(jnp.logical_not(mine))
-        def _():
-            deliver(m, k).wait_send()
-
-        spread(m, k, place(m, k, r)).wait_send()
-        spread_arrival(m, k).wait_recv()
-    for j in range(n_fs):
-        over(j).wait_send()
-        if j:
-            normed_send(j).wait_send()
+        tall_total = tall_total + tall_all[j]
+    o_tall_sq[...] = tall_total
+
+    for m in range(3):
+        for k in range(kb):
+            for j in range(2):
+                pair(m, k, j).wait_send()
+            swap(m, k).wait_send()
+
+            @pl.when(kb * c + k != z)
+            def _():
+                deliver(m, k).wait_send()
+
+            spread(m, k, place(m, k, r)).wait_send()
+            block_out(m, k).wait()
+    pltpu.make_async_copy(v_out, o_tokens, out_sem.at[3, 0]).wait()
+    for b in range(n_fs):
+        over(b).wait_send()
+    normed_sent()
     inv_send().wait_send()
-    inv_arrival().wait_recv()
     last_send().wait_send()
-    last_arrival().wait_recv()
-
-
     act_sent(1)
     for m in range(3):
         weight_sent(m)
-
-
-def layer(n_fs, tokens, cot, w_gate, w_up, w_down, gain):
+    fan_sent(row_fan, n_tp)
+    fan_sent(gain_fan, 2 * n_fs)
+    fan_sent(tall_fan, n_fs)
+    fan_ready(wide_fan, n_tp)
+    wide_total = wide_all[0]
+    for j in range(1, n_tp):
+        wide_total = wide_total + wide_all[j]
+    o_wide_sq[...] = wide_total
+    fan_sent(wide_fan, n_tp)
+
+
+def layer(n_fs, n_tp, tokens, cot, w_gate, w_up, w_down, gain):
     half, local = tokens.shape[0] // CORES, tokens.shape[1]
     rows, hidden = w_gate.shape
     width = hidden * CORES // n_fs
@@ -1182,16 +1391,15 @@
     def f32(*shape):
         return pltpu.VMEM(shape, jnp.float32)
 
-    shapes = [(rows, kb * width)] * 2 + [(kb * width, rows)]
+    hidden = kb * width
+    shapes = [(rows, hidden)] * 2 + [(hidden, rows)]
     return pl.pallas_call(
-        functools.partial(layer_kernel, n_fs),
+        functools.partial(layer_kernel, n_fs, n_tp),
         out_shape=[jax.ShapeDtypeStruct(s, dtype) for s in shapes]
-        + [
-            jax.ShapeDtypeStruct((CORES * half, local), dtype),
-            jax.ShapeDtypeStruct((CORES * half, LANES), jnp.float32),
-        ],
+        + [jax.ShapeDtypeStruct((CORES * half, local), dtype)]
+        + [jax.ShapeDtypeStruct(s, jnp.float32) for s in ((1, local), (2, rows), (1, hidden))],
         in_specs=[hbm] * 5 + [vmem],
-        out_specs=[hbm] * 3 + [vmem] * 2,
+        out_specs=[hbm] * 4 + [vmem] * 3,
         scratch_shapes=[
             bf(count, model),
             bf(count, model),
@@ -1219,9 +1427,22 @@
             bf(kb, *tall),
             bf(n_fs, half, reach),
             bf(n_fs, half, reach),
-            bf(n_fs, half, reach),
+            bf(2, n_fs, half, reach),
             bf(half, local),
-            dma((5,)),
+            bf(rows, hidden),
+            bf(rows, hidden),
+            bf(hidden, rows),
+            bf(CORES * half, local),
+            bf(CORES * half, local),
+            bf(CORES * half, local),
+            f32(CORES * half, LANES),
+            bf(CORES * half, local),
+            f32(2, rows, LANES),
+            f32(n_tp, 1, CORES * half),
+            f32(2 * n_fs, 1, local),
+            f32(n_tp, 2, rows),
+            f32(n_fs, 1, hidden),
+            dma((7,)),
             dma((2, 2, CORES)),
             line,
             line,
@@ -1249,10 +1470,21 @@
             dma((n_fs,)),
             dma((n_fs,)),
             dma((n_fs,)),
-            dma((n_fs,)),
+            dma((2, n_fs)),
             dma((2,)),
             dma((2,)),
-            dma((3,)),
+            dma((3, kb)),
+            dma((n_tp - 1,)),
+            dma((n_tp - 1,)),
+            dma((2 * n_fs - 1,)),
+            dma((2 * n_fs - 1,)),
+            dma((n_tp - 1,)),
+            dma((n_tp - 1,)),
+            dma((n_fs - 1,)),
+            dma((n_fs - 1,)),
+            dma((4, kb)),
+            f32(half, reach),
+            f32(1, local),
         ],
         compiler_params=pltpu.CompilerParams(
             collective_id=4, has_side_effects=True, vmem_limit_bytes=67043328
@@ -1261,108 +1493,19 @@
     )(tokens, cot, w_gate, w_up, w_down, gain)
 
 
-def sums_kernel(n_fs, n_tp, n_rep, here, there, all_here, all_there, h_send, h_recv, o_send, o_recv):
-    r, z, t = lax.axis_index("rep"), lax.axis_index("fs"), lax.axis_index("tp")
-    groups = n_rep * n_fs
-    spot = r * n_fs + z
-
-    def group_of(j):
-        at = lax.rem(spot + j, groups)
-        return {"rep": lax.div(at, n_fs), "fs": lax.rem(at, n_fs)}
-
-    def lane_of(j):
-        return {"tp": lax.rem(t + j, n_tp)}
-
-    greet([lane_of(j) for j in range(1, n_tp)] + [group_of(j) for j in range(1, groups)])
-    sends = []
-    for j in range(1, n_tp):
-        sends.append(
-            remote(here, all_here.at[t], h_send.at[j - 1], h_recv.at[n_tp - j - 1], lane_of(j))
-        )
-    for j in range(1, groups):
-        sends.append(
-            remote(there, all_there.at[spot], o_send.at[j - 1], o_recv.at[groups - j - 1], group_of(j))
-        )
-    for copy in sends:
-        copy.start()
-    all_here[t] = here[...]
-    all_there[spot] = there[...]
-    for j in range(1, n_tp):
-        place = all_here.at[lax.rem(t + j, n_tp)]
-        remote(place, place, h_send.at[j - 1], h_recv.at[j - 1], lane_of(j)).wait_recv()
-    for j in range(1, groups):
-        place = all_there.at[lax.rem(spot + j, groups)]
-        remote(place, place, o_send.at[j - 1], o_recv.at[j - 1], group_of(j)).wait_recv()
-    for copy in sends:
-        copy.wait_send()
-
-
-def exchange_sums(n_fs, n_tp, n_rep, here, there):
-    dma = pltpu.SemaphoreType.DMA
-    vmem = pl.BlockSpec(memory_space=pltpu.VMEM)
-    groups = n_rep * n_fs
-    return pl.pallas_call(
-        functools.partial(sums_kernel, n_fs, n_tp, n_rep),
-        out_shape=[
-            jax.ShapeDtypeStruct((n_tp,) + here.shape, here.dtype),
-            jax.ShapeDtypeStruct((groups,) + there.shape, there.dtype),
-        ],
-        in_specs=[vmem] * 2,
-        out_specs=[vmem] * 2,
-        scratch_shapes=[dma((n_tp - 1,)), dma((n_tp - 1,)), dma((groups - 1,)), dma((groups - 1,))],
-        compiler_params=pltpu.CompilerParams(collective_id=6, has_side_effects=True),
-        name="exchange_sums",
-    )(here, there)
-
-
-def packed(parts):
-    flat = jnp.concatenate([p.reshape(-1) for p in parts])
-    size = -(-flat.shape[0] // 1024) * 1024
-    return jnp.pad(flat, (0, size - flat.shape[0])).reshape(-1, 128)
-
-
 def by_chip(tokens, norm_gain, w_gate, w_up, w_down, cotangent):
-    n_rep, n_fs, n_tp = lax.axis_size("rep"), lax.axis_size("fs"), lax.axis_size("tp")
-    count, local = tokens.shape
-    rows, wide = w_gate.shape
-    model = rows * n_fs
-    gain_f = norm_gain.astype(jnp.float32)
-    s_gate, s_up, s_down, d_normed, inv = layer(
-        n_fs, tokens, cotangent, w_gate, w_up, w_down, gain_f[None, :]
+    s_gate, s_up, s_down, grad_tokens, grad_gain, gate_up_sq, down_sq = layer(
+        lax.axis_size("fs"),
+        lax.axis_size("tp"),
+        tokens,
+        cotangent,
+        w_gate,
+        w_up,
+        w_down,
+        norm_gain[None, :],
     )
-
     grad_gate, grad_up, grad_down = (s.astype(jnp.float32) for s in (s_gate, s_up, s_down))
-    d_normed = d_normed.astype(jnp.float32)
-    inv = inv[:, :1]
-    gain_here = lax.dynamic_slice_in_dim(gain_f, lax.axis_index("tp") * local, local, 0)
-    local_tokens = tokens.astype(jnp.float32)
-    scaled = d_normed * gain_here
-    here = packed(
-        [
-            jnp.sum(scaled * local_tokens, axis=-1),
-            jnp.sum(grad_gate * grad_gate, axis=1),
-            jnp.sum(grad_up * grad_up, axis=1),
-        ]
-    )
-    there = packed(
-        [
-            jnp.sum(d_normed * local_tokens * inv, axis=0),
-            jnp.sum(grad_down * grad_down, axis=1),
-        ]
-    )
-    all_here, all_there = exchange_sums(n_fs, n_tp, n_rep, here, there)
-    here = jnp.sum(all_here, axis=0).reshape(-1)
-    rowdot = here[:count]
-    gate_up_sq = here[count : count + 2 * rows].reshape(2, rows)
-    flat = all_there.reshape(n_rep, n_fs, -1)
-    grad_gain = jnp.sum(flat[:, :, :local], axis=(0, 1))
-    down_sq = jnp.sum(flat[0, :, local : local + wide], axis=0)
-    grad_tokens = (
-        cotangent.astype(jnp.float32)
-        + inv * scaled
-        - local_tokens * inv**3 * rowdot[:, None] / model
-    ).astype(jnp.bfloat16)
-    return (grad_tokens, grad_gain, grad_gate, grad_up, grad_down, gate_up_sq, down_sq)
+    return (grad_tokens, grad_gain[0], grad_gate, grad_up, grad_down, gate_up_sq, down_sq[0])
 
 
 def fits_chips(mesh):

time: 228 us -> 204 us (0.89)
  Pallas kernels: 210 us -> 193 us
  other arithmetic: 14.3 us -> 7.24 us
    pallas_call x2 -> x1, Pallas kernels: 210 us -> 193 us  [layer(): pl.pallas_call(functools.partial(layer_kernel, n_fs, n_tp), out_shape=[ja...]
    reduce_sum x6 -> x0, other arithmetic: 9.6 us -> none  [the longest x1 4.42 us: by_chip(): jnp.sum(grad_up * grad_up, axis=1)]
    convert_element_type x2 -> x3, other arithmetic: 2.35 us -> 6.62 us  [by_chip(): s.astype(jnp.float32)]
where the time goes in v3:
time: 204 us
  Pallas kernels  193 us (95%)
  other arithmetic  7.24 us (4%)
  local copies, waits for them, and re-layouts  3.23 us (2%)
    pallas_call x1, Pallas kernels, layer(): pl.pallas_call(functools.partial(layer_kernel, n_fs, n_tp), out_shape=[ja...  193 us
    convert_element_type x3, other arithmetic, by_chip(): s.astype(jnp.float32)  6.62 us

profile of v3, /device:TPU:0, one launch (start us, length us, event | category | flops | bytes accessed | tf_op | source)
XLA Modules:
  0.0 204.0 jit_solution(16345050390366731008)
XLA Ops:
  0.6 1.3 broadcast_in_dim.3.refs_5_
  1.9 192.9 %layer.1 = (bf16[512,1280]{1,0:T(8,128)(2,1)}, bf16[512,1280]{1,0:T(8,128)(2,1)}, bf16[1280,512]{1,0:T(8,128)(2,1)}, bf16[384,512]{1,0:T(8,128)(2,1)}, f32[1,512...) custom-call(bf16[384,512]{1,0:T(8,128)(2,1)} %refs_0_.1, bf16[384,512]{1,0:T(8,128)(2,1)} %refs_1_.1, ...), custom_call_target="tpu_custom_call" | custom-call | tf_op jit(solution)/shard_map/layer/pallas_call | solution.py:1396
  194.8 0.0 copy-start.1
  194.8 3.1 %convert_element_type.10 = f32[512,1280]{1,0:T(8,128)} convert(bf16[512,1280]{1,0:T(8,128)(2,1)} %get-tuple-element.17) | non-fusion elementwise | flops 655360 | bytes 3932160 | tf_op jit(solution)/shard_map/convert_element_type | solution.py:1507
  197.9 0.0 copy-done.1
  197.9 0.0 copy-start
  197.9 1.9 convert_element_type.11
  199.8 0.0 copy-done
  199.8 0.0 copy-start.3
  199.8 0.0 copy-start.2
  199.8 0.0 copy-start.5
  199.8 0.0 copy-start.4
  199.8 1.7 convert_element_type.9
  201.5 0.0 copy-done.3
  201.5 0.6 reduce
  202.1 0.0 copy-done.2
  202.1 0.7 copy.16
  202.9 0.0 copy-done.5
  202.9 0.6 copy.17
  203.4 0.0 copy-done.4
  203.4 0.6 copy.18
Async XLA Ops:
  194.8 3.1 %copy-start.1 = (bf16[1280,512]{1,0:T(8,128)(2,1)S(1)}, bf16[1280,512]{1,0:T(8,128)(2,1)}, u32[]{:S(2)}) copy-start(bf16[1280,512]{1,0:T(8,128)(2,1)} %get-tuple-element.18) | copy-start | bytes 3932164
  197.9 1.9 copy-start
  199.8 1.7 copy-start.3
  199.8 2.3 %copy-start.2 = (bf16[384,512]{1,0:T(8,128)(2,1)S(1)}, bf16[384,512]{1,0:T(8,128)(2,1)}, u32[]{:S(2)}) copy-start(bf16[384,512]{1,0:T(8,128)(2,1)} %get-tuple-element.28) | copy-start | bytes 1179652
  199.8 3.1 %copy-start.5 = (f32[1,512]{1,0:T(1,128)S(1)}, f32[1,512]{1,0:T(1,128)}, u32[]{:S(2)}) copy-start(f32[1,512]{1,0:T(1,128)} %get-tuple-element.15) | copy-start | bytes 6148
  199.8 3.6 %copy-start.4 = (f32[2,512]{1,0:T(2,128)S(1)}, f32[2,512]{1,0:T(2,128)}, u32[]{:S(2)}) copy-start(f32[2,512]{1,0:T(2,128)} %get-tuple-element.33) | copy-start | bytes 12292

commit v4 on v3

--- a/solution.py
+++ b/solution.py
@@ -485,6 +485,7 @@
 CORES = 2
 LANES = 128
 TILE = 256
+PARTS = 2
 
 
 def line_next(z, n_fs, side):
@@ -492,7 +493,7 @@
 
 
 def layer_kernel(n_fs, n_tp, *refs):
-    tokens, cot, w_gate, w_up, w_down, gain = refs[:6]
+    tokens, cot, w_gate, w_up, w_down, gain_in = refs[:6]
     o_gate, o_up, o_down, o_tokens, o_gain, o_wide_sq, o_tall_sq = refs[6:13]
     full = refs[13:18]
     x_full, dy_full, f_gate, f_up, f_down = full
@@ -507,7 +508,8 @@
     (p_send, p_recv, x_send, x_recv, z_send, z_recv, f_send, f_recv) = refs[71:79]
     (y_send, y_recv, d_send, d_recv, n_send, n_recv, own_sem) = refs[79:86]
     (row_send, row_recv, gain_send, gain_recv) = refs[86:90]
-    (wide_send, wide_recv, tall_send, tall_recv, out_sem, total, gain_sum) = refs[90:]
+    (wide_send, wide_recv, tall_send, tall_recv, out_sem, total, gain_sum) = refs[90:97]
+    gain_load, gain, v_wide, v_tall, v_half = refs[97:]
     r, z, t = lax.axis_index("rep"), lax.axis_index("fs"), lax.axis_index("tp")
     y, c = lax.div(t, CORES), lax.rem(t, CORES)
     acts, weights = (tokens, cot), (w_gate, w_up, w_down)
@@ -541,60 +543,83 @@
             pl.ds(pl.multiple_of(column * local, local), local),
         ]
 
+    sub = half // PARTS
+
+    def own_part(a, h, q):
+        start = h * half + q * sub
+        return acts[a].at[pl.ds(start, sub), :]
+
+    def act_part(a, source, column, q):
+        return full[a].at[
+            pl.ds(pl.multiple_of(source * half + q * sub, sub), sub),
+            pl.ds(pl.multiple_of(column * local, local), local),
+        ]
+
     def source_of(side, d):
         return z - d if side == 0 else z + d
 
     def next_of(side):
         return z + 1 if side == 0 else z - 1
 
-    def act_first(a, side, h):
+    def line_turn(source, at):
+        return lax.rem(source - at + n_fs, n_fs) - 1
+
+    def act_first(a, side, h, q):
+        return remote(
+            own_part(a, h, q),
+            act_part(a, z, t, q),
+            az_own.at[a, side],
+            az_recv.at[a, line_turn(z, next_of(side)), c, q],
+            {"fs": next_of(side), "tp": y * CORES + h},
+        )
+
+    def act_arrival(a, side, d, core, q):
+        place = act_part(a, source_of(side, d), y * CORES + core, q)
+        return remote(
+            place,
+            place,
+            az_fwd.at[a],
+            az_recv.at[a, line_turn(source_of(side, d), z), core, q],
+            partner,
+        )
+
+    def act_forward(a, side, d, core, q):
+        place = act_part(a, source_of(side, d), y * CORES + core, q)
+        return remote(
+            place,
+            place,
+            az_fwd.at[a],
+            az_recv.at[a, line_turn(source_of(side, d), next_of(side)), core, q],
+            {"fs": next_of(side)},
+        )
+
+    def act_over(a, side, d, core, q):
+        source = source_of(side, d)
+        place = act_part(a, source, y * CORES + core, q)
+        return remote(
+            place,
+            place,
+            ay_fwd.at[a],
+            ay_recv.at[a, source, core, q],
+            {"tp": (1 - y) * CORES + c},
+        )
+
+    def act_over_arrival(a, source, core, q):
+        place = act_part(a, source, (1 - y) * CORES + core, q)
+        return remote(place, place, ay_own.at[a], ay_recv.at[a, source, core, q], partner)
+
+    def act_over_own(a, h):
         return remote(
             own_act(a, h),
             act_place(a, z, t),
-            az_own.at[a, side, h],
-            az_recv.at[a, side, 0, c],
-            {"fs": next_of(side), "tp": y * CORES + h},
-        )
-
-    def act_arrival(a, side, d, core):
-        place = act_place(a, source_of(side, d), y * CORES + core)
-        return remote(
-            place, place, az_fwd.at[a, side, d - 1, core], az_recv.at[a, side, d - 1, core], partner
-        )
-
-    def act_forward(a, side, d, core):
-        place = act_place(a, source_of(side, d), y * CORES + core)
-        return remote(
-            place,
-            place,
-            az_fwd.at[a, side, d - 1, core],
-            az_recv.at[a, side, d, core],
-            {"fs": next_of(side)},
-        )
-
-    def act_over(a, side, d, core):
-        source = source_of(side, d)
-        place = act_place(a, source, y * CORES + core)
-        return remote(
-            place,
-            place,
-            ay_fwd.at[a, side, d - 1, core],
-            ay_recv.at[a, source, core],
-            {"tp": (1 - y) * CORES + c},
-        )
-
-    def act_over_own(a, h):
-        return remote(
-            own_act(a, h),
-            act_place(a, z, t),
-            ay_own.at[a, h],
-            ay_recv.at[a, z, c],
+            ay_own.at[a],
+            ay_recv.at[a, z, c, 0],
             {"tp": (1 - y) * CORES + h},
         )
 
-    def act_over_arrival(a, source, core):
-        place = act_place(a, source, (1 - y) * CORES + core)
-        return remote(place, place, ay_own.at[a, 0], ay_recv.at[a, source, core], partner)
+    def act_over_own_arrival(a, core):
+        place = act_place(a, z, (1 - y) * CORES + core)
+        return remote(place, place, ay_own.at[a], ay_recv.at[a, z, core, 0], partner)
 
     def act_partner(a):
         return remote(own_act(a, 1 - c), act_place(a, z, t), ap_send.at[a], ap_recv.at[a], partner)
@@ -638,33 +663,33 @@
         return remote(
             own_quarter(m, k, core),
             quarter(m, z, r, core),
-            w_send.at[m, k, core],
+            w_send.at[m, k],
             w_recv.at[m, z],
             {"fs": kb * c + k, "tp": y * CORES + core},
         )
 
     def weight_arrival(m, source):
         place = quarter(m, source, r, c)
-        return remote(place, place, wx_send.at[m, source], w_recv.at[m, source], partner)
+        return remote(place, place, wx_send.at[m], w_recv.at[m, source], partner)
 
     def weight_across(m, source):
         place = quarter(m, source, r, c)
-        return remote(place, place, wx_send.at[m, source], wx_recv.at[m, source], across)
+        return remote(place, place, wx_send.at[m], wx_recv.at[m, source], across)
 
     def weight_across_arrival(m, source):
         place = quarter(m, source, 1 - r, c)
-        return remote(place, place, wx_send.at[m, source], wx_recv.at[m, source], across)
+        return remote(place, place, wx_send.at[m], wx_recv.at[m, source], across)
 
     def weight_beside(m, source, which):
         place = quarter(m, source, r if which == 0 else 1 - r, c)
         return remote(
-            place, place, wp_send.at[m, source, which], wp_recv.at[m, source, which], partner
+            place, place, wp_send.at[m], wp_recv.at[m, source, which], partner
         )
 
     def weight_beside_arrival(m, source, which):
         place = quarter(m, source, r if which == 0 else 1 - r, 1 - c)
         return remote(
-            place, place, wp_send.at[m, source, which], wp_recv.at[m, source, which], partner
+            place, place, wp_send.at[m], wp_recv.at[m, source, which], partner
         )
 
     def own_beside(m):
@@ -693,7 +718,7 @@
         return remote(
             grad_piece(m, kb * (1 - c) + k, rep_of(j)),
             slot(pair_wide, pair_tall, m, k, j),
-            p_send.at[m, k, j],
+            p_send.at[m],
             p_recv.at[m, k, j],
             partner,
         )
@@ -702,7 +727,7 @@
         return remote(
             slot(sum_wide, sum_tall, m, k),
             slot(x_wide, x_tall, m, k),
-            x_send.at[m, k],
+            x_send.at[m],
             x_recv.at[m, k],
             across,
         )
@@ -729,11 +754,11 @@
         return pltpu.make_async_copy(slot(t_wide, t_tall, m, k), place(m, k, r), own_sem.at[m, k])
 
     def spread(m, k, source):
-        return remote(source, place(m, k, r), f_send.at[m, k], f_recv.at[m, k], across)
+        return remote(source, place(m, k, r), f_send.at[m], f_recv.at[m, k], across)
 
     def spread_arrival(m, k):
         return remote(
-            place(m, k, 1 - r), place(m, k, 1 - r), f_send.at[m, k], f_recv.at[m, k], across
+            place(m, k, 1 - r), place(m, k, 1 - r), f_send.at[m], f_recv.at[m, k], across
         )
 
     def band_rows(band):
@@ -746,7 +771,7 @@
         return remote(
             x_full.at[band_rows(band), side_columns(1 - y)],
             y_buf.at[band],
-            y_send.at[band],
+            y_send.at[0],
             y_recv.at[band],
             beside,
         )
@@ -806,7 +831,8 @@
 
                 @pl.when(line_next(z, n_fs, side))
                 def _():
-                    act_first(a, side, h).start()
+                    for q in range(PARTS):
+                        act_first(a, side, h, q).start()
 
             act_over_own(a, h).start()
         act_partner(a).start()
@@ -818,18 +844,19 @@
 
     def act_round(a, d):
         for core in range(CORES):
-            for side in range(2):
-
-                @pl.when(line_receives(z, n_fs, side, d))
-                def _():
-                    act_arrival(a, side, d, core).wait_recv()
-                    if d < n_fs - 1:
-
-                        @pl.when(line_next(z, n_fs, side))
-                        def _():
-                            act_forward(a, side, d, core).start()
-
-                    act_over(a, side, d, core).start()
+            for q in range(PARTS):
+                for side in range(2):
+
+                    @pl.when(line_receives(z, n_fs, side, d))
+                    def _():
+                        act_arrival(a, side, d, core, q).wait_recv()
+                        if d < n_fs - 1:
+
+                            @pl.when(line_next(z, n_fs, side))
+                            def _():
+                                act_forward(a, side, d, core, q).start()
+
+                        act_over(a, side, d, core, q).start()
 
     def weight_start(m):
         for k in range(kb):
@@ -875,35 +902,34 @@
                 @pl.when(line_receives(z, n_fs, side, d))
                 def _():
                     for core in range(CORES):
-                        act_over_arrival(a, source_of(side, d), core).wait_recv()
+                        for q in range(PARTS):
+                            act_over_arrival(a, source_of(side, d), core, q).wait_recv()
 
         act_partner_arrival(a).wait_recv()
         for h in range(CORES):
-            act_over_arrival(a, z, h).wait_recv()
+            act_over_own_arrival(a, h).wait_recv()
         loaded(a).wait()
 
-    def act_sent(a):
-        for d in range(1, n_fs):
-            for side in range(2):
-
-                @pl.when(line_receives(z, n_fs, side, d))
-                def _():
-                    for core in range(CORES):
-                        act_over(a, side, d, core).wait_send()
-                        if d < n_fs - 1:
-
-                            @pl.when(line_next(z, n_fs, side))
-                            def _():
-                                act_forward(a, side, d, core).wait_send()
-
-        act_partner(a).wait_send()
-        for h in range(CORES):
-            act_over_own(a, h).wait_send()
+    def sent(ref, sem):
+        remote(ref, ref, sem, sem, partner).wait_send()
+
+    def act_sent(a, landed):
+        others = full[a].at[pl.ds(0, count - half), pl.ds(0, CORES * local)]
+        if landed:
+            sent(others, ay_fwd.at[a])
+
+            @pl.when(inner)
+            def _():
+                sent(others, az_fwd.at[a])
+
+        if a == 1 or not landed:
+            act_partner(a).wait_send()
+            sent(acts[a], ay_own.at[a])
             for side in range(2):
 
                 @pl.when(line_next(z, n_fs, side))
                 def _():
-                    act_first(a, side, h).wait_send()
+                    sent(acts[a], az_own.at[a, side])
 
     def weight_ready(ms):
         for m in ms:
@@ -924,26 +950,38 @@
                 own_beside_arrival(m).wait_recv()
 
     def weight_sent(m):
-        for d in range(1, n_fs):
-            for side in range(2):
-
-                @pl.when(line_receives(z, n_fs, side, d))
-                def _():
-                    source = source_of(side, d)
-                    weight_across(m, source).wait_send()
-                    for which in range(2):
-                        weight_beside(m, source, which).wait_send()
-
+        size = full[2 + m].shape[0 if m < 2 else 1] - rows
+        part = (rows if m < 2 else width) // (2 * CORES)
+        if m < 2:
+            sent(full[2 + m].at[pl.ds(0, (n_fs - 1) * part), :], wx_send.at[m])
+            sent(full[2 + m].at[pl.ds(0, 2 * (n_fs - 1) * part), :], wp_send.at[m])
+            half_block = weights[m].at[pl.ds(0, CORES * part), pl.ds(0, width)]
+        else:
+            sent(full[4].at[pl.ds(0, part), pl.ds(0, size)], wx_send.at[m])
+            sent(full[4].at[pl.ds(0, 2 * part), pl.ds(0, size)], wp_send.at[m])
+            half_block = weights[m].at[pl.ds(0, CORES * part), :]
         for k in range(kb):
 
             @pl.when(kb * c + k != z)
             def _():
-                for core in range(CORES):
-                    weight_send(m, k, core).wait_send()
+                sent(half_block, w_send.at[m, k])
 
         @pl.when(c == owner)
         def _():
             own_beside(m).wait_send()
+
+    def pairs_sent(m):
+        span = pl.ds(0, kb * rows)
+        sent(g_down.at[:, span] if m == 2 else grads[m].at[span, :], p_send.at[m])
+
+    def swaps_sent(m):
+        sent(sum_tall if m == 2 else sum_wide.at[m], x_send.at[m])
+
+    def spreads_sent(m):
+        sent(sum_tall if m == 2 else sum_wide.at[m], f_send.at[m])
+
+    def over_sent():
+        sent(x_full.at[:, side_columns(1 - y)], y_send.at[0])
 
     def tile(i, size):
         return pl.ds(pl.multiple_of(i * size, size), size)
@@ -952,7 +990,7 @@
         at = tile(i, LANES)
         wide = x_full[at, :].astype(jnp.float32)
         inv = lax.rsqrt(jnp.mean(wide * wide, axis=-1, keepdims=True) + 1e-06)
-        value = wide * inv * gain[...].astype(jnp.float32)
+        value = wide * inv * gain[...]
         normed[at, :] = value.astype(jnp.bfloat16)
         normed_t[:, at] = value.T.astype(jnp.bfloat16)
         inv_all[at, :] = jnp.broadcast_to(inv, (LANES, LANES))
@@ -1129,9 +1167,7 @@
     row_fan = fan(row_all, n_tp, t, row_send, row_recv, lane_peer)
     wide_fan = fan(wide_all, n_tp, t, wide_send, wide_recv, lane_peer)
     gain_fan = fan(gain_all, 2 * n_fs, r * n_fs + z, gain_send, gain_recv, group_peer)
-    tall_fan = fan(
-        tall_all, n_fs, z, tall_send, tall_recv, lambda j: {"fs": lax.rem(z + j, n_fs)}
-    )
+    tall_fan = fan(tall_all, 2 * n_fs, r * n_fs + z, tall_send, tall_recv, group_peer)
 
     def fan_start(pair_of, count_of):
         for j in range(1, count_of):
@@ -1146,7 +1182,7 @@
             pair_of[0](j).wait_send()
 
     def gain_here():
-        return gain[:, pl.ds(pl.multiple_of(t * local, local), local)].astype(jnp.float32)
+        return gain[:, pl.ds(pl.multiple_of(t * local, local), local)]
 
     def token_sums():
         last_arrival().wait_recv()
@@ -1200,28 +1236,26 @@
             outs[m].at[:, at], (o_gate, o_up)[m].at[:, at], out_sem.at[m, k]
         )
 
-    def squares(m, k):
-        spread_arrival(m, k).wait_recv()
-        mine = kb * c + k == z
-
-        @pl.when(mine)
+    def strip_squares(m, k):
+        @pl.when(kb * c + k == z)
         def _():
             keep(m, k).wait()
 
-        block_out(m, k).start()
         if m == 2:
+            columns = pl.ds(pl.multiple_of(r * strip, strip), strip)
 
             @pl.loop(0, width // LANES)
             def _(i):
                 at = pl.ds(pl.multiple_of(k * width + i * LANES, LANES), LANES)
-                value = v_down[at, :].astype(jnp.float32)
-                tall_all[z, :, at] = row_of(fold(value * value))
+                value = v_down[at, columns].astype(jnp.float32)
+                tall_all[r * n_fs + z, :, at] = row_of(fold(value * value))
         else:
 
-            @pl.loop(0, rows // LANES)
+            @pl.loop(0, strip // LANES)
             def _(i):
                 at = tile(i, LANES)
-                value = outs[m][at, k * width : (k + 1) * width].astype(jnp.float32)
+                from_row = pl.ds(pl.multiple_of(r * strip + i * LANES, LANES), LANES)
+                value = outs[m][from_row, k * width : (k + 1) * width].astype(jnp.float32)
                 part = fold(value * value)
                 if k > 0:
                     part = part + lane_sq[m, at, :]
@@ -1230,6 +1264,26 @@
                 else:
                     wide_all[t, m : m + 1, at] = row_of(part)
 
+    def wide_cross():
+        strips = pl.ds(pl.multiple_of(r * strip, strip), strip)
+        return remote(v_half, v_wide.at[:, strips], n_send.at[2], n_recv.at[2], across)
+
+    def wide_cross_arrival():
+        place = v_wide.at[:, pl.ds(pl.multiple_of((1 - r) * strip, strip), strip)]
+        return remote(place, place, n_send.at[2], n_recv.at[2], across)
+
+    def summed(buffer, count_of):
+        value = buffer[0]
+        for j in range(1, count_of):
+            value = value + buffer[j]
+        return value
+
+    def whole_block(m, k):
+        spread_arrival(m, k).wait_recv()
+        block_out(m, k).start()
+
+    gain_copy = pltpu.make_async_copy(gain_in, gain_load, out_sem.at[3, 1])
+    gain_copy.start()
     for a in range(2):
         loaded(a).start()
 
@@ -1255,6 +1309,9 @@
     act_round(1, 1)
     weight_all(1)
     across_all(0)
+    gain_copy.wait()
+    for i in range(model // LANES):
+        gain[:, i * LANES : (i + 1) * LANES] = gain_load[i : i + 1, :].astype(jnp.float32)
     act_ready(0)
     pl.loop(0, count // LANES)(normalize)
     inv_send().start()
@@ -1275,7 +1332,7 @@
     gradients(2, 1)
     weight_ready((2,))
     pl.loop(0, count // TILE)(backward)
-    act_sent(0)
+    act_sent(0, True)
 
     @pl.loop(0, n_fs)
     def _(i):
@@ -1312,60 +1369,70 @@
     third(0, 0)
     third(0, 1)
     normed_inner(1)
+    for k in range(kb):
+        strip_squares(2, k)
+    fan_start(tall_fan, 2 * n_fs)
+    for k in range(kb):
+        strip_squares(0, k)
     third(1, 0)
+    strip_squares(1, 0)
     third(1, 1)
+    strip_squares(1, 1)
+    fan_start(wide_fan, n_tp)
     normed_last()
-    squares(2, 0)
-    squares(2, 1)
-    fan_start(tall_fan, n_fs)
+    whole_block(2, 0)
+    whole_block(2, 1)
     token_sums()
-    squares(0, 0)
-    squares(0, 1)
+    fan_ready(wide_fan, n_tp)
+    v_half[...] = summed(wide_all, n_tp)
+    wide_cross().start()
+    v_wide[:, pl.ds(pl.multiple_of(r * strip, strip), strip)] = v_half[...]
+    fan_ready(tall_fan, 2 * n_fs)
+    v_tall[...] = summed(tall_all, 2 * n_fs)
+    tall_out = pltpu.make_async_copy(v_tall, o_tall_sq, out_sem.at[4, 1])
+    tall_out.start()
     token_grads()
-    squares(1, 0)
-    squares(1, 1)
-    fan_start(wide_fan, n_tp)
-    fan_ready(gain_fan, 2 * n_fs)
-    gain_total = gain_all[0]
-    for j in range(1, 2 * n_fs):
-        gain_total = gain_total + gain_all[j]
-    o_gain[...] = gain_total
-    fan_ready(tall_fan, n_fs)
-    tall_total = tall_all[0]
-    for j in range(1, n_fs):
-        tall_total = tall_total + tall_all[j]
-    o_tall_sq[...] = tall_total
-
+    whole_block(0, 0)
+    whole_block(0, 1)
+    act_sent(0, False)
+    act_sent(1, True)
     for m in range(3):
+        weight_sent(m)
+    over_sent()
+    normed_sent()
+    inv_send().wait_send()
+    last_send().wait_send()
+    fan_sent(row_fan, n_tp)
+    fan_sent(wide_fan, n_tp)
+    for m in range(3):
+        pairs_sent(m)
+        swaps_sent(m)
         for k in range(kb):
-            for j in range(2):
-                pair(m, k, j).wait_send()
-            swap(m, k).wait_send()
 
             @pl.when(kb * c + k != z)
             def _():
                 deliver(m, k).wait_send()
 
-            spread(m, k, place(m, k, r)).wait_send()
+    whole_block(1, 0)
+    fan_ready(gain_fan, 2 * n_fs)
+    gain_sum[...] = summed(gain_all, 2 * n_fs)
+    gain_out = pltpu.make_async_copy(gain_sum, o_gain, out_sem.at[4, 0])
+    gain_out.start()
+    wide_cross_arrival().wait_recv()
+    wide_out = pltpu.make_async_copy(v_wide, o_wide_sq, out_sem.at[4, 2])
+    wide_out.start()
+    whole_block(1, 1)
+    wide_cross().wait_send()
+    fan_sent(gain_fan, 2 * n_fs)
+    fan_sent(tall_fan, 2 * n_fs)
+    gain_out.wait()
+    tall_out.wait()
+    wide_out.wait()
+    pltpu.make_async_copy(v_out, o_tokens, out_sem.at[3, 0]).wait()
+    for m in range(3):
+        spreads_sent(m)
+        for k in range(kb):
             block_out(m, k).wait()
-    pltpu.make_async_copy(v_out, o_tokens, out_sem.at[3, 0]).wait()
-    for b in range(n_fs):
-        over(b).wait_send()
-    normed_sent()
-    inv_send().wait_send()
-    last_send().wait_send()
-    act_sent(1)
-    for m in range(3):
-        weight_sent(m)
-    fan_sent(row_fan, n_tp)
-    fan_sent(gain_fan, 2 * n_fs)
-    fan_sent(tall_fan, n_fs)
-    fan_ready(wide_fan, n_tp)
-    wide_total = wide_all[0]
-    for j in range(1, n_tp):
-        wide_total = wide_total + wide_all[j]
-    o_wide_sq[...] = wide_total
-    fan_sent(wide_fan, n_tp)
 
 
 def layer(n_fs, n_tp, tokens, cot, w_gate, w_up, w_down, gain):
@@ -1380,9 +1447,7 @@
     reach = model // 2
     wide, tall = (strip, width), (width, strip)
     dma = pltpu.SemaphoreType.DMA
-    vmem = pl.BlockSpec(memory_space=pltpu.VMEM)
     hbm = pl.BlockSpec(memory_space=pl.ANY)
-    line = dma((2, 2, n_fs - 1, CORES))
     pairs, singles = dma((3, kb, 2)), dma((3, kb))
 
     def bf(*shape):
@@ -1398,8 +1463,8 @@
         out_shape=[jax.ShapeDtypeStruct(s, dtype) for s in shapes]
         + [jax.ShapeDtypeStruct((CORES * half, local), dtype)]
         + [jax.ShapeDtypeStruct(s, jnp.float32) for s in ((1, local), (2, rows), (1, hidden))],
-        in_specs=[hbm] * 5 + [vmem],
-        out_specs=[hbm] * 4 + [vmem] * 3,
+        in_specs=[hbm] * 6,
+        out_specs=[hbm] * 7,
         scratch_shapes=[
             bf(count, model),
             bf(count, model),
@@ -1437,42 +1502,42 @@
             bf(CORES * half, local),
             f32(CORES * half, LANES),
             bf(CORES * half, local),
-            f32(2, rows, LANES),
+            f32(2, strip, LANES),
             f32(n_tp, 1, CORES * half),
             f32(2 * n_fs, 1, local),
-            f32(n_tp, 2, rows),
-            f32(n_fs, 1, hidden),
+            f32(n_tp, 2, strip),
+            f32(2 * n_fs, 1, hidden),
             dma((7,)),
-            dma((2, 2, CORES)),
-            line,
-            line,
-            dma((2, CORES)),
-            line,
-            dma((2, n_fs, CORES)),
+            dma((2, 2)),
+            dma((2,)),
+            dma((2, n_fs - 1, CORES, PARTS)),
             dma((2,)),
             dma((2,)),
-            dma((3, kb, CORES)),
+            dma((2, n_fs, CORES, PARTS)),
+            dma((2,)),
+            dma((2,)),
+            dma((3, kb)),
             dma((3, n_fs)),
+            dma((3,)),
             dma((3, n_fs)),
-            dma((3, n_fs)),
-            dma((3, n_fs, 2)),
+            dma((3,)),
             dma((3, n_fs, 2)),
             dma((3,)),
             dma((3,)),
+            dma((3,)),
             pairs,
-            pairs,
+            dma((3,)),
             singles,
             singles,
             singles,
+            dma((3,)),
             singles,
-            singles,
-            singles,
-            dma((n_fs,)),
+            dma((1,)),
             dma((n_fs,)),
             dma((n_fs,)),
             dma((2, n_fs)),
-            dma((2,)),
-            dma((2,)),
+            dma((3,)),
+            dma((3,)),
             dma((3, kb)),
             dma((n_tp - 1,)),
             dma((n_tp - 1,)),
@@ -1480,11 +1545,16 @@
             dma((2 * n_fs - 1,)),
             dma((n_tp - 1,)),
             dma((n_tp - 1,)),
-            dma((n_fs - 1,)),
-            dma((n_fs - 1,)),
-            dma((4, kb)),
+            dma((2 * n_fs - 1,)),
+            dma((2 * n_fs - 1,)),
+            dma((5, max(kb, 3))),
             f32(half, reach),
             f32(1, local),
+            bf(model // LANES, LANES),
+            f32(1, model),
+            f32(2, rows),
+            f32(1, hidden),
+            f32(2, strip),
         ],
         compiler_params=pltpu.CompilerParams(
             collective_id=4, has_side_effects=True, vmem_limit_bytes=67043328
@@ -1502,7 +1572,7 @@
         w_gate,
         w_up,
         w_down,
-        norm_gain[None, :],
+        norm_gain.reshape(-1, LANES),
     )
     grad_gate, grad_up, grad_down = (s.astype(jnp.float32) for s in (s_gate, s_up, s_down))
     return (grad_tokens, grad_gain[0], grad_gate, grad_up, grad_down, gate_up_sq, down_sq[0])

time: 204 us -> 199 us (0.975)
  Pallas kernels: 193 us -> 189 us
    pallas_call x1, Pallas kernels: 193 us -> 189 us  [layer(): pl.pallas_call(functools.partial(layer_kernel, n_fs, n_tp), out_shape=[ja...]
where the time goes in v4:
time: 199 us
  Pallas kernels  189 us (95%)
  other arithmetic  7.24 us (4%)
    pallas_call x1, Pallas kernels, layer(): pl.pallas_call(functools.partial(layer_kernel, n_fs, n_tp), out_shape=[ja...  189 us
    convert_element_type x3, other arithmetic, by_chip(): s.astype(jnp.float32)  6.62 us

profile of v4, /device:TPU:0, one launch (start us, length us, event | category | flops | bytes accessed | tf_op | source)
XLA Modules:
  0.0 198.7 jit_solution(11937155998720184663)
XLA Ops:
  0.6 188.8 %layer.1 = (bf16[512,1280]{1,0:T(8,128)(2,1)}, bf16[512,1280]{1,0:T(8,128)(2,1)}, bf16[1280,512]{1,0:T(8,128)(2,1)}, bf16[384,512]{1,0:T(8,128)(2,1)}, f32[1,512...) custom-call(bf16[384,512]{1,0:T(8,128)(2,1)} %refs_0_.1, bf16[384,512]{1,0:T(8,128)(2,1)} %refs_1_.1, ...), custom_call_target="tpu_custom_call" | custom-call | tf_op jit(solution)/shard_map/layer/pallas_call | solution.py:1461
  189.5 0.0 copy-start.1
  189.5 3.1 %convert_element_type.10 = f32[512,1280]{1,0:T(8,128)} convert(bf16[512,1280]{1,0:T(8,128)(2,1)} %get-tuple-element.17) | non-fusion elementwise | flops 655360 | bytes 3932160 | tf_op jit(solution)/shard_map/convert_element_type | solution.py:1577
  192.6 0.0 copy-done.1
  192.6 0.0 copy-start
  192.6 1.9 convert_element_type.11
  194.4 0.0 copy-done
  194.4 0.0 copy-start.3
  194.4 0.0 copy-start.2
  194.4 0.0 copy-start.5
  194.4 0.0 copy-start.4
  194.4 1.7 convert_element_type.9
  196.1 0.0 copy-done.3
  196.1 0.6 reduce
  196.7 0.0 copy-done.2
  196.7 0.7 copy.16
  197.5 0.0 copy-done.5
  197.5 0.6 copy.17
  198.1 0.0 copy-done.4
  198.1 0.6 copy.18
Async XLA Ops:
  189.5 3.1 %copy-start.1 = (bf16[1280,512]{1,0:T(8,128)(2,1)S(1)}, bf16[1280,512]{1,0:T(8,128)(2,1)}, u32[]{:S(2)}) copy-start(bf16[1280,512]{1,0:T(8,128)(2,1)} %get-tuple-element.18) | copy-start | bytes 3932164
  192.6 1.9 copy-start
  194.4 1.7 copy-start.3
  194.4 2.3 %copy-start.2 = (bf16[384,512]{1,0:T(8,128)(2,1)S(1)}, bf16[384,512]{1,0:T(8,128)(2,1)}, u32[]{:S(2)}) copy-start(bf16[384,512]{1,0:T(8,128)(2,1)} %get-tuple-element.28) | copy-start | bytes 1179652
  194.4 3.1 %copy-start.5 = (f32[1,512]{1,0:T(1,128)S(1)}, f32[1,512]{1,0:T(1,128)}, u32[]{:S(2)}) copy-start(f32[1,512]{1,0:T(1,128)} %get-tuple-element.15) | copy-start | bytes 6148
  194.4 3.6 %copy-start.4 = (f32[2,512]{1,0:T(2,128)S(1)}, f32[2,512]{1,0:T(2,128)}, u32[]{:S(2)}) copy-start(f32[2,512]{1,0:T(2,128)} %get-tuple-element.33) | copy-start | bytes 12292

commit v5 on v4

--- a/solution.py
+++ b/solution.py
@@ -486,6 +486,7 @@
 LANES = 128
 TILE = 256
 PARTS = 2
+STEPS = 2
 
 
 def line_next(z, n_fs, side):
@@ -600,26 +601,22 @@
             place,
             place,
             ay_fwd.at[a],
-            ay_recv.at[a, source, core, q],
+            ay_recv.at[a],
             {"tp": (1 - y) * CORES + c},
         )
-
-    def act_over_arrival(a, source, core, q):
-        place = act_part(a, source, (1 - y) * CORES + core, q)
-        return remote(place, place, ay_own.at[a], ay_recv.at[a, source, core, q], partner)
 
     def act_over_own(a, h):
         return remote(
             own_act(a, h),
             act_place(a, z, t),
             ay_own.at[a],
-            ay_recv.at[a, z, c, 0],
+            ay_recv.at[a],
             {"tp": (1 - y) * CORES + h},
         )
 
-    def act_over_own_arrival(a, core):
-        place = act_place(a, z, (1 - y) * CORES + core)
-        return remote(place, place, ay_own.at[a], ay_recv.at[a, z, core, 0], partner)
+    def act_over_arrivals(a):
+        place = full[a].at[:, side_columns(1 - y)]
+        return remote(place, place, ay_own.at[a], ay_recv.at[a], partner)
 
     def act_partner(a):
         return remote(own_act(a, 1 - c), act_place(a, z, t), ap_send.at[a], ap_recv.at[a], partner)
@@ -683,14 +680,16 @@
     def weight_beside(m, source, which):
         place = quarter(m, source, r if which == 0 else 1 - r, c)
         return remote(
-            place, place, wp_send.at[m], wp_recv.at[m, source, which], partner
-        )
-
-    def weight_beside_arrival(m, source, which):
-        place = quarter(m, source, r if which == 0 else 1 - r, 1 - c)
-        return remote(
-            place, place, wp_send.at[m], wp_recv.at[m, source, which], partner
-        )
+            place, place, wp_send.at[m], wp_recv.at[m], partner
+        )
+
+    def weight_beside_arrivals(m):
+        part = (width if m == 2 else rows) // (2 * CORES)
+        if m == 2:
+            place = full[4].at[pl.ds(0, 2 * part), pl.ds(0, model - rows)]
+        else:
+            place = full[2 + m].at[pl.ds(0, 2 * (n_fs - 1) * part), :]
+        return remote(place, place, wp_send.at[m], wp_recv.at[m], partner)
 
     def own_beside(m):
         return remote(
@@ -896,18 +895,8 @@
             across_round((m,), d)
 
     def act_ready(a):
-        for d in range(1, n_fs):
-            for side in range(2):
-
-                @pl.when(line_receives(z, n_fs, side, d))
-                def _():
-                    for core in range(CORES):
-                        for q in range(PARTS):
-                            act_over_arrival(a, source_of(side, d), core, q).wait_recv()
-
+        act_over_arrivals(a).wait_recv()
         act_partner_arrival(a).wait_recv()
-        for h in range(CORES):
-            act_over_own_arrival(a, h).wait_recv()
         loaded(a).wait()
 
     def sent(ref, sem):
@@ -933,13 +922,7 @@
 
     def weight_ready(ms):
         for m in ms:
-            for d in range(1, n_fs):
-                for side in range(2):
-
-                    @pl.when(line_receives(z, n_fs, side, d))
-                    def _():
-                        for which in range(2):
-                            weight_beside_arrival(m, source_of(side, d), which).wait_recv()
+            weight_beside_arrivals(m).wait_recv()
 
             @pl.when(c == owner)
             def _():
@@ -1153,33 +1136,21 @@
         return {"rep": lax.div(at, n_fs), "fs": lax.rem(at, n_fs)}
 
     def fan(buffer, count_of, mine, send, recv, peer):
-        def sent(j):
-            return remote(
-                buffer.at[mine], buffer.at[mine], send.at[j - 1], recv.at[count_of - j - 1], peer(j)
-            )
-
-        def received(j):
-            place = buffer.at[lax.rem(mine + j, count_of)]
-            return remote(place, place, send.at[j - 1], recv.at[j - 1], peer(j))
-
-        return sent, received
+        def start():
+            for j in range(1, count_of):
+                place = buffer.at[mine]
+                remote(place, place, send.at[0], recv.at[0], peer(j)).start()
+
+        def others():
+            place = buffer.at[pl.ds(0, count_of - 1)]
+            return remote(place, place, send.at[0], recv.at[0], partner)
+
+        return start, others
 
     row_fan = fan(row_all, n_tp, t, row_send, row_recv, lane_peer)
     wide_fan = fan(wide_all, n_tp, t, wide_send, wide_recv, lane_peer)
     gain_fan = fan(gain_all, 2 * n_fs, r * n_fs + z, gain_send, gain_recv, group_peer)
     tall_fan = fan(tall_all, 2 * n_fs, r * n_fs + z, tall_send, tall_recv, group_peer)
-
-    def fan_start(pair_of, count_of):
-        for j in range(1, count_of):
-            pair_of[0](j).start()
-
-    def fan_ready(pair_of, count_of):
-        for j in range(1, count_of):
-            pair_of[1](j).wait_recv()
-
-    def fan_sent(pair_of, count_of):
-        for j in range(1, count_of):
-            pair_of[0](j).wait_send()
 
     def gain_here():
         return gain[:, pl.ds(pl.multiple_of(t * local, local), local)]
@@ -1201,11 +1172,11 @@
             gain_sum[...] += jnp.sum(d_tokens * inv, axis=0, keepdims=True)
 
         gain_all[r * n_fs + z] = gain_sum[...]
-        fan_start(row_fan, n_tp)
-        fan_start(gain_fan, 2 * n_fs)
+        row_fan[0]()
+        gain_fan[0]()
 
     def token_grads():
-        fan_ready(row_fan, n_tp)
+        row_fan[1]().wait_recv()
         gain_l = gain_here()
 
         @pl.loop(0, CORES * half // LANES)
@@ -1222,7 +1193,7 @@
             value = value - v_tokens[at, :].astype(jnp.float32) * scale
             v_out[at, :] = value.astype(jnp.bfloat16)
 
-        pltpu.make_async_copy(v_out, o_tokens, out_sem.at[3, 0]).start()
+        pltpu.make_async_copy(v_out, o_tokens, out_sem.at[3]).start()
 
     def own_loaded(i):
         source, target = ((tokens, v_tokens), (cot, v_cot))[i]
@@ -1231,9 +1202,9 @@
     def block_out(m, k):
         at = pl.ds(k * width, width)
         if m == 2:
-            return pltpu.make_async_copy(v_down.at[at, :], o_down.at[at, :], out_sem.at[m, k])
+            return pltpu.make_async_copy(v_down.at[at, :], o_down.at[at, :], out_sem.at[m])
         return pltpu.make_async_copy(
-            outs[m].at[:, at], (o_gate, o_up)[m].at[:, at], out_sem.at[m, k]
+            outs[m].at[:, at], (o_gate, o_up)[m].at[:, at], out_sem.at[m]
         )
 
     def strip_squares(m, k):
@@ -1282,7 +1253,7 @@
         spread_arrival(m, k).wait_recv()
         block_out(m, k).start()
 
-    gain_copy = pltpu.make_async_copy(gain_in, gain_load, out_sem.at[3, 1])
+    gain_copy = pltpu.make_async_copy(gain_in, gain_load, out_sem.at[4])
     gain_copy.start()
     for a in range(2):
         loaded(a).start()
@@ -1371,25 +1342,25 @@
     normed_inner(1)
     for k in range(kb):
         strip_squares(2, k)
-    fan_start(tall_fan, 2 * n_fs)
+    tall_fan[0]()
     for k in range(kb):
         strip_squares(0, k)
     third(1, 0)
     strip_squares(1, 0)
     third(1, 1)
     strip_squares(1, 1)
-    fan_start(wide_fan, n_tp)
+    wide_fan[0]()
     normed_last()
     whole_block(2, 0)
     whole_block(2, 1)
     token_sums()
-    fan_ready(wide_fan, n_tp)
+    wide_fan[1]().wait_recv()
     v_half[...] = summed(wide_all, n_tp)
     wide_cross().start()
     v_wide[:, pl.ds(pl.multiple_of(r * strip, strip), strip)] = v_half[...]
-    fan_ready(tall_fan, 2 * n_fs)
+    tall_fan[1]().wait_recv()
     v_tall[...] = summed(tall_all, 2 * n_fs)
-    tall_out = pltpu.make_async_copy(v_tall, o_tall_sq, out_sem.at[4, 1])
+    tall_out = pltpu.make_async_copy(v_tall, o_tall_sq, out_sem.at[6])
     tall_out.start()
     token_grads()
     whole_block(0, 0)
@@ -1402,8 +1373,8 @@
     normed_sent()
     inv_send().wait_send()
     last_send().wait_send()
-    fan_sent(row_fan, n_tp)
-    fan_sent(wide_fan, n_tp)
+    row_fan[1]().wait_send()
+    wide_fan[1]().wait_send()
     for m in range(3):
         pairs_sent(m)
         swaps_sent(m)
@@ -1414,25 +1385,24 @@
                 deliver(m, k).wait_send()
 
     whole_block(1, 0)
-    fan_ready(gain_fan, 2 * n_fs)
+    gain_fan[1]().wait_recv()
     gain_sum[...] = summed(gain_all, 2 * n_fs)
-    gain_out = pltpu.make_async_copy(gain_sum, o_gain, out_sem.at[4, 0])
+    gain_out = pltpu.make_async_copy(gain_sum, o_gain, out_sem.at[5])
     gain_out.start()
     wide_cross_arrival().wait_recv()
-    wide_out = pltpu.make_async_copy(v_wide, o_wide_sq, out_sem.at[4, 2])
+    wide_out = pltpu.make_async_copy(v_wide, o_wide_sq, out_sem.at[7])
     wide_out.start()
     whole_block(1, 1)
     wide_cross().wait_send()
-    fan_sent(gain_fan, 2 * n_fs)
-    fan_sent(tall_fan, 2 * n_fs)
+    gain_fan[1]().wait_send()
+    tall_fan[1]().wait_send()
     gain_out.wait()
     tall_out.wait()
     wide_out.wait()
-    pltpu.make_async_copy(v_out, o_tokens, out_sem.at[3, 0]).wait()
+    pltpu.make_async_copy(v_out, o_tokens, out_sem.at[3]).wait()
     for m in range(3):
         spreads_sent(m)
-        for k in range(kb):
-            block_out(m, k).wait()
+        pltpu.make_async_copy(outs[m], (o_gate, o_up, o_down)[m], out_sem.at[m]).wait()
 
 
 def layer(n_fs, n_tp, tokens, cot, w_gate, w_up, w_down, gain):
@@ -1513,7 +1483,7 @@
             dma((2, n_fs - 1, CORES, PARTS)),
             dma((2,)),
             dma((2,)),
-            dma((2, n_fs, CORES, PARTS)),
+            dma((2,)),
             dma((2,)),
             dma((2,)),
             dma((3, kb)),
@@ -1521,7 +1491,7 @@
             dma((3,)),
             dma((3, n_fs)),
             dma((3,)),
-            dma((3, n_fs, 2)),
+            dma((3,)),
             dma((3,)),
             dma((3,)),
             dma((3,)),
@@ -1539,15 +1509,15 @@
             dma((3,)),
             dma((3,)),
             dma((3, kb)),
-            dma((n_tp - 1,)),
-            dma((n_tp - 1,)),
-            dma((2 * n_fs - 1,)),
-            dma((2 * n_fs - 1,)),
-            dma((n_tp - 1,)),
-            dma((n_tp - 1,)),
-            dma((2 * n_fs - 1,)),
-            dma((2 * n_fs - 1,)),
-            dma((5, max(kb, 3))),
+            dma((1,)),
+            dma((1,)),
+            dma((1,)),
+            dma((1,)),
+            dma((1,)),
+            dma((1,)),
+            dma((1,)),
+            dma((1,)),
+            dma((8,)),
             f32(half, reach),
             f32(1, local),
             bf(model // LANES, LANES),
@@ -1563,8 +1533,42 @@
     )(tokens, cot, w_gate, w_up, w_down, gain)
 
 
+def widen_kernel(*refs):
+    g_gate, g_up, g_down, tokens, gain, wide_sq, tall_sq = refs[:7]
+    o_gate, o_up, o_down, o_tokens, o_gain, o_wide_sq, o_tall_sq = refs[7:]
+    o_gate[...] = g_gate[...].astype(jnp.float32)
+    o_up[...] = g_up[...].astype(jnp.float32)
+    o_down[...] = g_down[...].astype(jnp.float32)
+    o_tokens[...] = tokens[...]
+    o_gain[...] = gain[0, :]
+    o_wide_sq[...] = wide_sq[...]
+    o_tall_sq[...] = tall_sq[0, :]
+
+
+def widen(*arrays):
+    shapes = [a.shape for a in arrays]
+
+    def split(shape):
+        return pl.BlockSpec((shape[0] // STEPS, shape[1]), lambda i: (i, 0))
+
+    def whole(shape):
+        return pl.BlockSpec(shape, lambda i: (0,) * len(shape))
+
+    outs = shapes[:4] + [shapes[4][1:], shapes[5], shapes[6][1:]]
+    kinds = [jnp.float32] * 3 + [arrays[3].dtype] + [jnp.float32] * 3
+    return pl.pallas_call(
+        widen_kernel,
+        grid=(STEPS,),
+        out_shape=[jax.ShapeDtypeStruct(s, k) for s, k in zip(outs, kinds)],
+        in_specs=[split(s) for s in shapes[:4]] + [whole(s) for s in shapes[4:]],
+        out_specs=[split(s) for s in outs[:4]] + [whole(s) for s in outs[4:]],
+        compiler_params=pltpu.CompilerParams(dimension_semantics=("arbitrary",)),
+        name="widen",
+    )(*arrays)
+
+
 def by_chip(tokens, norm_gain, w_gate, w_up, w_down, cotangent):
-    s_gate, s_up, s_down, grad_tokens, grad_gain, gate_up_sq, down_sq = layer(
+    found = layer(
         lax.axis_size("fs"),
         lax.axis_size("tp"),
         tokens,
@@ -1574,8 +1578,8 @@
         w_down,
         norm_gain.reshape(-1, LANES),
     )
-    grad_gate, grad_up, grad_down = (s.astype(jnp.float32) for s in (s_gate, s_up, s_down))
-    return (grad_tokens, grad_gain[0], grad_gate, grad_up, grad_down, gate_up_sq, down_sq[0])
+    grad_gate, grad_up, grad_down, grad_tokens, grad_gain, gate_up_sq, down_sq = widen(*found)
+    return (grad_tokens, grad_gain, grad_gate, grad_up, grad_down, gate_up_sq, down_sq)
 
 
 def fits_chips(mesh):

time: 199 us -> 194 us (0.975)
  other arithmetic: 7.24 us -> 0 us
  Pallas kernels: 189 us -> 193 us
    convert_element_type x3 -> x0, other arithmetic: 6.62 us -> none  [by_chip(): s.astype(jnp.float32)]
    pallas_call x0 -> x1, Pallas kernels: none -> 5.1 us  [widen(): pl.pallas_call(widen_kernel, grid=(STEPS,), out_shape=[jax.ShapeDtypeStru...]
where the time goes in v5:
time: 194 us
  Pallas kernels  193 us (99%)
    pallas_call x1, Pallas kernels, layer(): pl.pallas_call(functools.partial(layer_kernel, n_fs, n_tp), out_shape=[ja...  188 us
    pallas_call x1, Pallas kernels, widen(): pl.pallas_call(widen_kernel, grid=(STEPS,), out_shape=[jax.ShapeDtypeStru...  5.1 us

profile of v5, /device:TPU:0, one launch (start us, length us, event | category | flops | bytes accessed | tf_op | source)
XLA Modules:
  0.0 193.9 jit_solution(4439179540347333188)
XLA Ops:
  0.6 188.0 %layer.1 = (bf16[512,1280]{1,0:T(8,128)(2,1)}, bf16[512,1280]{1,0:T(8,128)(2,1)}, bf16[1280,512]{1,0:T(8,128)(2,1)}, bf16[384,512]{1,0:T(8,128)(2,1)}, f32[1,512...) custom-call(bf16[384,512]{1,0:T(8,128)(2,1)} %refs_0_.1, bf16[384,512]{1,0:T(8,128)(2,1)} %refs_1_.1, ...), custom_call_target="tpu_custom_call" | custom-call | tf_op jit(solution)/shard_map/layer/pallas_call | solution.py:1431
  188.6 5.1 %widen.1 = (f32[512,1280]{1,0:T(8,128)}, f32[512,1280]{1,0:T(8,128)}, f32[1280,512]{1,0:T(8,128)}, bf16[384,512]{1,0:T(8,128)(2,1)}, f32[512]{0:T(512)}, /*index=5*/f32[2,512]{1,0:T(2,128)}, f32[1280]{0:T(1024)}) custom-call(bf16[512,1280]{1,0:T(8,128)(2,1)} %get-tuple-element.21.refs_0_, bf16[512,1280]{1,0:T(8,128)(2,1)} %get-tuple-element.22.refs_1_, ...), custom_call_target="tpu_custom_call" | custom-call | tf_op jit(solution)/shard_map/widen/pallas_call | solution.py:1559

commit v6 on v5

--- a/solution.py
+++ b/solution.py
@@ -485,8 +485,8 @@
 CORES = 2
 LANES = 128
 TILE = 256
-PARTS = 2
-STEPS = 2
+PARTS = 4
+STEPS = 4
 
 
 def line_next(z, n_fs, side):
@@ -1297,13 +1297,21 @@
         act_round(1, d)
     across_all(2)
     act_ready(1)
-    gradients(2, 0)
     for k in range(kb):
-        first(2, k)
+        gradient(2, False, 0, k)
+        pair(2, k, 0).start()
+        if k:
+            first(2, k - 1)
+        gradient(2, True, 0, k)
+    first(2, kb - 1)
     gradients(2, 1)
     weight_ready((2,))
     pl.loop(0, count // TILE)(backward)
     act_sent(0, True)
+
+    gradients(0, 0)
+    for k in range(kb):
+        first(0, k)
 
     @pl.loop(0, n_fs)
     def _(i):
@@ -1311,9 +1319,6 @@
         pull_back(band, 1 - y)
         over(band).start()
 
-    gradients(0, 0)
-    for k in range(kb):
-        first(0, k)
     gradients(1, 0)
     for k in range(kb):
         first(1, k)
@@ -1533,36 +1538,68 @@
     )(tokens, cot, w_gate, w_up, w_down, gain)
 
 
-def widen_kernel(*refs):
-    g_gate, g_up, g_down, tokens, gain, wide_sq, tall_sq = refs[:7]
-    o_gate, o_up, o_down, o_tokens, o_gain, o_wide_sq, o_tall_sq = refs[7:]
-    o_gate[...] = g_gate[...].astype(jnp.float32)
-    o_up[...] = g_up[...].astype(jnp.float32)
-    o_down[...] = g_down[...].astype(jnp.float32)
-    o_tokens[...] = tokens[...]
-    o_gain[...] = gain[0, :]
-    o_wide_sq[...] = wide_sq[...]
-    o_tall_sq[...] = tall_sq[0, :]
+def widen_kernel(n, *refs):
+    sources, targets = refs[:n], refs[n : 2 * n]
+    narrow, wide = refs[2 * n : 3 * n], refs[3 * n : 3 * n + 3]
+    flat, load_sem, store_sem = refs[3 * n + 3 : -2], *refs[-2:]
+
+    def rows_of(i, step):
+        size = sources[i].shape[0] // STEPS
+        return pl.ds(step * size, size)
+
+    def load(i, step):
+        at = rows_of(i, step)
+        return pltpu.make_async_copy(sources[i].at[at], narrow[i].at[at], load_sem.at[i, step])
+
+    def store(i, step):
+        at = rows_of(i, step)
+        return pltpu.make_async_copy(wide[i].at[at], targets[i].at[at], store_sem.at[i, step])
+
+    def load_whole(i):
+        return pltpu.make_async_copy(sources[i], narrow[i], load_sem.at[i, 0])
+
+    def store_whole(i):
+        source = {4: flat[0], 6: flat[1]}.get(i, narrow[i])
+        return pltpu.make_async_copy(source, targets[i], store_sem.at[i, 0])
+
+    for i in range(3, n):
+        load_whole(i).start()
+    for step in range(STEPS):
+        for i in range(3):
+            load(i, step).start()
+    for i in range(3, n):
+        load_whole(i).wait()
+        if i in (4, 6):
+            flat[(i - 4) // 2][...] = narrow[i][0, :]
+        store_whole(i).start()
+    for step in range(STEPS):
+        for i in range(3):
+            load(i, step).wait()
+            at = rows_of(i, step)
+            wide[i][at] = narrow[i][at].astype(jnp.float32)
+            store(i, step).start()
+    for step in range(STEPS):
+        for i in range(3):
+            store(i, step).wait()
+    for i in range(3, n):
+        store_whole(i).wait()
 
 
 def widen(*arrays):
-    shapes = [a.shape for a in arrays]
-
-    def split(shape):
-        return pl.BlockSpec((shape[0] // STEPS, shape[1]), lambda i: (i, 0))
-
-    def whole(shape):
-        return pl.BlockSpec(shape, lambda i: (0,) * len(shape))
-
-    outs = shapes[:4] + [shapes[4][1:], shapes[5], shapes[6][1:]]
-    kinds = [jnp.float32] * 3 + [arrays[3].dtype] + [jnp.float32] * 3
+    n = len(arrays)
+    hbm = pl.BlockSpec(memory_space=pl.ANY)
+    shapes = [a.shape[1:] if a.shape[0] == 1 else a.shape for a in arrays]
+    kinds = [jnp.float32] * 3 + [a.dtype for a in arrays[3:]]
+    dma = pltpu.SemaphoreType.DMA
     return pl.pallas_call(
-        widen_kernel,
-        grid=(STEPS,),
-        out_shape=[jax.ShapeDtypeStruct(s, k) for s, k in zip(outs, kinds)],
-        in_specs=[split(s) for s in shapes[:4]] + [whole(s) for s in shapes[4:]],
-        out_specs=[split(s) for s in outs[:4]] + [whole(s) for s in outs[4:]],
-        compiler_params=pltpu.CompilerParams(dimension_semantics=("arbitrary",)),
+        functools.partial(widen_kernel, n),
+        out_shape=[jax.ShapeDtypeStruct(s, k) for s, k in zip(shapes, kinds)],
+        in_specs=[hbm] * n,
+        out_specs=[hbm] * n,
+        scratch_shapes=[pltpu.VMEM(a.shape, a.dtype) for a in arrays]
+        + [pltpu.VMEM(a.shape, jnp.float32) for a in arrays[:3]]
+        + [pltpu.VMEM(s, jnp.float32) for s in (shapes[4], shapes[6])]
+        + [dma((n, STEPS)), dma((n, STEPS))],
         name="widen",
     )(*arrays)
 

time: 194 us -> 192 us (0.990)
  Pallas kernels: 193 us -> 191 us
where the time goes in v6:
time: 192 us
  Pallas kernels  191 us (99%)
    pallas_call x1, Pallas kernels, layer(): pl.pallas_call(functools.partial(layer_kernel, n_fs, n_tp), out_shape=[ja...  186 us
    pallas_call x1, Pallas kernels, widen(): pl.pallas_call(functools.partial(widen_kernel, n), out_shape=[jax.ShapeDt...  4.78 us

profile of v6, /device:TPU:0, one launch (start us, length us, event | category | flops | bytes accessed | tf_op | source)
XLA Modules:
  0.0 191.8 jit_solution(6328154111400244581)
XLA Ops:
  0.6 186.2 %layer.1 = (bf16[512,1280]{1,0:T(8,128)(2,1)}, bf16[512,1280]{1,0:T(8,128)(2,1)}, bf16[1280,512]{1,0:T(8,128)(2,1)}, bf16[384,512]{1,0:T(8,128)(2,1)}, f32[1,512...) custom-call(bf16[384,512]{1,0:T(8,128)(2,1)} %refs_0_.1, bf16[384,512]{1,0:T(8,128)(2,1)} %refs_1_.1, ...), custom_call_target="tpu_custom_call" | custom-call | tf_op jit(solution)/shard_map/layer/pallas_call | solution.py:1436
  186.9 4.8 %widen.1 = (f32[512,1280]{1,0:T(8,128)}, f32[512,1280]{1,0:T(8,128)}, f32[1280,512]{1,0:T(8,128)}, bf16[384,512]{1,0:T(8,128)(2,1)}, f32[512]{0:T(512)}, /*index=5*/f32[2,512]{1,0:T(2,128)}, f32[1280]{0:T(1024)}) custom-call(bf16[512,1280]{1,0:T(8,128)(2,1)} %get-tuple-element.21.refs_0_, bf16[512,1280]{1,0:T(8,128)(2,1)} %get-tuple-element.22.refs_1_, ...), custom_call_target="tpu_custom_call" | custom-call | tf_op jit(solution)/shard_map/widen/pallas_call | solution.py:1594

commit v7 on v6

--- a/solution.py
+++ b/solution.py
@@ -510,7 +510,7 @@
     (y_send, y_recv, d_send, d_recv, n_send, n_recv, own_sem) = refs[79:86]
     (row_send, row_recv, gain_send, gain_recv) = refs[86:90]
     (wide_send, wide_recv, tall_send, tall_recv, out_sem, total, gain_sum) = refs[90:97]
-    gain_load, gain, v_wide, v_tall, v_half = refs[97:]
+    gain_load, gain, v_wide, v_tall, v_half, relay_sem = refs[97:]
     r, z, t = lax.axis_index("rep"), lax.axis_index("fs"), lax.axis_index("tp")
     y, c = lax.div(t, CORES), lax.rem(t, CORES)
     acts, weights = (tokens, cot), (w_gate, w_up, w_down)
@@ -527,13 +527,46 @@
     beside = {"tp": (1 - y) * CORES + c}
     owner = lax.div(z, kb)
 
-    peers = [partner, across]
-    peers += [{"tp": (1 - y) * CORES + h} for h in range(CORES)]
-    for j in range(1, n_fs):
-        for h in range(CORES):
-            peers.append({"fs": lax.rem(z + j, n_fs), "tp": y * CORES + h})
-        peers.append({"rep": 1 - r, "fs": lax.rem(z + j, n_fs)})
-    greet(peers)
+    ends = jnp.logical_or(z == 0, z == n_fs - 1)
+
+    def beyond(side):
+        return {"fs": z + 1 if side == 0 else z - 1}
+
+    barrier = pltpu.get_barrier_semaphore()
+    close = [partner, across] + [{"tp": (1 - y) * CORES + h} for h in range(CORES)]
+    for peer in close:
+        pl.semaphore_signal(barrier, inc=1, device_id=peer, device_id_type=MESH)
+    for side in range(2):
+
+        @pl.when(line_next(z, n_fs, side))
+        def _():
+            for h in range(CORES):
+                peer = {**beyond(side), "tp": y * CORES + h}
+                pl.semaphore_signal(barrier, inc=1, device_id=peer, device_id_type=MESH)
+
+    pl.semaphore_wait(barrier, jnp.where(ends, len(close) + CORES, len(close) + 2 * CORES))
+
+    def tell(side):
+        pl.semaphore_signal(
+            relay_sem.at[side], inc=1, device_id=beyond(side), device_id_type=MESH
+        )
+
+    for side in range(2):
+
+        @pl.when(z == 0 if side == 0 else z == n_fs - 1)
+        def _():
+            tell(side)
+
+    def greet_far():
+        for side in range(2):
+
+            @pl.when(line_next(z, n_fs, 1 - side))
+            def _():
+                pl.semaphore_wait(relay_sem.at[side], 1)
+
+                @pl.when(line_next(z, n_fs, side))
+                def _():
+                    tell(side)
 
     def own_act(a, h):
         return acts[a].at[pl.ds(pl.multiple_of(h * half, half), half), :]
@@ -1269,6 +1302,7 @@
     for i in range(2):
         own_loaded(i).start()
     act_round(0, 1)
+    greet_far()
     act_round(0, 2)
     weight_start(0)
     weight_start(1)
@@ -1530,6 +1564,7 @@
             f32(2, rows),
             f32(1, hidden),
             f32(2, strip),
+            pltpu.SemaphoreType.REGULAR((2,)),
         ],
         compiler_params=pltpu.CompilerParams(
             collective_id=4, has_side_effects=True, vmem_limit_bytes=67043328

time: 192 us -> 191 us (level)
  no operation moved by 1% of the time
where the time goes in v7:
time: 191 us
  Pallas kernels  191 us (100%)
    pallas_call x1, Pallas kernels, layer(): pl.pallas_call(functools.partial(layer_kernel, n_fs, n_tp), out_shape=[ja...  186 us
    pallas_call x1, Pallas kernels, widen(): pl.pallas_call(functools.partial(widen_kernel, n), out_shape=[jax.ShapeDt...  4.78 us

profile of v7, /device:TPU:0, one launch (start us, length us, event | category | flops | bytes accessed | tf_op | source)
XLA Modules:
  0.0 191.3 jit_solution(17539977174811565904)
XLA Ops:
  0.6 185.7 %layer.1 = (bf16[512,1280]{1,0:T(8,128)(2,1)}, bf16[512,1280]{1,0:T(8,128)(2,1)}, bf16[1280,512]{1,0:T(8,128)(2,1)}, bf16[384,512]{1,0:T(8,128)(2,1)}, f32[1,512...) custom-call(bf16[384,512]{1,0:T(8,128)(2,1)} %refs_0_.1, bf16[384,512]{1,0:T(8,128)(2,1)} %refs_1_.1, ...), custom_call_target="tpu_custom_call" | custom-call | tf_op jit(solution)/shard_map/layer/pallas_call | solution.py:1470
  186.4 4.8 %widen.1 = (f32[512,1280]{1,0:T(8,128)}, f32[512,1280]{1,0:T(8,128)}, f32[1280,512]{1,0:T(8,128)}, bf16[384,512]{1,0:T(8,128)(2,1)}, f32[512]{0:T(512)}, /*index=5*/f32[2,512]{1,0:T(2,128)}, f32[1280]{0:T(1024)}) custom-call(bf16[512,1280]{1,0:T(8,128)(2,1)} %get-tuple-element.21.refs_0_, bf16[512,1280]{1,0:T(8,128)(2,1)} %get-tuple-element.22.refs_1_, ...), custom_call_target="tpu_custom_call" | custom-call | tf_op jit(solution)/shard_map/widen/pallas_call | solution.py:1629

commit v8 on v7

--- a/solution.py
+++ b/solution.py
@@ -1314,6 +1314,7 @@
     act_round(1, 1)
     weight_all(1)
     across_all(0)
+    weight_start(2)
     gain_copy.wait()
     for i in range(model // LANES):
         gain[:, i * LANES : (i + 1) * LANES] = gain_load[i : i + 1, :].astype(jnp.float32)
@@ -1321,7 +1322,6 @@
     pl.loop(0, count // LANES)(normalize)
     inv_send().start()
     v_inv[own_rows(c), :] = inv_all[band_rows(z), :]
-    weight_start(2)
     across_all(1)
     act_round(1, 2)
     weight_ready((0, 1))

time: 191 us -> 191 us (level)
  no operation moved by 1% of the time
where the time goes in v8:
time: 191 us
  Pallas kernels  190 us (99%)
    pallas_call x1, Pallas kernels, layer(): pl.pallas_call(functools.partial(layer_kernel, n_fs, n_tp), out_shape=[ja...  186 us
    pallas_call x1, Pallas kernels, widen(): pl.pallas_call(functools.partial(widen_kernel, n), out_shape=[jax.ShapeDt...  4.78 us

profile of v8, /device:TPU:0, one launch (start us, length us, event | category | flops | bytes accessed | tf_op | source)
XLA Modules:
  0.0 191.1 jit_solution(11028683984923962655)
XLA Ops:
  0.6 185.5 %layer.1 = (bf16[512,1280]{1,0:T(8,128)(2,1)}, bf16[512,1280]{1,0:T(8,128)(2,1)}, bf16[1280,512]{1,0:T(8,128)(2,1)}, bf16[384,512]{1,0:T(8,128)(2,1)}, f32[1,512...) custom-call(bf16[384,512]{1,0:T(8,128)(2,1)} %refs_0_.1, bf16[384,512]{1,0:T(8,128)(2,1)} %refs_1_.1, ...), custom_call_target="tpu_custom_call" | custom-call | tf_op jit(solution)/shard_map/layer/pallas_call | solution.py:1470
  186.2 4.8 %widen.1 = (f32[512,1280]{1,0:T(8,128)}, f32[512,1280]{1,0:T(8,128)}, f32[1280,512]{1,0:T(8,128)}, bf16[384,512]{1,0:T(8,128)(2,1)}, f32[512]{0:T(512)}, /*index=5*/f32[2,512]{1,0:T(2,128)}, f32[1280]{0:T(1024)}) custom-call(bf16[512,1280]{1,0:T(8,128)(2,1)} %get-tuple-element.21.refs_0_, bf16[512,1280]{1,0:T(8,128)(2,1)} %get-tuple-element.22.refs_1_, ...), custom_call_target="tpu_custom_call" | custom-call | tf_op jit(solution)/shard_map/widen/pallas_call | solution.py:1629
